TPU v7x, 256 devices: a whole 4x4x8 slice. The times are simulated.
256 devices in a mesh: kv: 32 (over z, y), tp: 8 (over x, core).
Axes of the slice: x: 4, y: 4, z: 8, core: 2. Of those that a mesh axis runs over, the one named last changes fastest.
Arguments:
- residual_in: bfloat16 [256, 2048], P(None, ('kv', 'tp')), may hold values from -14 to 14
- delta_state: float32 [256, 32, 128, 128], P('kv', 'tp'), may hold values from -1 to 1
- norm_gain_first: float32 [2048], P('kv'), may hold values from 0.1 to 1.9
- gate_first: bfloat16 [2048, 5632], P('kv', 'tp'), may hold values from -0.125 to 0.125
- up_first: bfloat16 [2048, 5632], P('kv', 'tp'), may hold values from -0.125 to 0.125
- down_first: bfloat16 [5632, 2048], P('tp', 'kv'), may hold values from -0.15625 to 0.15625
- norm_gain_mixer: float32 [2048], P('kv'), may hold values from 0.1 to 1.9
- query_weight: bfloat16 [2048, 2048], P('kv', 'tp'), may hold values from -0.125 to 0.125
- key_weight: bfloat16 [2048, 2048], P('kv', 'tp'), may hold values from -0.125 to 0.125
- value_weight: bfloat16 [2048, 4096], P('kv', 'tp'), may hold values from -0.125 to 0.125
- output_gate_weight: bfloat16 [2048, 4096], P('kv', 'tp'), may hold values from -0.125 to 0.125
- beta_weight: bfloat16 [2048, 32], P('kv'), may hold values from -0.125 to 0.125
- decay_weight: bfloat16 [2048, 32], P('kv'), may hold values from -0.125 to 0.125
- decay_rate: float32 [32], P('tp'), may hold values from -2.3 to 1.1
- decay_bias: float32 [32], P('tp'), may hold values from -1 to 1
- head_gain: float32 [128], replicated, may hold values from 0.1 to 1.9
- out_weight: bfloat16 [4096, 2048], P('tp', 'kv'), may hold values from -0.125 to 0.125
- norm_gain_second: float32 [2048], P('kv'), may hold values from 0.1 to 1.9
- gate_second: bfloat16 [2048, 5632], P('kv', 'tp'), may hold values from -0.125 to 0.125
- up_second: bfloat16 [2048, 5632], P('kv', 'tp'), may hold values from -0.125 to 0.125
- down_second: bfloat16 [5632, 2048], P('tp', 'kv'), may hold values from -0.15625 to 0.15625
Outputs:
- residual_out: bfloat16 [256, 2048], P(None, ('kv', 'tp'))
- delta_state_out: float32 [256, 32, 128, 128], P('kv', 'tp')
All inputs are finite; a program needn't handle non-finite values.
Results may differ from a plain program's by a relative error of at most 0.03.
Values may be sent and summed in bfloat16 or wider, within the bound.
A program may use at most 64 MiB of HBM per device.

v0:
```python
import jax
import jax.numpy as jnp
from jax import lax
from jax.sharding import PartitionSpec as P

D = 2048


epsilon = 1e-06


def in_blocks(value, dim, size):
    before, after = (value.shape[:dim], value.shape[dim + 1 :])
    return jnp.moveaxis(value.reshape(*before, size, -1, *after), dim, 0)


def summed_on_arrival(value, axis, dim):
    blocks = in_blocks(value, dim, lax.axis_size(axis))
    arrived = lax.all_to_all(blocks, axis, split_axis=0, concat_axis=0, tiled=True)
    return arrived.astype(jnp.float32).sum(axis=0)


def side_by_side(arrays, axis, dim, along):
    columns = [a.reshape(*a.shape[:along], -1) for a in arrays]
    both = jnp.concatenate(columns, axis=along)
    result, at, outs = (summed_on_arrival(both, axis, dim), 0, [])
    for a, column in zip(arrays, columns):
        piece = result[..., at : at + column.shape[along]]
        outs.append(piece.reshape(*piece.shape[:along], *a.shape[along:]))
        at += column.shape[along]
    return tuple(outs)


def joined_along(blocks, dim):
    dims = list(blocks.shape[1:])
    dims[dim] *= blocks.shape[0]
    return jnp.moveaxis(blocks, 0, dim).reshape(dims)


def from_everyone(value, axis):
    copies = jnp.broadcast_to(value, (lax.axis_size(axis), *value.shape))
    return lax.all_to_all(copies, axis, split_axis=0, concat_axis=0, tiled=True)


def collect(value, axis, dim):
    return joined_along(from_everyone(value, axis), dim)


def activate(summed, square_sums, hidden_cols):
    rowscale = lax.rsqrt(square_sums / D + epsilon)[:, None]
    gate_act = summed[:, :hidden_cols] * rowscale
    up_act = summed[:, hidden_cols:] * rowscale
    return (jax.nn.silu(gate_act) * up_act).astype(jnp.bfloat16)


def feed_forward(residual, norm_gain, gate_weight, up_weight, down_weight, finish):
    as_float = residual.astype(jnp.float32)
    squares = jnp.sum(as_float * as_float, axis=1)
    scaled = (as_float * norm_gain).astype(jnp.bfloat16)
    joined = jnp.concatenate([gate_weight, up_weight], axis=1)
    partial_value = jnp.dot(scaled, joined, preferred_element_type=jnp.float32)
    hidden_cols = gate_weight.shape[1]
    summed, square_sums = side_by_side(
        (partial_value.astype(jnp.bfloat16), squares.astype(jnp.bfloat16)), "kv", 0, 1
    )
    hidden = activate(summed, square_sums, hidden_cols)
    projected = jnp.dot(
        collect(hidden, "kv", 0), down_weight, preferred_element_type=jnp.float32
    ).astype(jnp.bfloat16)
    if finish:
        col_count = residual.shape[1] // lax.axis_size("tp")
        own_cols = lax.dynamic_slice_in_dim(
            as_float, lax.axis_index("tp") * col_count, col_count, 1
        )
        branch = summed_on_arrival(projected, "tp", 1)
        return (own_cols + 0.5 * branch).astype(jnp.bfloat16)
    branch = lax.psum(projected, "tp").astype(jnp.float32)
    return (as_float + 0.5 * branch).astype(jnp.bfloat16)


def unit_heads(projected, head_size):
    activated = jax.nn.silu(projected).reshape(projected.shape[0], -1, head_size)
    return activated * lax.rsqrt(jnp.sum(activated * activated, axis=-1, keepdims=True) + epsilon)


def delta_step(old_state, key_rows, queries, values, beta_gate, decay_gate):
    faded_state = old_state * decay_gate[:, :, None, None]
    predicted = jnp.einsum("rhab,rha->rhb", faded_state, key_rows, precision=lax.Precision.HIGHEST)
    correction = beta_gate[:, :, None] * (values - predicted)
    updated = faded_state + key_rows[:, :, :, None] * correction[:, :, None, :]
    reading = jnp.einsum("rhab,rha->rhb", updated, queries, precision=lax.Precision.HIGHEST)
    return (updated, reading)


def token_mixer(
    residual,
    norm_gain,
    query_weight,
    key_weight,
    value_weight,
    output_gate_weight,
    beta_weight,
    decay_weight,
    decay_rate,
    decay_bias,
    head_gain,
    out_weight,
    old_state,
):
    as_float = residual.astype(jnp.float32)
    squares = jnp.sum(as_float * as_float, axis=1)
    scaled = (as_float * norm_gain).astype(jnp.bfloat16)
    joined = jnp.concatenate([query_weight, key_weight, value_weight, output_gate_weight], axis=1)
    partial_value = jnp.dot(scaled, joined, preferred_element_type=jnp.float32)
    heads_dev = decay_rate.shape[0]
    head_start = lax.axis_index("tp") * heads_dev
    gate_cols = jnp.concatenate(
        [
            lax.dynamic_slice_in_dim(beta_weight, head_start, heads_dev, 1),
            lax.dynamic_slice_in_dim(decay_weight, head_start, heads_dev, 1),
        ],
        axis=1,
    )
    gate_part = jnp.dot(scaled, gate_cols, preferred_element_type=jnp.float32)
    row_count = old_state.shape[0]
    summed, gate_summed, square_sums = side_by_side(
        (
            partial_value.astype(jnp.bfloat16),
            gate_part.astype(jnp.bfloat16),
            squares.astype(jnp.bfloat16),
        ),
        "kv",
        0,
        1,
    )
    rowscale = lax.rsqrt(square_sums / D + epsilon)[:, None]
    summed = summed * rowscale
    gate_summed = gate_summed * rowscale
    head_size = old_state.shape[2]
    key_cols = query_weight.shape[1]
    value_cols = value_weight.shape[1]
    repeat_count = heads_dev // (key_cols // head_size)
    queries = jnp.repeat(
        unit_heads(summed[:, :key_cols], head_size) * head_size ** (-0.5), repeat_count, axis=1
    )
    key_rows = jnp.repeat(
        unit_heads(summed[:, key_cols : 2 * key_cols], head_size), repeat_count, axis=1
    )
    values = jax.nn.silu(summed[:, 2 * key_cols : 2 * key_cols + value_cols]).reshape(
        row_count, heads_dev, head_size
    )
    out_gate = jax.nn.silu(summed[:, 2 * key_cols + value_cols :]).reshape(
        row_count, heads_dev, head_size
    )
    beta_gate = jax.nn.sigmoid(gate_summed[:, :heads_dev])
    decay_gate = jnp.exp(
        -jnp.exp(decay_rate)[None, :]
        * jax.nn.softplus(gate_summed[:, heads_dev:] + decay_bias[None, :])
    )
    new_state, reading = delta_step(old_state, key_rows, queries, values, beta_gate, decay_gate)
    normed = reading * lax.rsqrt(jnp.mean(reading * reading, axis=-1, keepdims=True) + epsilon)
    normed = (
        (normed * head_gain * out_gate)
        .reshape(row_count, heads_dev * head_size)
        .astype(jnp.bfloat16)
    )
    projected = jnp.dot(
        collect(normed, "kv", 0), out_weight, preferred_element_type=jnp.float32
    ).astype(jnp.bfloat16)
    branch = lax.psum(projected, "tp").astype(jnp.float32)
    return ((as_float + branch).astype(jnp.bfloat16), new_state)


def body(
    residual_in,
    delta_state,
    norm_gain_first,
    gate_first,
    up_first,
    down_first,
    norm_gain_mixer,
    query_weight,
    key_weight,
    value_weight,
    output_gate_weight,
    beta_weight,
    decay_weight,
    decay_rate,
    decay_bias,
    head_gain,
    out_weight,
    norm_gain_second,
    gate_second,
    up_second,
    down_second,
):
    columns = lax.all_gather(residual_in, "tp", axis=1, tiled=True)
    after_first = feed_forward(columns, norm_gain_first, gate_first, up_first, down_first, False)
    after_mixer, new_state = token_mixer(
        after_first,
        norm_gain_mixer,
        query_weight,
        key_weight,
        value_weight,
        output_gate_weight,
        beta_weight,
        decay_weight,
        decay_rate,
        decay_bias,
        head_gain,
        out_weight,
        delta_state,
    )
    residual_out = feed_forward(
        after_mixer, norm_gain_second, gate_second, up_second, down_second, True
    )
    return (residual_out, new_state)


def solution(mesh):
    placed = (
        P(None, ("kv", "tp")),
        P("kv", "tp", None, None),
        P("kv"),
        P("kv", "tp"),
        P("kv", "tp"),
        P("tp", "kv"),
        P("kv"),
        P("kv", "tp"),
        P("kv", "tp"),
        P("kv", "tp"),
        P("kv", "tp"),
        P("kv", None),
        P("kv", None),
        P("tp"),
        P("tp"),
        P(),
        P("tp", "kv"),
        P("kv"),
        P("kv", "tp"),
        P("kv", "tp"),
        P("tp", "kv"),
    )
    return jax.shard_map(
        body,
        mesh=mesh,
        in_specs=placed,
        out_specs=(P(None, ("kv", "tp")), P("kv", "tp", None, None)),
        check_vma=False,
    )
```

profile of v0, /device:TPU:1, one launch (start us, length us, event | category | flops | bytes accessed | tf_op | source)
XLA Modules:
  0.0 230.6 jit_solution(4892839816095156955)
XLA Ops:
  0.6 16.2 %all_gather.3 = bf16[256,64]{0,1:T(8,128)(2,1)S(1)} all-gather(bf16[256,8]{0,1:T(8,128)(2,1)} %param.21), channel_id=1, replica_groups=mesh['kv'=32,'tp'=8] {'tp'}, dimensions={1}, use_global_device_ids=true | all-gather | bytes 36864 | tf_op jit(solution)/shard_map/all_gather | solution.py:197
  16.9 0.2 convert_element_type.152
  17.1 1.4 fusion
  18.7 31.4 %all_to_all.35 = bf16[32,8,1409]{2,1,0:T(8,128)(2,1)S(1)} all-to-all(bf16[32,8,1409]{2,1,0:T(8,128)(2,1)S(1)} %pad_maximum_fusion), channel_id=1, replica_groups=mesh['kv'=32,'tp'=8] {'kv'}, dimensions={0} | all-to-all | bytes 1442816 | tf_op jit(solution)/shard_map/all_to_all | solution.py:19
  50.1 0.1 convert_reduce_fusion.2
  50.2 0.1 fusion.57
  50.3 0.1 fusion.36
  50.4 0.8 broadcast_in_dim.10
  51.2 5.6 %all-to-all-start.1 = ((bf16[32,8,704]{2,1,0:T(8,128)(2,1)}), bf16[32,8,704]{2,1,0:T(8,128)(2,1)S(1)}, u32[]{:S(2)}, u32[]{:S(2)}) async-start(bf16[32,8,704]{2,1,0:T(8,128)(2,1)} %broadcast_in_dim.10), calls=%async_computation.1 | async-start | bytes 786432 | tf_op jit(solution)/shard_map/all_to_all | solution.py:42
  56.8 0.7 constant_dynamic-slice_fusion
  57.5 12.1 %all-to-all-done.1 = bf16[32,8,704]{2,1,0:T(8,128)(2,1)S(1)} async-done(((bf16[32,8,704]{2,1,0:T(8,128)(2,1)}), bf16[32,8,704]{2,1,0:T(8,128)(2,1)S(1)}, u32[]{:S(2)}, u32[]{:S(2)}) %all-to-all-start.1) | async-done | bytes 360480 | tf_op jit(solution)/shard_map/all_to_all | solution.py:42
  69.6 0.2 convolution_convert_fusion.5
  69.8 23.5 %psum.14 = bf16[256,64]{0,1:T(8,128)(2,1)S(1)} all-reduce(bf16[256,64]{0,1:T(8,128)(2,1)S(1)} %convolution_convert_fusion.5), channel_id=1, replica_groups=mesh['kv'=32,'tp'=8] {'tp'}, use_global_device_ids=true, to_apply=%region_2.3 | all-reduce | flops 16384 | bytes 65536 | tf_op jit(solution)/shard_map/psum | solution.py:77
  93.4 0.2 convolution_convert_fusion.6
  93.6 0.1 copy.64
  93.7 0.2 convert_element_type.153
  94.0 0.5 fusion.1
  94.5 1.1 concatenate.39
  95.6 4.6 %all-to-all-start.2 = ((bf16[32,8,1545]{2,1,0:T(8,128)(2,1)}), bf16[32,8,1545]{2,1,0:T(8,128)(2,1)S(1)}, u32[]{:S(2)}, u32[]{:S(2)}) async-start(bf16[32,8,1545]{2,1,0:T(8,128)(2,1)} %concatenate.39), calls=%async_computation.2 | async-start | bytes 1703936 | tf_op jit(solution)/shard_map/all_to_all | solution.py:19
  100.3 19.5 %all-to-all-done.2 = bf16[32,8,1545]{2,1,0:T(8,128)(2,1)S(1)} async-done(((bf16[32,8,1545]{2,1,0:T(8,128)(2,1)}), bf16[32,8,1545]{2,1,0:T(8,128)(2,1)S(1)}, u32[]{:S(2)}, u32[]{:S(2)}) %all-to-all-start.2) | async-done | bytes 791072 | tf_op jit(solution)/shard_map/all_to_all | solution.py:19
  119.7 0.1 convert_reduce_fusion
  119.8 0.2 fusion.54
  120.0 0.1 slice_multiply_fusion.7
  120.1 0.1 slice_multiply_fusion
  120.2 0.1 fusion.43
  120.3 0.1 add_divide_fusion
  120.4 0.1 copy.56
  120.5 0.1 fusion.44
  120.6 2.0 fusion.3
  122.7 0.7 multiply_add_fusion
  123.6 1.2 copy-done.2
  124.8 1.9 fusion.67
  126.7 0.1 fusion.38
  126.8 0.1 fusion.46
  126.9 17.3 %all_to_all.36 = bf16[32,8,512]{2,1,0:T(8,128)(2,1)S(1)} all-to-all(bf16[32,8,512]{2,1,0:T(8,128)(2,1)S(1)} %broadcast_in_dim.13), channel_id=1, replica_groups=mesh['kv'=32,'tp'=8] {'kv'}, dimensions={0} | all-to-all | bytes 524288 | tf_op jit(solution)/shard_map/all_to_all | solution.py:42
  144.2 0.2 convolution_convert_fusion.3
  144.4 26.0 %psum.15 = bf16[256,64]{0,1:T(8,128)(2,1)S(1)} all-reduce(bf16[256,64]{0,1:T(8,128)(2,1)S(1)} %convolution_convert_fusion.3), channel_id=1, replica_groups=mesh['kv'=32,'tp'=8] {'tp'}, use_global_device_ids=true, to_apply=%region_8.9 | all-reduce | flops 16384 | bytes 65536 | tf_op jit(solution)/shard_map/psum | solution.py:170
  170.4 0.2 convert_element_type.154
  170.7 0.5 fusion.2
  171.2 22.8 %all_to_all.37 = bf16[32,8,1409]{2,1,0:T(8,128)(2,1)S(1)} all-to-all(bf16[32,8,1409]{2,1,0:T(8,128)(2,1)S(1)} %pad_maximum_fusion.1), channel_id=1, replica_groups=mesh['kv'=32,'tp'=8] {'kv'}, dimensions={0} | all-to-all | bytes 1442816 | tf_op jit(solution)/shard_map/all_to_all | solution.py:19
  194.0 0.1 convert_reduce_fusion.1
  194.1 0.1 fusion.51
  194.2 0.1 fusion.34
  194.4 18.7 %all_to_all.38 = bf16[32,8,704]{2,1,0:T(8,128)(2,1)S(1)} all-to-all(bf16[32,8,704]{2,1,0:T(8,128)(2,1)S(1)} %broadcast_in_dim.14), channel_id=1, replica_groups=mesh['kv'=32,'tp'=8] {'kv'}, dimensions={0} | all-to-all | bytes 720896 | tf_op jit(solution)/shard_map/all_to_all | solution.py:42
  213.1 0.9 fusion.5
  214.0 11.3 %all-to-all-start.6 = ((bf16[8,256,8]{1,2,0:T(8,128)(2,1)}), bf16[8,256,8]{1,2,0:T(8,128)(2,1)S(1)}, u32[]{:S(2)}, u32[]{:S(2)}) async-start(bf16[8,256,8]{1,2,0:T(8,128)(2,1)} %fusion.5), calls=%async_computation.6 | async-start | bytes 65536 | tf_op jit(solution)/shard_map/all_to_all | solution.py:19
  225.2 4.7 %all-to-all-done.6 = bf16[8,256,8]{1,2,0:T(8,128)(2,1)S(1)} async-done(((bf16[8,256,8]{1,2,0:T(8,128)(2,1)}), bf16[8,256,8]{1,2,0:T(8,128)(2,1)S(1)}, u32[]{:S(2)}, u32[]{:S(2)}) %all-to-all-start.6) | async-done | bytes 32800 | tf_op jit(solution)/shard_map/all_to_all | solution.py:19
  230.0 0.6 add_convert_fusion
  (49 shorter events, 0.5 us)
Async XLA Ops:
  0.6 68.9 %copy-start = (bf16[704,64]{0,1:T(8,128)(2,1)S(1)}, bf16[704,64]{0,1:T(8,128)(2,1)}, u32[]{:S(2)}) copy-start(bf16[704,64]{0,1:T(8,128)(2,1)} %param.26) | copy-start | bytes 270340
  18.6 74.8 %copy-start.11 = (f32[64]{0:T(128)S(1)}, f32[64]{0:T(128)}, u32[]{:S(2)}) copy-start(f32[64]{0:T(128)} %param.27) | copy-start | bytes 772
  18.6 75.4 %copy-start.6 = (bf16[64,512]{1,0:T(8,128)(2,1)S(1)}, bf16[64,512]{1,0:T(8,128)(2,1)}, u32[]{:S(2)}) copy-start(bf16[64,512]{1,0:T(8,128)(2,1)} %param.31) | copy-start | bytes 196612
  18.6 75.4 %copy-start.7 = (bf16[64,512]{1,0:T(8,128)(2,1)S(1)}, bf16[64,512]{1,0:T(8,128)(2,1)}, u32[]{:S(2)}) copy-start(bf16[64,512]{1,0:T(8,128)(2,1)} %param.30) | copy-start | bytes 196612
  18.6 75.4 %copy-start.9 = (bf16[64,256]{1,0:T(8,128)(2,1)S(1)}, bf16[64,256]{1,0:T(8,128)(2,1)}, u32[]{:S(2)}) copy-start(bf16[64,256]{1,0:T(8,128)(2,1)} %param.29) | copy-start | bytes 98308
  18.7 75.4 %copy-start.10 = (bf16[64,256]{1,0:T(8,128)(2,1)S(1)}, bf16[64,256]{1,0:T(8,128)(2,1)}, u32[]{:S(2)}) copy-start(bf16[64,256]{1,0:T(8,128)(2,1)} %param.28) | copy-start | bytes 98308
  51.2 18.4 %all-to-all-start.1 = ((bf16[32,8,704]{2,1,0:T(8,128)(2,1)}), bf16[32,8,704]{2,1,0:T(8,128)(2,1)S(1)}, u32[]{:S(2)}, u32[]{:S(2)}) async-start(bf16[32,8,704]{2,1,0:T(8,128)(2,1)} %broadcast_in_dim.10), calls=%async_computation.1 | async-start | bytes 786432 | tf_op jit(solution)/shard_map/all_to_all | solution.py:42
  94.0 6.2 %copy-start.15 = (f32[4]{0:T(128)S(1)}, f32[4]{0:T(128)}, u32[]{:S(2)}) copy-start(f32[4]{0:T(128)} %param.34) | copy-start | bytes 52
  94.5 25.8 %copy-start.14 = (f32[4]{0:T(128)S(1)}, f32[4]{0:T(128)}, u32[]{:S(2)}) copy-start(f32[4]{0:T(128)} %param.35) | copy-start | bytes 52
  94.5 26.1 %copy-start.1 = (f32[8,4,128,128]{3,2,1,0:T(8,128)S(1)}, f32[8,4,128,128]{3,2,1,0:T(8,128)}, u32[]{:S(2)}) copy-start(f32[8,4,128,128]{3,2,1,0:T(8,128)} %param.22) | copy-start | bytes 6291460
  95.6 24.1 %all-to-all-start.2 = ((bf16[32,8,1545]{2,1,0:T(8,128)(2,1)}), bf16[32,8,1545]{2,1,0:T(8,128)(2,1)S(1)}, u32[]{:S(2)}, u32[]{:S(2)}) async-start(bf16[32,8,1545]{2,1,0:T(8,128)(2,1)} %concatenate.39), calls=%async_computation.2 | async-start | bytes 1703936 | tf_op jit(solution)/shard_map/all_to_all | solution.py:19
  123.5 1.3 copy-start.2
  123.5 3.3 %copy-start.13 = (f32[128]{0:T(128)S(1)}, f32[128]{0:T(128)}, u32[]{:S(2)}) copy-start(f32[128]{0:T(128)} %param.36) | copy-start | bytes 1540
  123.5 20.7 %copy-start.8 = (bf16[512,64]{0,1:T(8,128)(2,1)S(1)}, bf16[512,64]{0,1:T(8,128)(2,1)}, u32[]{:S(2)}) copy-start(bf16[512,64]{0,1:T(8,128)(2,1)} %param.37) | copy-start | bytes 196612
  123.5 47.1 %copy-start.3 = (bf16[64,704]{1,0:T(8,128)(2,1)S(1)}, bf16[64,704]{1,0:T(8,128)(2,1)}, u32[]{:S(2)}) copy-start(bf16[64,704]{1,0:T(8,128)(2,1)} %param.40) | copy-start | bytes 270340
  123.5 47.1 %copy-start.4 = (bf16[64,704]{1,0:T(8,128)(2,1)S(1)}, bf16[64,704]{1,0:T(8,128)(2,1)}, u32[]{:S(2)}) copy-start(bf16[64,704]{1,0:T(8,128)(2,1)} %param.39) | copy-start | bytes 270340
  123.5 47.1 %copy-start.12 = (f32[64]{0:T(128)S(1)}, f32[64]{0:T(128)}, u32[]{:S(2)}) copy-start(f32[64]{0:T(128)} %param.38) | copy-start | bytes 772
  171.2 41.9 %copy-start.5 = (bf16[704,64]{0,1:T(8,128)(2,1)S(1)}, bf16[704,64]{0,1:T(8,128)(2,1)}, u32[]{:S(2)}) copy-start(bf16[704,64]{0,1:T(8,128)(2,1)} %param.41) | copy-start | bytes 270340
  214.0 16.0 %all-to-all-start.6 = ((bf16[8,256,8]{1,2,0:T(8,128)(2,1)}), bf16[8,256,8]{1,2,0:T(8,128)(2,1)S(1)}, u32[]{:S(2)}, u32[]{:S(2)}) async-start(bf16[8,256,8]{1,2,0:T(8,128)(2,1)} %fusion.5), calls=%async_computation.6 | async-start | bytes 65536 | tf_op jit(solution)/shard_map/all_to_all | solution.py:19
where the time goes:
time: 231 us
  blocking collectives  156 us (68%)
  waiting for transfers between devices  36.3 us (16%)
  starting transfers between devices  21.5 us (9%)
  matrix products  7.71 us (3%)
  local copies, waits for them, and re-layouts  4.91 us (2%)
  other arithmetic  3.23 us (1%)
    all_to_all x2, blocking collectives, summed_on_arrival(): lax.all_to_all(blocks, axis, split_axis=0, concat_axis=0, tiled=True)  54.2 us
    all_to_all x2, blocking collectives, from_everyone(): return lax.all_to_all(copies, axis, split_axis=0, concat_axis=0, tiled=True)  36 us
    psum x1, blocking collectives, token_mixer(): branch = lax.psum(projected, 'tp').astype(jnp.float32)  26 us
    all_to_all x2, waiting for transfers between devices, summed_on_arrival(): lax.all_to_all(blocks, axis, split_axis=0, concat_axis=0, tiled=True)  24.2 us
    psum x1, blocking collectives, feed_forward(): branch = lax.psum(projected, 'tp').astype(jnp.float32)  23.5 us
    all_gather x1, blocking collectives, body(): columns = lax.all_gather(residual_in, 'tp', axis=1, tiled=True)  16.2 us
    all_to_all x2, starting transfers between devices, summed_on_arrival(): lax.all_to_all(blocks, axis, split_axis=0, concat_axis=0, tiled=True)  15.9 us
    all_to_all x1, waiting for transfers between devices, from_everyone(): return lax.all_to_all(copies, axis, split_axis=0, concat_axis=0, tiled=True)  12.1 us
  transfers between devices with their start and end apart: 3, of which 3 were waited for; matrix products, arithmetic and copies ran while one was open for 0% of the time, Pallas kernels for 0%

commit v1 on v0

v1 whole, which is shorter than its diff:
```python
import jax
import jax.numpy as jnp
from jax import lax
from jax.experimental import pallas as pl
from jax.experimental.pallas import tpu as pltpu
from jax.sharding import PartitionSpec as P

MESH = pl.DeviceIdType.MESH
BF, F32 = jnp.bfloat16, jnp.float32
D, EPS = 2048, 1e-6
NZ, NY, NT = 8, 4, 8
PLANE = NY * NT
KV = NZ * NY
ROWS = 256
KEEP, GROUP = 22, 24
HID = NZ * KEEP
PAD = NZ * GROUP
HEAD = 128

X1, X2, X3, RS1, RS2, AG1, AG2, PR1, PR2, PR3, MIX, EXT, NRM = range(13)
GU1, GU2, DD, MW, WO, GN = range(13, 19)
N_SEM = 19


def dot(a, b, ca, cb):
    return lax.dot_general(a, b, (((ca,), (cb,)), ((), ())), preferred_element_type=F32)


def iota(shape, dim):
    return lax.broadcasted_iota(jnp.int32, shape, dim)


def one_hot(cond):
    return jnp.where(cond, 1.0, 0.0).astype(BF)


def silu(v):
    return v / (1.0 + jnp.exp(-v))


def kernel(
    res, state, gain1, gain2, gain3, gate1, up1, down1, gate2, up2, down2,
    wq, wk, wv, wg, wbeta, wdecay, rate, bias, hgain, wo,
    out, k_out, c_out, d_out,
    s_buf, s_sem, send, recv,
    gu_src, gu_rcv, dd_src, dd_rcv, mw_src, mw_rcv, wo_src, wo_rcv, gn,
    a_w, d_w, g_col,
    xg, rs_src, rs_rcv, hg, pr_src, pr_rcv, m_src, m_rcv, e_src, e_rcv, n_src, n_rcv,
):
    kv = lax.axis_index("kv")
    t = lax.axis_index("tp")
    z, y = lax.div(kv, NY), lax.rem(kv, NY)
    me = y * NT + t

    barrier = pltpu.get_barrier_semaphore()

    def hello_plane(o, c):
        p = lax.rem(me + o, PLANE)
        peer = (z * NY + lax.div(p, NT), lax.rem(p, NT))
        pl.semaphore_signal(barrier, inc=1, device_id=peer, device_id_type=MESH)
        return c

    def hello_kv(o, c):
        pz = lax.rem(z + 1 + lax.div(o, NY), NZ)
        peer = (pz * NY + lax.rem(o, NY), t)
        pl.semaphore_signal(barrier, inc=1, device_id=peer, device_id_type=MESH)
        return c

    lax.fori_loop(1, PLANE, hello_plane, 0)
    lax.fori_loop(0, KV - NY, hello_kv, 0)

    fetch = pltpu.make_async_copy(state, s_buf, s_sem)
    fetch.start()

    def put(src, dst, k, peer):
        pltpu.make_async_remote_copy(
            src_ref=src, dst_ref=dst, send_sem=send.at[k], recv_sem=recv.at[k], device_id=peer, device_id_type=MESH
        ).start()

    def arrived(part, k):
        pltpu.make_async_copy(part, part, recv.at[k]).wait()

    def left(part, k):
        pltpu.make_async_copy(part, part, send.at[k]).wait()

    def to_y(src, dst, k, each):
        def step(o, c):
            p = lax.rem(y + o, NY)
            put(src.at[p] if each else src.at[y], dst.at[y], k, (z * NY + p, t))
            return c

        lax.fori_loop(1, NY, step, 0)
        if each:
            dst[y] = src[y]

    def to_z(src, dst, k, each):
        def step(o, c):
            p = lax.rem(z + o, NZ)
            put(src.at[p] if each else src.at[z], dst.at[z], k, (p * NY + y, t))
            return c

        lax.fori_loop(1, NZ, step, 0)
        if each:
            dst[z] = src[z]

    def to_plane(src, dst, k, each):
        def step(o, c):
            p = lax.rem(me + o, PLANE)
            put(src.at[p] if each else src.at[me], dst.at[me], k, (z * NY + lax.div(p, NT), lax.rem(p, NT)))
            return c

        lax.fori_loop(1, PLANE, step, 0)
        if each:
            dst[me] = src[me]

    eye8 = one_hot(iota((8, 8), 0) == iota((8, 8), 1))
    low = one_hot(iota((64, 128), 0) == iota((64, 128), 1))
    high = one_hot(iota((64, 128), 0) + 64 == iota((64, 128), 1))
    own0 = dot(eye8, res[...], 1, 1)
    xg[0, me] = own0.astype(BF)

    def gate_up(i, gate, up):
        both = dot(gate[...], low, 0, 0) + dot(up[...], high, 0, 0)
        gu_src[i] = both.astype(BF).reshape(NY, HID, 128)

    gate_up(0, gate1, up1)
    eye64 = iota((64, 64), 0) == iota((64, 64), 1)
    gn[y, 0:8] = jnp.broadcast_to(gain1[...], (8, 64))
    gn[y, 8:16] = jnp.broadcast_to(gain2[...], (8, 64))
    gn[y, 16:24] = jnp.broadcast_to(gain3[...], (8, 64))

    pl.semaphore_wait(barrier, PLANE - 1 + KV - NY)

    to_plane(xg.at[0], xg.at[0], X1, False)
    to_y(gn, gn, GN, False)
    to_y(gu_src.at[0], gu_rcv.at[0], GU1, True)

    dd = dot(down1[...], low, 1, 0) + dot(down2[...], high, 1, 0)
    dd_src[...] = dd.astype(BF).reshape(NY, HID, 128)
    to_y(dd_src, dd_rcv, DD, True)

    sel_b = one_hot((iota((32, 128), 0) == iota((32, 128), 1) + 4 * t) & (iota((32, 128), 1) < 4))
    sel_d = one_hot((iota((32, 128), 0) == iota((32, 128), 1) - 4 + 4 * t) & (iota((32, 128), 1) >= 4) & (iota((32, 128), 1) < 8))
    extra = (dot(wbeta[...], sel_b, 1, 0) + dot(wdecay[...], sel_d, 1, 0)).astype(BF)
    blocks = []
    for w in (wq, wk, wv, wg):
        blocks += [(w, j) for j in range(w.shape[1] // 128)]
    for p in range(NY):
        for b in range(3):
            w, j = blocks[3 * p + b]
            mw_src[p, b] = w[:, 128 * j : 128 * (j + 1)]
        mw_src[p, 3] = extra
    to_y(mw_src, mw_rcv, MW, True)

    wo_t = dot(one_hot(eye64), wo[...], 1, 1).astype(BF)
    for p in range(NY):
        wo_src[p] = wo_t[:, 128 * p : 128 * (p + 1)]
    to_y(wo_src, wo_rcv, WO, True)

    gate_up(1, gate2, up2)
    to_y(gu_src.at[1], gu_rcv.at[1], GU2, True)

    def spread(r, c):
        group = jnp.zeros_like(r)
        for i in range(1, NZ):
            group = group + jnp.where(r >= GROUP * i, 1, 0)
        return one_hot((c == r - (GROUP - KEEP) * group) & (r - GROUP * group < KEEP))

    pick = spread(iota((PAD, HID), 0), iota((PAD, HID), 1))
    pick_t = spread(iota((HID, PAD), 1), iota((HID, PAD), 0))
    lane = iota((PAD, 128), 1)

    def make_gate_up(i):
        parts = [dot(pick, gu_rcv[i, p], 1, 0) for p in range(NY)]
        for h in range(2):
            a, b = parts[2 * h], parts[2 * h + 1]
            a_w[i, 0:PAD, 128 * h : 128 * (h + 1)] = jnp.where(lane < 64, a, pltpu.roll(b, 64, 1)).astype(BF)
            a_w[i, PAD : 2 * PAD, 128 * h : 128 * (h + 1)] = jnp.where(lane < 64, pltpu.roll(a, 64, 1), b).astype(BF)

    def make_down():
        for p in range(NY):
            both = dot(dd_rcv[p], pick_t, 0, 0).astype(BF)
            d_w[0, 64 * p : 64 * (p + 1)] = both[0:64]
            d_w[1, 64 * p : 64 * (p + 1)] = both[64:128]

    arrived(gn.at[pl.ds(0, NY - 1)], GN)
    for i in range(3):
        for p in range(NY):
            row = gn[p, 8 * i : 8 * i + 1]
            col = jnp.sum(jnp.where(eye64, jnp.broadcast_to(row, (64, 64)), 0.0), axis=1, keepdims=True)
            g_col[i, 64 * p : 64 * (p + 1)] = jnp.broadcast_to(col, (64, 128))
    arrived(gu_rcv.at[0, pl.ds(0, NY - 1)], GU1)
    make_gate_up(0)

    def gathered(i, k):
        arrived(xg.at[i, pl.ds(0, PLANE - 1)], k)
        x = xg[i].astype(F32).reshape(ROWS, ROWS)
        gain = jnp.concatenate([g_col[i], g_col[i]], axis=1)
        return x * x, (x * gain).astype(BF)

    def half_ffn(i, ix, kx, krs, kag, kpr, prepare):
        squares, scaled = gathered(ix, kx)
        part = dot(a_w[i], scaled, 1, 0)
        total = jnp.sum(squares, axis=0, keepdims=True)
        coarse = total.astype(BF).astype(F32)
        row = iota((NZ, GROUP, ROWS), 1)
        gate = part[0:PAD].reshape(NZ, GROUP, ROWS)
        up = part[PAD : 2 * PAD].reshape(NZ, GROUP, ROWS)
        gate = jnp.where(row == KEEP, coarse.reshape(1, 1, ROWS), gate)
        gate = jnp.where(row == KEEP + 1, (total - coarse).reshape(1, 1, ROWS), gate)
        both = jnp.concatenate([gate, up], axis=1).astype(BF)
        rs_src[i] = both.reshape(NZ, 2 * GROUP // 8, 8, ROWS)
        to_z(rs_src.at[i], rs_rcv.at[i], krs, True)
        prepare()
        arrived(rs_rcv.at[i, pl.ds(0, NZ - 1)], krs)
        both = jnp.sum(rs_rcv[i].astype(F32), axis=0).reshape(2 * GROUP, ROWS)
        gate, up = both[0:GROUP], both[GROUP:]
        scale = lax.rsqrt((gate[KEEP : KEEP + 1] + gate[KEEP + 1 : KEEP + 2]) / D + EPS)
        hidden = silu(gate * scale) * (up * scale)
        hidden = jnp.where(iota((GROUP, ROWS), 0) < KEEP, hidden, 0.0)
        hg[i, z] = hidden.reshape(GROUP // 8, 8, ROWS).astype(BF)
        to_z(hg.at[i], hg.at[i], kag, False)
        arrived(hg.at[i, pl.ds(0, NZ - 1)], kag)
        h = hg[i].astype(F32).reshape(PAD, ROWS).astype(BF)
        return summed(dot(d_w[i], h, 1, 0), 2 * i, kpr)

    def summed(part, j, k):
        pr_src[j] = part.reshape(PLANE, 8, ROWS).astype(BF)
        to_plane(pr_src.at[j], pr_rcv.at[j], k, True)
        arrived(pr_rcv.at[j, pl.ds(0, PLANE - 1)], k)
        return jnp.sum(pr_rcv[j].astype(F32), axis=0)

    def first_prepare():
        arrived(dd_rcv.at[pl.ds(0, NY - 1)], DD)
        make_down()
        arrived(mw_rcv.at[pl.ds(0, NY - 1)], MW)
        arrived(wo_rcv.at[pl.ds(0, NY - 1)], WO)
        arrived(gu_rcv.at[1, pl.ds(0, NY - 1)], GU2)
        make_gate_up(1)

    branch = half_ffn(0, 0, X1, RS1, AG1, PR1, first_prepare)
    own1 = (own0 + 0.5 * branch).astype(BF)
    xg[1, me] = own1
    to_plane(xg.at[1], xg.at[1], X2, False)

    squares, scaled = gathered(1, X2)
    coarse = squares.astype(BF)
    fine = (squares - coarse.astype(F32)).astype(BF)
    at8 = one_hot(iota((ROWS, 128), 1) == 8)
    for b in range(4):
        w = mw_rcv[:, b].reshape(ROWS, 128)
        part = dot(scaled, w, 0, 0)
        if b < 3:
            m_src[:, :, 128 * b : 128 * (b + 1)] = part.reshape(KV, 8, 128).astype(BF)
        else:
            part = part + dot(coarse, at8, 0, 0) + dot(fine, at8, 0, 0)
            e_src[...] = part.reshape(KV, 8, 128)

    def mix_step(o, c):
        p = lax.rem(kv + o, KV)
        put(m_src.at[p], m_rcv.at[kv], MIX, (p, t))
        return c

    lax.fori_loop(1, KV, mix_step, 0)

    def ext_step(o, c):
        p = lax.rem(z + o, NZ) * NY + y
        put(e_src.at[p], e_rcv.at[z], EXT, (p, t))
        return c

    lax.fori_loop(1, NZ, ext_step, 0)
    m_rcv[kv] = m_src[kv]
    e_rcv[z] = e_src[kv]
    fetch.wait()
    arrived(e_rcv.at[pl.ds(0, NZ - 1)], EXT)
    arrived(m_rcv.at[pl.ds(0, KV - 1)], MIX)

    ext = jnp.sum(e_rcv[...], axis=0)
    rowscale = lax.rsqrt(ext[:, 8:9] / D + EPS)
    quarters = [jnp.zeros((8, 384), F32) for _ in range(NY)]
    for s in range(KV):
        quarters[s % NY] = quarters[s % NY] + m_rcv[s].astype(F32)
    heads = []
    for p in range(NY):
        for b in range(3):
            heads.append(quarters[p][:, 128 * b : 128 * (b + 1)] * rowscale)

    def unit(v):
        a = silu(v)
        return a * lax.rsqrt(jnp.sum(a * a, axis=-1, keepdims=True) + EPS)

    q = [unit(heads[m]) * HEAD**-0.5 for m in range(2)]
    k = [unit(heads[2 + m]) for m in range(2)]
    q_t = [jnp.transpose(v) for v in q]
    k_t = [jnp.transpose(v) for v in k]
    kq = [jnp.sum(k[m] * q[m], axis=-1, keepdims=True) for m in range(2)]
    ext = ext * rowscale
    for h in range(4):
        m = h // 2
        val = silu(heads[4 + h])
        gate = silu(heads[8 + h])
        pre = ext[:, h : h + 1]
        beta = 1.0 / (1.0 + jnp.exp(-pre))
        pre = ext[:, 4 + h : 5 + h] + bias[0, h]
        soft = jnp.maximum(pre, 0.0) + jnp.log1p(jnp.exp(-jnp.abs(pre)))
        decay = jnp.exp(-jnp.exp(jnp.full((8, 1), rate[0, h], F32)) * soft)
        by_k, by_q = [], []
        for r in range(8):
            s = s_buf[r, h]
            by_k.append(jnp.sum(s * k_t[m][:, r : r + 1], axis=0, keepdims=True))
            by_q.append(jnp.sum(s * q_t[m][:, r : r + 1], axis=0, keepdims=True))
        by_k = jnp.concatenate(by_k, axis=0)
        by_q = jnp.concatenate(by_q, axis=0)
        corr = beta * (val - decay * by_k)
        reading = decay * by_q + kq[m] * corr
        norm = lax.rsqrt(jnp.mean(reading * reading, axis=-1, keepdims=True) + EPS)
        n_src[h] = (reading * norm * hgain[...] * gate).astype(BF)
        c_out[:, h] = corr
        d_out[:, h : h + 1] = decay
    for m in range(2):
        k_out[:, m] = k[m]

    def norm_step(o, c):
        p = lax.rem(kv + o, KV)
        put(n_src.at[lax.rem(p, NY)], n_rcv.at[kv], NRM, (p, t))
        return c

    lax.fori_loop(1, KV, norm_step, 0)
    n_rcv[kv] = n_src[y]
    arrived(n_rcv.at[pl.ds(0, KV - 1)], NRM)
    normed = n_rcv[...].astype(F32).reshape(ROWS, HEAD).astype(BF)
    branch = summed(dot(wo_rcv[...].reshape(ROWS, HEAD), normed, 1, 1), 1, PR2)
    own2 = (own1.astype(F32) + branch).astype(BF)
    xg[2, me] = own2
    to_plane(xg.at[2], xg.at[2], X3, False)

    branch = half_ffn(1, 2, X3, RS2, AG2, PR3, lambda: None)
    own3 = (own2.astype(F32) + 0.5 * branch).astype(BF)
    out[...] = dot(own3, eye8, 0, 0).astype(BF)

    for i, kk in enumerate((X1, X2, X3)):
        left(xg.at[i, pl.ds(0, PLANE - 1)], kk)
    for i, kk in enumerate((PR1, PR2, PR3)):
        left(pr_src.at[i, pl.ds(0, PLANE - 1)], kk)
    for i, kk in enumerate((RS1, RS2)):
        left(rs_src.at[i, pl.ds(0, NZ - 1)], kk)
    for i, kk in enumerate((AG1, AG2)):
        left(hg.at[i, pl.ds(0, NZ - 1)], kk)
    for i, kk in enumerate((GU1, GU2)):
        left(gu_src.at[i, pl.ds(0, NY - 1)], kk)
    left(dd_src.at[pl.ds(0, NY - 1)], DD)
    left(mw_src.at[pl.ds(0, NY - 1)], MW)
    left(wo_src.at[pl.ds(0, NY - 1)], WO)
    left(gn.at[pl.ds(0, NY - 1)], GN)
    left(m_src.at[pl.ds(0, KV - 1)], MIX)
    left(e_src.at[pl.ds(0, NZ - 1)], EXT)
    left(n_rcv.at[pl.ds(0, KV - 1)], NRM)


def layer(res, state, gain1, gate1, up1, down1, gain2, wq, wk, wv, wg, wbeta, wdecay, rate, bias, hgain, wo, gain3, gate2, up2, down2):
    vmem = pl.BlockSpec(memory_space=pltpu.VMEM)
    smem = pl.BlockSpec(memory_space=pltpu.SMEM)
    specs = [vmem, pl.BlockSpec(memory_space=pl.ANY)] + [vmem] * 15 + [smem] * 2 + [vmem] * 2
    out, k, corr, decay = pl.pallas_call(
        kernel,
        out_shape=(
            jax.ShapeDtypeStruct((ROWS, 8), BF),
            jax.ShapeDtypeStruct((8, 2, HEAD), F32),
            jax.ShapeDtypeStruct((8, 4, HEAD), F32),
            jax.ShapeDtypeStruct((8, 4), F32),
        ),
        in_specs=specs,
        out_specs=(vmem,) * 4,
        scratch_shapes=[
            pltpu.VMEM((8, 4, HEAD, HEAD), F32),
            pltpu.SemaphoreType.DMA,
            pltpu.SemaphoreType.DMA((N_SEM,)),
            pltpu.SemaphoreType.DMA((N_SEM,)),
            pltpu.VMEM((2, NY, HID, 128), BF),
            pltpu.VMEM((2, NY, HID, 128), BF),
            pltpu.VMEM((NY, HID, 128), BF),
            pltpu.VMEM((NY, HID, 128), BF),
            pltpu.VMEM((NY, 4, 64, 128), BF),
            pltpu.VMEM((NY, 4, 64, 128), BF),
            pltpu.VMEM((NY, 64, 128), BF),
            pltpu.VMEM((NY, 64, 128), BF),
            pltpu.VMEM((NY, 24, 64), F32),
            pltpu.VMEM((2, 2 * PAD, ROWS), BF),
            pltpu.VMEM((2, ROWS, PAD), BF),
            pltpu.VMEM((3, ROWS, 128), F32),
            pltpu.VMEM((3, PLANE, 8, ROWS), BF),
            pltpu.VMEM((2, NZ, 2 * GROUP // 8, 8, ROWS), BF),
            pltpu.VMEM((2, NZ, 2 * GROUP // 8, 8, ROWS), BF),
            pltpu.VMEM((2, NZ, GROUP // 8, 8, ROWS), BF),
            pltpu.VMEM((3, PLANE, 8, ROWS), BF),
            pltpu.VMEM((3, PLANE, 8, ROWS), BF),
            pltpu.VMEM((KV, 8, 384), BF),
            pltpu.VMEM((KV, 8, 384), BF),
            pltpu.VMEM((KV, 8, 128), F32),
            pltpu.VMEM((NZ, 8, 128), F32),
            pltpu.VMEM((4, 8, HEAD), BF),
            pltpu.VMEM((KV, 8, HEAD), BF),
        ],
        compiler_params=pltpu.CompilerParams(collective_id=0, has_side_effects=True, vmem_limit_bytes=48 << 20),
    )(
        res, state, gain1[None], gain2[None], gain3[None], gate1, up1, down1, gate2, up2, down2,
        wq, wk, wv, wg, wbeta, wdecay, rate[None], bias[None], hgain[None], wo,
    )
    keys = jnp.repeat(k, 2, axis=1)
    return out, state * decay[:, :, None, None] + keys[:, :, :, None] * corr[:, :, None, :]


def solution(mesh):
    placed = (
        P(None, ("kv", "tp")),
        P("kv", "tp", None, None),
        P("kv"),
        P("kv", "tp"),
        P("kv", "tp"),
        P("tp", "kv"),
        P("kv"),
        P("kv", "tp"),
        P("kv", "tp"),
        P("kv", "tp"),
        P("kv", "tp"),
        P("kv", None),
        P("kv", None),
        P("tp"),
        P("tp"),
        P(),
        P("tp", "kv"),
        P("kv"),
        P("kv", "tp"),
        P("kv", "tp"),
        P("tp", "kv"),
    )
    return jax.shard_map(
        layer,
        mesh=mesh,
        in_specs=placed,
        out_specs=(P(None, ("kv", "tp")), P("kv", "tp", None, None)),
        check_vma=False,
    )
```

time: 231 us -> 111 us (0.48)
  blocking collectives: 156 us -> 0 us
  Pallas kernels: 0 us -> 89.1 us
  waiting for transfers between devices: 36.3 us -> 0 us
  starting transfers between devices: 21.5 us -> 0 us
  local copies, waits for them, and re-layouts: 4.91 us -> 18.4 us
  matrix products: 7.71 us -> 0 us
    all_to_all x4 -> x0, blocking collectives: 90.2 us -> none  [the longest x2 54.2 us: summed_on_arrival(): lax.all_to_all(blocks, axis, split_axis=0, concat_axis=0, tiled=True)]
    pallas_call x0 -> x1, Pallas kernels: none -> 89.1 us  [layer(): pl.pallas_call(kernel, out_shape=(jax.ShapeDtypeStruct((ROWS, 8), BF), ja...]
    psum x2 -> x0, blocking collectives: 49.5 us -> none  [the longest x1 26 us: token_mixer(): branch = lax.psum(projected, 'tp').astype(jnp.float32)]
    all_to_all x3 -> x0, waiting for transfers between devices: 36.3 us -> none  [the longest x2 24.2 us: summed_on_arrival(): lax.all_to_all(blocks, axis, split_axis=0, concat_axis=0, tiled=True)]
    all_to_all x3 -> x0, starting transfers between devices: 21.5 us -> none  [the longest x2 15.9 us: summed_on_arrival(): lax.all_to_all(blocks, axis, split_axis=0, concat_axis=0, tiled=True)]
    unnamed x32 -> x39, local copies, waits for them, and re-layouts: 1.34 us -> 18.4 us
    all_gather x1 -> x0, blocking collectives: 16.2 us -> none  [body(): columns = lax.all_gather(residual_in, 'tp', axis=1, tiled=True)]
    dot_general x9 -> x0, matrix products: 7.71 us -> none  [the longest x1 2 us: delta_step(): jnp.einsum('rhab,rha->rhb', faded_state, key_rows, precision=lax.Precisio...]
  transfers between devices with their start and end apart: 3 -> 0, of which waited for: 3 -> 0; matrix products, arithmetic and copies ran while one was open for 0% -> 0% of each run, Pallas kernels for 0% -> 0%
where the time goes in v1:
time: 111 us; the launch traced here: 110 us
  Pallas kernels  89.1 us (80%)
  local copies, waits for them, and re-layouts  18.4 us (17%)
  other arithmetic  1.72 us (2%)
    pallas_call x1, Pallas kernels, layer(): pl.pallas_call(kernel, out_shape=(jax.ShapeDtypeStruct((ROWS, 8), BF), ja...  89.1 us
    unnamed x39, local copies, waits for them, and re-layouts  18.4 us

profile of v1, /device:TPU:1, one launch (start us, length us, event | category | flops | bytes accessed | tf_op | source)
XLA Modules:
  0.0 110.0 jit_solution(15432018378907336050)
XLA Ops:
  0.6 0.8 copy.26.wbeta
  1.4 0.8 copy.27.wdecay
  2.2 0.8 copy.23.res
  3.0 1.0 copy.28.wo
  4.0 1.1 copy.24.down1
  5.0 1.1 copy.25.down2
  6.1 0.0 copy-start
  6.1 1.6 %copy-done = f32[8,4,128,128]{3,2,1,0:T(8,128)S(1)} copy-done((f32[8,4,128,128]{3,2,1,0:T(8,128)S(1)}, f32[8,4,128,128]{3,2,1,0:T(8,128)}, u32[]{:S(2)}) %copy-start) | copy-done | bytes 2097176
  7.7 0.0 copy-start.2
  7.7 0.9 copy-done.2
  8.6 0.0 copy-start.3
  8.6 0.9 copy-done.3
  9.5 0.0 copy-start.4
  9.5 0.9 copy-done.4
  10.4 0.0 copy-start.5
  10.4 0.9 copy-done.5
  11.3 0.0 copy-start.6
  11.3 0.8 copy-done.6
  12.1 0.0 copy-start.7
  12.1 0.8 copy-done.7
  13.0 0.0 copy-start.8
  13.0 0.8 copy-done.8
  13.7 0.0 copy-start.9
  13.7 0.8 copy-done.9
  14.5 0.0 copy-start.10
  14.5 0.7 copy-done.10
  15.1 0.0 copy-start.11
  15.1 0.7 copy-done.11
  15.8 0.0 copy-start.12
  15.8 0.7 copy-done.12
  16.4 0.0 copy-start.13
  16.4 0.7 copy-done.13
  17.1 0.0 copy-start.14
  17.1 0.7 copy-done.14
  17.8 0.0 copy-start.15
  17.8 0.7 copy-done.15
  18.4 0.0 copy-start.1
  18.4 89.1 %shard_map.212 = (bf16[256,8]{1,0:T(8,128)(2,1)S(1)}, f32[8,2,128]{2,1,0:T(2,128)S(1)}, f32[8,4,128]{2,1,0:T(4,128)S(1)}, f32[8,4]{1,0:T(8,128)S(1)}) custom-call(bf16[256,8]{1,0:T(8,128)(2,1)S(1)} %copy.23.res, f32[8,4,128,128]{3,2,1,0:T(8,128)S(1)} %copy-done, f32[1,64]{1,0:T(1,128)S(1)} %bitcast.7, f32[1,64]{1,0:T(1,128)S(1)} %bitcast.8, ...), custom_call_target="tpu_custom_call" | custom-call | tf_op jit(solution)/shard_map/pallas_call | solution.py:364
  107.6 0.7 copy.29
  108.2 0.0 copy-done.1
  108.2 1.7 %multiply_add_fusion = f32[8,4,128,128]{3,2,1,0:T(8,128)} fusion(f32[8,4,128,128]{3,2,1,0:T(8,128)S(1)} %copy-done.1, f32[8,4,128]{2,1,0:T(4,128)S(1)} %get-tuple-element.9, f32[8,4,128]{2,1,0:T(4,128)S(1)} %bitcast.13, f32[8,4]{1,0:T(8,128)S(1)} %get-tuple-element.7), kind=kLoop, calls=%fused_computation | loop fusion | flops 1572864 | bytes 4227200 | tf_op jit(solution)/shard_map/add | solution.py:410
  (1 shorter events, 0.0 us)
Async XLA Ops:
  6.1 1.6 %copy-start = (f32[8,4,128,128]{3,2,1,0:T(8,128)S(1)}, f32[8,4,128,128]{3,2,1,0:T(8,128)}, u32[]{:S(2)}) copy-start(f32[8,4,128,128]{3,2,1,0:T(8,128)} %state.1) | copy-start | bytes 6291460
  7.7 0.9 copy-start.2
  8.6 0.9 copy-start.3
  9.5 0.9 copy-start.4
  10.4 0.9 copy-start.5
  11.3 0.8 copy-start.6
  12.1 0.8 copy-start.7
  13.0 0.8 copy-start.8
  13.7 0.8 copy-start.9
  14.5 0.7 copy-start.10
  15.1 0.7 copy-start.11
  15.8 0.7 copy-start.12
  16.4 0.7 copy-start.13
  17.1 0.7 copy-start.14
  17.8 0.7 copy-start.15
  18.4 89.8 %copy-start.1 = (f32[8,4,128,128]{3,2,1,0:T(8,128)S(1)}, f32[8,4,128,128]{3,2,1,0:T(8,128)}, u32[]{:S(2)}) copy-start(f32[8,4,128,128]{3,2,1,0:T(8,128)} %state.1) | copy-start | bytes 6291460

commit v2 on v1

--- a/solution.py
+++ b/solution.py
@@ -20,6 +20,7 @@
 X1, X2, X3, RS1, RS2, AG1, AG2, PR1, PR2, PR3, MIX, EXT, NRM = range(13)
 GU1, GU2, DD, MW, WO, GN = range(13, 19)
 N_SEM = 19
+STATE_SPACE = pltpu.HBM
 
 
 def dot(a, b, ca, cb):
@@ -39,10 +40,12 @@
 
 
 def kernel(
-    res, state, gain1, gain2, gain3, gate1, up1, down1, gate2, up2, down2,
+    res_h, state, gain1_h, gain2_h, gain3_h, gate1_h, up1_h, down1_h, gate2_h, up2_h, down2_h,
+    wq_h, wk_h, wv_h, wg_h, wbeta_h, wdecay_h, rate_h, bias_h, hgain_h, wo_h,
+    out, state_out,
+    res, s_buf, gain1, gain2, gain3, gate1, up1, down1, gate2, up2, down2,
     wq, wk, wv, wg, wbeta, wdecay, rate, bias, hgain, wo,
-    out, k_out, c_out, d_out,
-    s_buf, s_sem, send, recv,
+    in_sem, out_sem, send, recv,
     gu_src, gu_rcv, dd_src, dd_rcv, mw_src, mw_rcv, wo_src, wo_rcv, gn,
     a_w, d_w, g_col,
     xg, rs_src, rs_rcv, hg, pr_src, pr_rcv, m_src, m_rcv, e_src, e_rcv, n_src, n_rcv,
@@ -69,8 +72,18 @@
     lax.fori_loop(1, PLANE, hello_plane, 0)
     lax.fori_loop(0, KV - NY, hello_kv, 0)
 
-    fetch = pltpu.make_async_copy(state, s_buf, s_sem)
-    fetch.start()
+    named = {}
+    for i, (src, dst) in enumerate((
+        (res_h, res), (gate1_h, gate1), (up1_h, up1), (gain1_h, gain1), (gain2_h, gain2), (gain3_h, gain3),
+        (down1_h, down1), (down2_h, down2), (wbeta_h, wbeta), (wdecay_h, wdecay), (wq_h, wq), (wk_h, wk), (wv_h, wv), (wg_h, wg),
+        (wo_h, wo), (gate2_h, gate2), (up2_h, up2), (rate_h, rate), (bias_h, bias), (hgain_h, hgain), (state, s_buf),
+    )):
+        named[id(dst)] = pltpu.make_async_copy(src, dst, in_sem.at[i])
+        named[id(dst)].start()
+
+    def ready(*refs):
+        for ref in refs:
+            named[id(ref)].wait()
 
     def put(src, dst, k, peer):
         pltpu.make_async_remote_copy(
@@ -113,17 +126,19 @@
         if each:
             dst[me] = src[me]
 
-    eye8 = one_hot(iota((8, 8), 0) == iota((8, 8), 1))
     low = one_hot(iota((64, 128), 0) == iota((64, 128), 1))
     high = one_hot(iota((64, 128), 0) + 64 == iota((64, 128), 1))
-    own0 = dot(eye8, res[...], 1, 1)
-    xg[0, me] = own0.astype(BF)
-
-    def gate_up(i, gate, up):
-        both = dot(gate[...], low, 0, 0) + dot(up[...], high, 0, 0)
-        gu_src[i] = both.astype(BF).reshape(NY, HID, 128)
-
-    gate_up(0, gate1, up1)
+    ready(res)
+    own0 = res[...].astype(F32)
+    xg[0, me] = res[...]
+
+    def beside(a, b):
+        ready(a, b)
+        both = dot(a[...], low, 0, 0) + dot(b[...], high, 0, 0)
+        return both.astype(BF).reshape(NY, HID, 128)
+
+    gu_src[0] = beside(gate1, up1)
+    ready(gain1, gain2, gain3)
     eye64 = iota((64, 64), 0) == iota((64, 64), 1)
     gn[y, 0:8] = jnp.broadcast_to(gain1[...], (8, 64))
     gn[y, 8:16] = jnp.broadcast_to(gain2[...], (8, 64))
@@ -135,13 +150,13 @@
     to_y(gn, gn, GN, False)
     to_y(gu_src.at[0], gu_rcv.at[0], GU1, True)
 
-    dd = dot(down1[...], low, 1, 0) + dot(down2[...], high, 1, 0)
-    dd_src[...] = dd.astype(BF).reshape(NY, HID, 128)
+    dd_src[...] = beside(down1, down2)
     to_y(dd_src, dd_rcv, DD, True)
 
     sel_b = one_hot((iota((32, 128), 0) == iota((32, 128), 1) + 4 * t) & (iota((32, 128), 1) < 4))
     sel_d = one_hot((iota((32, 128), 0) == iota((32, 128), 1) - 4 + 4 * t) & (iota((32, 128), 1) >= 4) & (iota((32, 128), 1) < 8))
-    extra = (dot(wbeta[...], sel_b, 1, 0) + dot(wdecay[...], sel_d, 1, 0)).astype(BF)
+    ready(wbeta, wdecay, wq, wk, wv, wg)
+    extra = (dot(wbeta[...], sel_b, 0, 0) + dot(wdecay[...], sel_d, 0, 0)).astype(BF)
     blocks = []
     for w in (wq, wk, wv, wg):
         blocks += [(w, j) for j in range(w.shape[1] // 128)]
@@ -152,12 +167,12 @@
         mw_src[p, 3] = extra
     to_y(mw_src, mw_rcv, MW, True)
 
-    wo_t = dot(one_hot(eye64), wo[...], 1, 1).astype(BF)
+    ready(wo)
     for p in range(NY):
-        wo_src[p] = wo_t[:, 128 * p : 128 * (p + 1)]
+        wo_src[p] = wo[:, 128 * p : 128 * (p + 1)]
     to_y(wo_src, wo_rcv, WO, True)
 
-    gate_up(1, gate2, up2)
+    gu_src[1] = beside(gate2, up2)
     to_y(gu_src.at[1], gu_rcv.at[1], GU2, True)
 
     def spread(r, c):
@@ -271,7 +286,7 @@
     lax.fori_loop(1, NZ, ext_step, 0)
     m_rcv[kv] = m_src[kv]
     e_rcv[z] = e_src[kv]
-    fetch.wait()
+    ready(s_buf, rate, bias, hgain)
     arrived(e_rcv.at[pl.ds(0, NZ - 1)], EXT)
     arrived(m_rcv.at[pl.ds(0, KV - 1)], MIX)
 
@@ -295,15 +310,16 @@
     k_t = [jnp.transpose(v) for v in k]
     kq = [jnp.sum(k[m] * q[m], axis=-1, keepdims=True) for m in range(2)]
     ext = ext * rowscale
+    new = []
     for h in range(4):
         m = h // 2
         val = silu(heads[4 + h])
         gate = silu(heads[8 + h])
         pre = ext[:, h : h + 1]
         beta = 1.0 / (1.0 + jnp.exp(-pre))
-        pre = ext[:, 4 + h : 5 + h] + bias[0, h]
+        pre = ext[:, 4 + h : 5 + h] + bias[:, h : h + 1]
         soft = jnp.maximum(pre, 0.0) + jnp.log1p(jnp.exp(-jnp.abs(pre)))
-        decay = jnp.exp(-jnp.exp(jnp.full((8, 1), rate[0, h], F32)) * soft)
+        decay = jnp.exp(-jnp.exp(rate[:, h : h + 1]) * soft)
         by_k, by_q = [], []
         for r in range(8):
             s = s_buf[r, h]
@@ -315,10 +331,7 @@
         reading = decay * by_q + kq[m] * corr
         norm = lax.rsqrt(jnp.mean(reading * reading, axis=-1, keepdims=True) + EPS)
         n_src[h] = (reading * norm * hgain[...] * gate).astype(BF)
-        c_out[:, h] = corr
-        d_out[:, h : h + 1] = decay
-    for m in range(2):
-        k_out[:, m] = k[m]
+        new.append((decay, corr))
 
     def norm_step(o, c):
         p = lax.rem(kv + o, KV)
@@ -327,6 +340,13 @@
 
     lax.fori_loop(1, KV, norm_step, 0)
     n_rcv[kv] = n_src[y]
+    for h in range(4):
+        decay, corr = new[h]
+        for r in range(8):
+            col = k_t[h // 2][:, r : r + 1]
+            s_buf[r, h] = s_buf[r, h] * decay[r : r + 1] + col * corr[r : r + 1]
+    store = pltpu.make_async_copy(s_buf, state_out, out_sem)
+    store.start()
     arrived(n_rcv.at[pl.ds(0, KV - 1)], NRM)
     normed = n_rcv[...].astype(F32).reshape(ROWS, HEAD).astype(BF)
     branch = summed(dot(wo_rcv[...].reshape(ROWS, HEAD), normed, 1, 1), 1, PR2)
@@ -336,7 +356,8 @@
 
     branch = half_ffn(1, 2, X3, RS2, AG2, PR3, lambda: None)
     own3 = (own2.astype(F32) + 0.5 * branch).astype(BF)
-    out[...] = dot(own3, eye8, 0, 0).astype(BF)
+    out[...] = own3
+    store.wait()
 
     for i, kk in enumerate((X1, X2, X3)):
         left(xg.at[i, pl.ds(0, PLANE - 1)], kk)
@@ -358,21 +379,18 @@
 
 
 def layer(res, state, gain1, gate1, up1, down1, gain2, wq, wk, wv, wg, wbeta, wdecay, rate, bias, hgain, wo, gain3, gate2, up2, down2):
-    vmem = pl.BlockSpec(memory_space=pltpu.VMEM)
-    smem = pl.BlockSpec(memory_space=pltpu.SMEM)
-    specs = [vmem, pl.BlockSpec(memory_space=pl.ANY)] + [vmem] * 15 + [smem] * 2 + [vmem] * 2
-    out, k, corr, decay = pl.pallas_call(
+    args = (
+        res.T, state, gain1[None], gain2[None], gain3[None], gate1, up1, down1.T, gate2, up2, down2.T,
+        wq, wk, wv, wg, wbeta.T, wdecay.T, rate[None], bias[None], hgain[None], wo.T,
+    )
+    out, new_state = pl.pallas_call(
         kernel,
-        out_shape=(
-            jax.ShapeDtypeStruct((ROWS, 8), BF),
-            jax.ShapeDtypeStruct((8, 2, HEAD), F32),
-            jax.ShapeDtypeStruct((8, 4, HEAD), F32),
-            jax.ShapeDtypeStruct((8, 4), F32),
-        ),
-        in_specs=specs,
-        out_specs=(vmem,) * 4,
-        scratch_shapes=[
-            pltpu.VMEM((8, 4, HEAD, HEAD), F32),
+        out_shape=(jax.ShapeDtypeStruct((8, ROWS), BF), jax.ShapeDtypeStruct(state.shape, F32)),
+        in_specs=[pl.BlockSpec(memory_space=pltpu.HBM)] * len(args),
+        out_specs=(pl.BlockSpec(memory_space=pltpu.VMEM), pl.BlockSpec(memory_space=STATE_SPACE)),
+        scratch_shapes=[pltpu.VMEM(a.shape, a.dtype) for a in args]
+        + [
+            pltpu.SemaphoreType.DMA((len(args),)),
             pltpu.SemaphoreType.DMA,
             pltpu.SemaphoreType.DMA((N_SEM,)),
             pltpu.SemaphoreType.DMA((N_SEM,)),
@@ -401,13 +419,9 @@
             pltpu.VMEM((4, 8, HEAD), BF),
             pltpu.VMEM((KV, 8, HEAD), BF),
         ],
-        compiler_params=pltpu.CompilerParams(collective_id=0, has_side_effects=True, vmem_limit_bytes=48 << 20),
-    )(
-        res, state, gain1[None], gain2[None], gain3[None], gate1, up1, down1, gate2, up2, down2,
-        wq, wk, wv, wg, wbeta, wdecay, rate[None], bias[None], hgain[None], wo,
-    )
-    keys = jnp.repeat(k, 2, axis=1)
-    return out, state * decay[:, :, None, None] + keys[:, :, :, None] * corr[:, :, None, :]
+        compiler_params=pltpu.CompilerParams(collective_id=0, has_side_effects=True, vmem_limit_bytes=67_043_328),
+    )(*args)
+    return out.T, new_state
 
 
 def solution(mesh):

time: 111 us -> 94.7 us (0.85)
  local copies, waits for them, and re-layouts: 18.4 us -> 4.4 us
  other arithmetic: 1.72 us -> 0 us
    unnamed x39 -> x2, local copies, waits for them, and re-layouts: 18.4 us -> 4.4 us
    add x1 -> x0, other arithmetic: 1.72 us -> none  [layer(): state * decay[:, :, None, None] + keys[:, :, :, None] * corr[:, :, None, :]]
where the time goes in v2:
time: 94.7 us; the launch traced here: 94.5 us
  Pallas kernels  89.5 us (95%)
  local copies, waits for them, and re-layouts  4.4 us (5%)
    pallas_call x1, Pallas kernels, layer(): pl.pallas_call(kernel, out_shape=(jax.ShapeDtypeStruct((8, ROWS), BF), ja...  89.5 us
    unnamed x2, local copies, waits for them, and re-layouts  4.4 us

profile of v2, /device:TPU:1, one launch (start us, length us, event | category | flops | bytes accessed | tf_op | source)
XLA Modules:
  0.0 94.5 jit_solution(8857286391898222137)
XLA Ops:
  0.6 89.5 %shard_map.212 = (bf16[8,256]{1,0:T(8,128)(2,1)}, f32[8,4,128,128]{3,2,1,0:T(8,128)}) custom-call(bf16[8,256]{1,0:T(8,128)(2,1)} %bitcast.18, f32[8,4,128,128]{3,2,1,0:T(8,128)} %state.1, f32[1,64]{1,0:T(1,128)} %bitcast.20, f32[1,64]{1,0:T(1,128)} %bitcast.21, f32[1,64]{1,0:T(1,128)} %bitcast.22, bf16[64,704]{1,0:T(8,128)(2,1)} %gate1_h.1, ...), custom_call_target="tpu_custom_call" | custom-call | tf_op jit(solution)/shard_map/pallas_call | solution.py:386
  90.1 1.3 %copy.25 = bf16[256,8]{0,1:T(8,128)(2,1)} copy(bf16[256,8]{0,1:T(8,128)(2,1)} %bitcast.19) | data formatting | bytes 8192
  91.4 3.1 %copy.26 = f32[8,4,128,128]{3,2,1,0:T(8,128)} copy(f32[8,4,128,128]{3,2,1,0:T(8,128)} %get-tuple-element.9) | data formatting | bytes 4194304

commit v3 on v1

v3 whole, which is shorter than its diff:
```python
import jax
import jax.numpy as jnp
from jax import lax
from jax.experimental import pallas as pl
from jax.experimental.pallas import tpu as pltpu
from jax.sharding import PartitionSpec as P

MESH = pl.DeviceIdType.MESH
BF, F32 = jnp.bfloat16, jnp.float32
D, EPS = 2048, 1e-6
NZ, NY, NT = 8, 4, 8
PLANE = NY * NT
KV = NZ * NY
ROWS = 256
KEEP, GROUP = 22, 24
HID = NZ * KEEP
PAD = NZ * GROUP
HEAD = 128

X1, X2, X3, RS1, RS2, AG1, AG2, PR1, PR2, PR3, MIX, NRM, GU1, DD, GN = range(15)
MW, WO, GU2, D2 = 15, 19, 23, 27
N_SEM = 31
MCOLS = 1664
FFT, FFP = 704, 768
RING_Z = (4, 3, 5, 2, 6, 1, 7)
FAR = (0, 1, 2, 1)


def dot(a, b, ca, cb):
    return lax.dot_general(a, b, (((ca,), (cb,)), ((), ())), preferred_element_type=F32)


def iota(shape, dim):
    return lax.broadcasted_iota(jnp.int32, shape, dim)


def one_hot(cond):
    return jnp.where(cond, 1.0, 0.0).astype(BF)


def silu(v):
    return v / (1.0 + jnp.exp(-v))


def kernel(
    res_h, state, gain1_h, gain2_h, gain3_h, gate1_h, up1_h, down1_h, gate2_h, up2_h, down2_h,
    wq_h, wk_h, wv_h, wg_h, wbeta_h, wdecay_h, rate_h, bias_h, hgain_h, wo_h,
    out, k_out, c_out, d_out,
    res, s_buf, gain1, gain2, gain3, gate1, up1, down1, wbeta, wdecay, rate, bias, hgain,
    in_sem, send, recv,
    gu_src, gu_rcv, dd_src, dd_rcv, gn, mw, wo, gu2, d2,
    a_w, d_w, g_col, g_row, xrow,
    xg, rs_src, rs_rcv, hg, pr1_src, pr1_rcv,
    xb, m_src, m_rcv, nb, pr2_src, pr2_rcv, rs2_src, rs2_rcv, hg2, pr3_src, pr3_rcv,
):
    kv = lax.axis_index("kv")
    t = lax.axis_index("tp")
    z, y = lax.div(kv, NY), lax.rem(kv, NY)
    x, core = lax.div(t, 2), lax.rem(t, 2)
    me = y * NT + t
    zs = [lax.rem(z + o, NZ) for o in range(NZ)]
    ys = [lax.rem(y + o, NY) for o in range(NY)]
    ts = [[lax.rem(x + o, 4) * 2 + c for c in (core, 1 - core)] for o in range(4)]

    z_peers = [(zs[o], (zs[o] * NY + y, t)) for o in RING_Z]
    y_peers = [(ys[o], (z * NY + ys[o], t)) for o in (2, 1, 3)]
    t_peers = [(ts[dx][dc], (kv, ts[dx][dc])) for dx in (2, 1, 3, 0) for dc in (0, 1) if dx or dc]
    plane = [(dy, dx, dc) for dy in range(4) for dx in range(4) for dc in range(2) if dy or dx or dc]
    plane.sort(key=lambda o: -(FAR[o[0]] + FAR[o[1]]))
    plane_peers = [(ys[dy] * NT + ts[dx][dc], (z * NY + ys[dy], ts[dx][dc])) for dy, dx, dc in plane]

    barrier = pltpu.get_barrier_semaphore()
    greet = z_peers[:3] + plane_peers[:10] + z_peers[3:5] + plane_peers[10:] + z_peers[5:]
    for _, peer in greet:
        pl.semaphore_signal(barrier, inc=1, device_id=peer, device_id_type=MESH)

    named = {}
    for i, (src, dst) in enumerate((
        (gate1_h, gate1), (up1_h, up1), (res_h, res), (gain1_h, gain1), (gain2_h, gain2), (gain3_h, gain3), (down1_h, down1),
        (wbeta_h, wbeta), (wdecay_h, wdecay),
        (wq_h, mw.at[y, :, 0:256]), (wk_h, mw.at[y, :, 256:512]), (wv_h, mw.at[y, :, 512:1024]), (wg_h, mw.at[y, :, 1024:1536]),
        (wo_h, wo.at[y]), (gate2_h, gu2.at[y, 0]), (up2_h, gu2.at[y, 1]), (down2_h, d2.at[y]),
        (rate_h, rate), (bias_h, bias), (hgain_h, hgain), (state, s_buf),
    )):
        named[id(src)] = pltpu.make_async_copy(src, dst, in_sem.at[i])
        named[id(src)].start()

    def ready(*refs):
        for ref in refs:
            named[id(ref)].wait()

    def put(src, dst, k, peer):
        pltpu.make_async_remote_copy(
            src_ref=src, dst_ref=dst, send_sem=send.at[k], recv_sem=recv.at[k], device_id=peer, device_id_type=MESH
        ).start()

    def arrived(part, k):
        pltpu.make_async_copy(part, part, recv.at[k]).wait()

    def left(part, k):
        pltpu.make_async_copy(part, part, send.at[k]).wait()

    def share(buf, own, k, peers):
        for _, peer in peers:
            put(buf.at[own], buf.at[own], k, peer)

    def deal(src, dst, own, k, peers):
        for p, peer in peers:
            put(src.at[p], dst.at[own], k, peer)
        dst[own] = src[own]

    above, below = (z * NY + ys[1], t), (z * NY + ys[3], t)

    def y_start(buf, k):
        put(buf.at[y], buf.at[y], k, above)
        put(buf.at[y], buf.at[y], k + 1, below)

    def halves(buf, p):
        n = buf.shape[1] // 2
        return buf.at[p, pl.ds(0, n)], buf.at[p, pl.ds(n, n)]

    def y_pass(buf, k):
        arrived(buf.at[ys[3]], k)
        first, second = halves(buf, ys[3])
        put(first, first, k + 2, above)
        arrived(buf.at[ys[1]], k + 1)
        first, second = halves(buf, ys[1])
        put(second, second, k + 3, below)

    def y_done(buf, k):
        first, second = halves(buf, ys[2])
        arrived(first, k + 2)
        arrived(second, k + 3)

    def y_left(buf, k):
        first, second = halves(buf, 0)
        left(buf.at[0], k)
        left(buf.at[0], k + 1)
        left(first, k + 2)
        left(second, k + 3)

    low = one_hot(iota((64, 128), 0) == iota((64, 128), 1))
    high = one_hot(iota((64, 128), 0) + 64 == iota((64, 128), 1))
    eye64 = iota((64, 64), 0) == iota((64, 64), 1)

    ready(gate1_h, up1_h)
    both = dot(gate1[...], low, 0, 0) + dot(up1[...], high, 0, 0)
    gu_src[...] = both.astype(BF).reshape(NY, HID, 128)
    ready(res_h, gain1_h, gain2_h, gain3_h)
    xg[me] = res[...]
    gn[y, 0:8] = jnp.broadcast_to(gain1[...], (8, 64))
    gn[y, 8:16] = jnp.broadcast_to(gain2[...], (8, 64))
    gn[y, 16:24] = jnp.broadcast_to(gain3[...], (8, 64))

    pl.semaphore_wait(barrier, len(greet))

    deal(gu_src, gu_rcv, y, GU1, y_peers)
    share(xg, me, X1, plane_peers)
    share(gn, y, GN, y_peers)

    ready(down1_h)
    dd_src[...] = dot(down1[...], low, 0, 0).astype(BF).reshape(NY, HID, 128)
    sel_b = one_hot((iota((32, 128), 0) == iota((32, 128), 1) + 4 * t) & (iota((32, 128), 1) < 4))
    sel_d = one_hot((iota((32, 128), 0) == iota((32, 128), 1) - 4 + 4 * t) & (iota((32, 128), 1) >= 4) & (iota((32, 128), 1) < 8))
    ready(wbeta_h, wdecay_h)
    mw[y, :, 1536:MCOLS] = (dot(wbeta[...], sel_b, 0, 0) + dot(wdecay[...], sel_d, 0, 0)).astype(BF)

    r, c = iota((PAD, HID), 0), iota((PAD, HID), 1)
    group = jnp.zeros_like(r)
    for i in range(1, NZ):
        group = group + jnp.where(r >= GROUP * i, 1, 0)
    pick = one_hot((c == r - (GROUP - KEEP) * group) & (r - GROUP * group < KEEP))
    lane = iota((PAD, 128), 1)

    def column(p, i):
        row = gn[p, 8 * i : 8 * i + 1]
        return jnp.sum(jnp.where(eye64, jnp.broadcast_to(row, (64, 64)), 0.0), axis=1, keepdims=True)

    arrived(gn.at[pl.ds(0, NY - 1)], GN)
    for p in range(NY):
        g_col[64 * p : 64 * (p + 1)] = jnp.broadcast_to(column(p, 0), (64, ROWS))
    arrived(gu_rcv.at[pl.ds(0, NY - 1)], GU1)
    parts = [dot(pick, gu_rcv[p], 1, 0) for p in range(NY)]
    for h in range(2):
        a, b = parts[2 * h], parts[2 * h + 1]
        a_w[0:PAD, 128 * h : 128 * (h + 1)] = jnp.where(lane < 64, a, pltpu.roll(b, 64, 1)).astype(BF)
        a_w[PAD : 2 * PAD, 128 * h : 128 * (h + 1)] = jnp.where(lane < 64, pltpu.roll(a, 64, 1), b).astype(BF)

    arrived(xg.at[pl.ds(0, PLANE - 1)], X1)
    x0 = xg[...].astype(F32).reshape(ROWS, ROWS)
    part = dot(a_w[...], (x0 * g_col[...]).astype(BF), 1, 0)
    total = jnp.sum(x0 * x0, axis=0, keepdims=True)
    coarse = total.astype(BF).astype(F32)
    row = iota((NZ, GROUP, ROWS), 1)
    gate = part[0:PAD].reshape(NZ, GROUP, ROWS)
    up = part[PAD : 2 * PAD].reshape(NZ, GROUP, ROWS)
    gate = jnp.where(row == KEEP, coarse.reshape(1, 1, ROWS), gate)
    gate = jnp.where(row == KEEP + 1, (total - coarse).reshape(1, 1, ROWS), gate)
    rs_src[...] = jnp.concatenate([gate, up], axis=1).astype(BF).reshape(NZ, 2 * GROUP // 8, 8, ROWS)
    deal(rs_src, rs_rcv, z, RS1, z_peers)

    for p, peer in y_peers:
        put(dd_src.at[p], dd_rcv.at[y], DD, peer)
    dd_rcv[y] = dd_src[y]
    ready(wq_h, wk_h, wv_h, wg_h)
    y_start(mw, MW)
    xrow[...] = jnp.transpose(x0).reshape(KV, 8, ROWS).astype(BF)
    lane64 = iota((64, 128), 1)
    for i in range(2):
        for h in range(2):
            spread = jnp.where(lane64 == iota((64, 128), 0), column(2 * h, i + 1), 0.0)
            spread = spread + jnp.where(lane64 == iota((64, 128), 0) + 64, column(2 * h + 1, i + 1), 0.0)
            g_row[i, :, 128 * h : 128 * (h + 1)] = jnp.broadcast_to(jnp.sum(spread, axis=0, keepdims=True), (8, 128))

    arrived(rs_rcv.at[pl.ds(0, NZ - 1)], RS1)
    both = jnp.sum(rs_rcv[...].astype(F32), axis=0).reshape(2 * GROUP, ROWS)
    gate, up = both[0:GROUP], both[GROUP:]
    scale = lax.rsqrt((gate[KEEP : KEEP + 1] + gate[KEEP + 1 : KEEP + 2]) / D + EPS)
    hidden = silu(gate * scale) * (up * scale)
    hidden = jnp.where(iota((GROUP, ROWS), 0) < KEEP, hidden, 0.0)
    hg[z] = hidden.reshape(GROUP // 8, 8, ROWS).astype(BF)
    share(hg, z, AG1, z_peers)

    arrived(dd_rcv.at[pl.ds(0, NY - 1)], DD)
    for h in range(2):
        a, b = dot(pick, dd_rcv[2 * h], 1, 0), dot(pick, dd_rcv[2 * h + 1], 1, 0)
        d_w[:, 128 * h : 128 * (h + 1)] = (a + pltpu.roll(b, 64, 1)).astype(BF)
    y_pass(mw, MW)
    arrived(hg.at[pl.ds(0, NZ - 1)], AG1)
    h = hg[...].astype(F32).reshape(PAD, ROWS).astype(BF)
    pr1_src[...] = dot(h, d_w[...], 0, 0).reshape(KV, 8, ROWS).astype(BF)
    for (dy, dx, dc), (_, peer) in zip(plane, plane_peers):
        put(pr1_src.at[ts[dx][dc] * NY + ys[dy]], pr1_rcv.at[me], PR1, peer)
    pr1_rcv[me] = pr1_src[t * NY + y]
    arrived(pr1_rcv.at[pl.ds(0, PLANE - 1)], PR1)
    branch = jnp.sum(pr1_rcv[...].astype(F32), axis=0)
    own1 = (xrow[t * NY + y].astype(F32) + 0.5 * branch).astype(BF)

    def gathered(i, own, k):
        xb[i, t] = own
        share(xb.at[i], t, k, t_peers)

    def scaled_of(i, k):
        arrived(xb.at[i, pl.ds(0, NT - 1)], k)
        v = xb[i].astype(F32).reshape(64, ROWS)
        squares = jnp.sum(v * v, axis=1, keepdims=True)
        coarse = squares.astype(BF).astype(F32)
        return v, (v * g_row[i, 0:1]).astype(BF), coarse, squares - coarse

    gathered(0, own1, X2)
    y_done(mw, MW)
    _, scaled, coarse, fine = scaled_of(0, X2)
    last = iota((64, 128), 1)
    for a, b in ((0, 512), (512, 1024), (1024, 1536), (1536, MCOLS)):
        part = dot(scaled, mw[:, :, a:b].reshape(ROWS, b - a), 1, 0)
        if a == 1536:
            part = part + jnp.where(last == 8, coarse, 0.0) + jnp.where(last == 9, fine, 0.0)
        m_src[:, :, a:b] = part.reshape(NZ, 8, b - a).astype(BF)
    deal(m_src, m_rcv, z, MIX, z_peers)
    ready(wo_h, gate2_h, up2_h, down2_h, state, rate_h, bias_h, hgain_h)
    y_start(wo, WO)
    y_start(gu2, GU2)
    arrived(m_rcv.at[pl.ds(0, NZ - 1)], MIX)

    mixed = jnp.sum(m_rcv[...].astype(F32), axis=0)
    ext = mixed[:, 1536:MCOLS]
    rowscale = lax.rsqrt((ext[:, 8:9] + ext[:, 9:10]) / D + EPS)
    heads = [mixed[:, 128 * i : 128 * (i + 1)] * rowscale for i in range(12)]

    def unit(v):
        a = silu(v)
        return a * lax.rsqrt(jnp.sum(a * a, axis=-1, keepdims=True) + EPS)

    q = [unit(heads[m]) * HEAD**-0.5 for m in range(2)]
    k = [unit(heads[2 + m]) for m in range(2)]
    q_t = [jnp.transpose(v) for v in q]
    k_t = [jnp.transpose(v) for v in k]
    kq = [jnp.sum(k[m] * q[m], axis=-1, keepdims=True) for m in range(2)]
    ext = ext * rowscale
    for h in range(4):
        m = h // 2
        val = silu(heads[4 + h])
        gate = silu(heads[8 + h])
        beta = 1.0 / (1.0 + jnp.exp(-ext[:, h : h + 1]))
        pre = ext[:, 4 + h : 5 + h] + bias[:, h : h + 1]
        soft = jnp.maximum(pre, 0.0) + jnp.log1p(jnp.exp(-jnp.abs(pre)))
        decay = jnp.exp(-jnp.exp(rate[:, h : h + 1]) * soft)
        by_k, by_q = [], []
        for i in range(8):
            s = s_buf[i, h]
            by_k.append(jnp.sum(s * k_t[m][:, i : i + 1], axis=0, keepdims=True))
            by_q.append(jnp.sum(s * q_t[m][:, i : i + 1], axis=0, keepdims=True))
        by_k = jnp.concatenate(by_k, axis=0)
        by_q = jnp.concatenate(by_q, axis=0)
        corr = beta * (val - decay * by_k)
        reading = decay * by_q + kq[m] * corr
        norm = lax.rsqrt(jnp.mean(reading * reading, axis=-1, keepdims=True) + EPS)
        nb[z, :, 128 * h : 128 * (h + 1)] = (reading * norm * hgain[...] * gate).astype(BF)
        c_out[:, h] = corr
        d_out[:, h : h + 1] = decay
    for m in range(2):
        k_out[:, m] = k[m]
    share(nb, z, NRM, z_peers)
    y_pass(wo, WO)
    y_pass(gu2, GU2)
    y_start(d2, D2)
    y_done(wo, WO)
    arrived(nb.at[pl.ds(0, NZ - 1)], NRM)
    normed = nb[...].astype(F32).reshape(64, 512).astype(BF)
    pr2_src[...] = dot(normed, wo[...].reshape(ROWS, 512), 1, 1).reshape(NT, 8, ROWS).astype(BF)
    deal(pr2_src, pr2_rcv, t, PR2, t_peers)
    arrived(pr2_rcv.at[pl.ds(0, NT - 1)], PR2)
    own2 = (own1.astype(F32) + jnp.sum(pr2_rcv[...].astype(F32), axis=0)).astype(BF)

    gathered(1, own2, X3)
    y_done(gu2, GU2)
    x3, scaled, coarse, fine = scaled_of(1, X3)
    gate = dot(scaled, gu2[:, 0].reshape(ROWS, FFT), 1, 0)
    up = dot(scaled, gu2[:, 1].reshape(ROWS, FFT), 1, 0)
    fill = jnp.where(iota((64, 64), 1) == 0, coarse, jnp.where(iota((64, 64), 1) == 1, fine, 0.0))
    rs2_src[:, :, 0:FFP] = jnp.concatenate([gate, fill], axis=1).reshape(NZ, 8, FFP).astype(BF)
    rs2_src[:, :, FFP:] = jnp.concatenate([up, jnp.zeros((64, 64), F32)], axis=1).reshape(NZ, 8, FFP).astype(BF)
    deal(rs2_src, rs2_rcv, z, RS2, z_peers)
    y_pass(d2, D2)
    x3_t = jnp.transpose(jnp.concatenate([jnp.zeros((64, ROWS), F32), x3], axis=0))
    arrived(rs2_rcv.at[pl.ds(0, NZ - 1)], RS2)
    both = jnp.sum(rs2_rcv[...].astype(F32), axis=0)
    gate, up = both[:, 0:FFP], both[:, FFP:]
    scale = lax.rsqrt((gate[:, FFT : FFT + 1] + gate[:, FFT + 1 : FFT + 2]) / D + EPS)
    hidden = silu(gate * scale) * (up * scale)
    hg2[z] = jnp.where(iota((8, FFP), 1) < FFT, hidden, 0.0).astype(BF)
    share(hg2, z, AG2, z_peers)
    y_done(d2, D2)
    arrived(hg2.at[pl.ds(0, NZ - 1)], AG2)
    h = hg2[...].astype(F32).reshape(64, FFP).astype(BF)[:, 0:FFT]
    h = jnp.concatenate([h, jnp.zeros((64, FFT), BF)], axis=0)
    part = dot(d2[...].reshape(ROWS, FFT), h, 1, 1) + x3_t
    pr3_src[...] = part.reshape(PLANE, 8, 128).astype(BF)
    deal(pr3_src, pr3_rcv, me, PR3, plane_peers)
    arrived(pr3_rcv.at[pl.ds(0, PLANE - 1)], PR3)
    final = jnp.zeros((8, ROWS), F32)
    l, b = iota((128, ROWS), 0), iota((128, ROWS), 1)
    for p in range(NY):
        total = jnp.sum(pr3_rcv[NT * p : NT * (p + 1)].astype(F32), axis=0)
        base = pltpu.roll(pr3_rcv[NT * p].astype(F32), 64, 1)
        place = one_hot((b == l + 24 * lax.shift_right_logical(l, 3) + 8 * p) & (l < 64))
        final = final + dot((base + 0.5 * total).astype(BF), place, 1, 0)
    out[...] = final.astype(BF)

    left(xg.at[pl.ds(0, PLANE - 1)], X1)
    left(pr1_src.at[pl.ds(0, PLANE - 1)], PR1)
    left(pr3_src.at[pl.ds(0, PLANE - 1)], PR3)
    left(rs_src.at[pl.ds(0, NZ - 1)], RS1)
    left(hg.at[pl.ds(0, NZ - 1)], AG1)
    left(xb.at[0, pl.ds(0, NT - 1)], X2)
    left(xb.at[1, pl.ds(0, NT - 1)], X3)
    left(pr2_src.at[pl.ds(0, NT - 1)], PR2)
    left(m_src.at[pl.ds(0, NZ - 1)], MIX)
    left(nb.at[pl.ds(0, NZ - 1)], NRM)
    left(rs2_src.at[pl.ds(0, NZ - 1)], RS2)
    left(hg2.at[pl.ds(0, NZ - 1)], AG2)
    left(gu_src.at[pl.ds(0, NY - 1)], GU1)
    left(dd_src.at[pl.ds(0, NY - 1)], DD)
    left(gn.at[pl.ds(0, NY - 1)], GN)
    y_left(mw, MW)
    y_left(wo, WO)
    y_left(gu2, GU2)
    y_left(d2, D2)


def layer(res, state, gain1, gate1, up1, down1, gain2, wq, wk, wv, wg, wbeta, wdecay, rate, bias, hgain, wo, gain3, gate2, up2, down2):
    vmem = pl.BlockSpec(memory_space=pltpu.VMEM)
    args = (
        res.T, state, gain1[None], gain2[None], gain3[None], gate1, up1, down1.T, gate2, up2, down2.T,
        wq, wk, wv, wg, wbeta.T, wdecay.T, rate[None], bias[None], hgain[None], wo.T,
    )
    held = [args[i] for i in (0, 1, 2, 3, 4, 5, 6, 7, 15, 16, 17, 18, 19)]
    out, k, corr, decay = pl.pallas_call(
        kernel,
        out_shape=(
            jax.ShapeDtypeStruct((8, ROWS), BF),
            jax.ShapeDtypeStruct((8, 2, HEAD), F32),
            jax.ShapeDtypeStruct((8, 4, HEAD), F32),
            jax.ShapeDtypeStruct((8, 4), F32),
        ),
        in_specs=[pl.BlockSpec(memory_space=pltpu.HBM)] * len(args),
        out_specs=(vmem,) * 4,
        scratch_shapes=[pltpu.VMEM(a.shape, a.dtype) for a in held]
        + [
            pltpu.SemaphoreType.DMA((len(args),)),
            pltpu.SemaphoreType.DMA((N_SEM,)),
            pltpu.SemaphoreType.DMA((N_SEM,)),
            pltpu.VMEM((NY, HID, 128), BF),
            pltpu.VMEM((NY, HID, 128), BF),
            pltpu.VMEM((NY, HID, 128), BF),
            pltpu.VMEM((NY, HID, 128), BF),
            pltpu.VMEM((NY, 24, 64), F32),
            pltpu.VMEM((NY, 64, MCOLS), BF),
            pltpu.VMEM((NY, 64, 512), BF),
            pltpu.VMEM((NY, 2, 64, FFT), BF),
            pltpu.VMEM((NY, 64, FFT), BF),
            pltpu.VMEM((2 * PAD, ROWS), BF),
            pltpu.VMEM((PAD, ROWS), BF),
            pltpu.VMEM((ROWS, ROWS), F32),
            pltpu.VMEM((2, 8, ROWS), F32),
            pltpu.VMEM((KV, 8, ROWS), BF),
            pltpu.VMEM((PLANE, 8, ROWS), BF),
            pltpu.VMEM((NZ, 2 * GROUP // 8, 8, ROWS), BF),
            pltpu.VMEM((NZ, 2 * GROUP // 8, 8, ROWS), BF),
            pltpu.VMEM((NZ, GROUP // 8, 8, ROWS), BF),
            pltpu.VMEM((PLANE, 8, ROWS), BF),
            pltpu.VMEM((PLANE, 8, ROWS), BF),
            pltpu.VMEM((2, NT, 8, ROWS), BF),
            pltpu.VMEM((NZ, 8, MCOLS), BF),
            pltpu.VMEM((NZ, 8, MCOLS), BF),
            pltpu.VMEM((NZ, 8, 512), BF),
            pltpu.VMEM((NT, 8, ROWS), BF),
            pltpu.VMEM((NT, 8, ROWS), BF),
            pltpu.VMEM((NZ, 8, 2 * FFP), BF),
            pltpu.VMEM((NZ, 8, 2 * FFP), BF),
            pltpu.VMEM((NZ, 8, FFP), BF),
            pltpu.VMEM((PLANE, 8, 128), BF),
            pltpu.VMEM((PLANE, 8, 128), BF),
        ],
        compiler_params=pltpu.CompilerParams(collective_id=0, has_side_effects=True, vmem_limit_bytes=67_043_328),
    )(*args)
    keys = jnp.repeat(k, 2, axis=1)
    return out.T, state * decay[:, :, None, None] + keys[:, :, :, None] * corr[:, :, None, :]


def solution(mesh):
    placed = (
        P(None, ("kv", "tp")),
        P("kv", "tp", None, None),
        P("kv"),
        P("kv", "tp"),
        P("kv", "tp"),
        P("tp", "kv"),
        P("kv"),
        P("kv", "tp"),
        P("kv", "tp"),
        P("kv", "tp"),
        P("kv", "tp"),
        P("kv", None),
        P("kv", None),
        P("tp"),
        P("tp"),
        P(),
        P("tp", "kv"),
        P("kv"),
        P("kv", "tp"),
        P("kv", "tp"),
        P("tp", "kv"),
    )
    return jax.shard_map(
        layer,
        mesh=mesh,
        in_specs=placed,
        out_specs=(P(None, ("kv", "tp")), P("kv", "tp", None, None)),
        check_vma=False,
    )
```

time: 111 us -> 81 us (0.73)
  local copies, waits for them, and re-layouts: 18.4 us -> 1.3 us
  Pallas kernels: 89.1 us -> 75.9 us
  other arithmetic: 1.72 us -> 2.96 us
    unnamed x39 -> x3, local copies, waits for them, and re-layouts: 18.4 us -> 0.6 us
    pallas_call x1, Pallas kernels: 89.1 us -> 75.9 us  [layer(): pl.pallas_call(kernel, out_shape=(jax.ShapeDtypeStruct((8, ROWS), BF), ja...]
    add x1, other arithmetic: 1.72 us -> 2.96 us  [layer(): state * decay[:, :, None, None] + keys[:, :, :, None] * corr[:, :, None, :]]
where the time goes in v3:
time: 81 us; the launch traced here: 80.8 us
  Pallas kernels  75.9 us (94%)
  other arithmetic  2.96 us (4%)
  local copies, waits for them, and re-layouts  1.3 us (2%)
    pallas_call x1, Pallas kernels, layer(): pl.pallas_call(kernel, out_shape=(jax.ShapeDtypeStruct((8, ROWS), BF), ja...  75.9 us
    add x1, other arithmetic, layer(): state * decay[:, :, None, None] + keys[:, :, :, None] * corr[:, :, None, :]  2.96 us

profile of v3, /device:TPU:1, one launch (start us, length us, event | category | flops | bytes accessed | tf_op | source)
XLA Modules:
  0.0 80.8 jit_solution(9418759653312556161)
XLA Ops:
  0.6 75.9 %shard_map.212 = (bf16[8,256]{1,0:T(8,128)(2,1)}, f32[8,2,128]{2,1,0:T(2,128)}, f32[8,4,128]{2,1,0:T(4,128)}, f32[8,4]{1,0:T(8,128)}) custom-call(bf16[8,256]{1,0:T(8,128)(2,1)} %bitcast.20, f32[8,4,128,128]{3,2,1,0:T(8,128)} %state.1, f32[1,64]{1,0:T(1,128)} %bitcast.22, f32[1,64]{1,0:T(1,128)} %bitcast.23, f32[1,64]{1,0:T(1,128)} %bitcast.24, ...), custom_call_target="tpu_custom_call" | custom-call | tf_op jit(solution)/shard_map/pallas_call | solution.py:378
  76.5 0.7 broadcast_in_dim.29
  77.2 0.0 copy-start
  77.2 3.0 %multiply_add_fusion = f32[8,4,128,128]{3,2,1,0:T(8,128)} fusion(f32[8,4,128,128]{3,2,1,0:T(8,128)} %state.1, f32[8,4,128]{2,1,0:T(4,128)} %get-tuple-element.9, f32[8,4,128]{2,1,0:T(4,128)S(1)} %bitcast.16, f32[8,4]{1,0:T(8,128)} %get-tuple-element.7), kind=kLoop, calls=%fused_computation | loop fusion | flops 1572864 | bytes 4227200 | tf_op jit(solution)/shard_map/add | solution.py:428
  80.2 0.0 copy-done
  80.2 0.6 copy.24
Async XLA Ops:
  77.2 3.0 %copy-start = (bf16[8,256]{1,0:T(8,128)(2,1)S(1)}, bf16[8,256]{1,0:T(8,128)(2,1)}, u32[]{:S(2)}) copy-start(bf16[8,256]{1,0:T(8,128)(2,1)} %get-tuple-element.6) | copy-start | bytes 12292

commit v4 on v3

--- a/solution.py
+++ b/solution.py
@@ -45,13 +45,13 @@
 def kernel(
     res_h, state, gain1_h, gain2_h, gain3_h, gate1_h, up1_h, down1_h, gate2_h, up2_h, down2_h,
     wq_h, wk_h, wv_h, wg_h, wbeta_h, wdecay_h, rate_h, bias_h, hgain_h, wo_h,
-    out, k_out, c_out, d_out,
+    out, state_out,
     res, s_buf, gain1, gain2, gain3, gate1, up1, down1, wbeta, wdecay, rate, bias, hgain,
-    in_sem, send, recv,
+    in_sem, out_sem, send, recv,
     gu_src, gu_rcv, dd_src, dd_rcv, gn, mw, wo, gu2, d2,
     a_w, d_w, g_col, g_row, xrow,
     xg, rs_src, rs_rcv, hg, pr1_src, pr1_rcv,
-    xb, m_src, m_rcv, nb, pr2_src, pr2_rcv, rs2_src, rs2_rcv, hg2, pr3_src, pr3_rcv,
+    xb, m_src, m_rcv, nb, pa_src, pa_rcv, pb, rs2_src, rs2_rcv, hg2, pr3_src, pr3_rcv,
 ):
     kv = lax.axis_index("kv")
     t = lax.axis_index("tp")
@@ -154,9 +154,9 @@
 
     pl.semaphore_wait(barrier, len(greet))
 
+    share(gn, y, GN, y_peers)
     deal(gu_src, gu_rcv, y, GU1, y_peers)
     share(xg, me, X1, plane_peers)
-    share(gn, y, GN, y_peers)
 
     ready(down1_h)
     dd_src[...] = dot(down1[...], low, 0, 0).astype(BF).reshape(NY, HID, 128)
@@ -236,20 +236,17 @@
     branch = jnp.sum(pr1_rcv[...].astype(F32), axis=0)
     own1 = (xrow[t * NY + y].astype(F32) + 0.5 * branch).astype(BF)
 
-    def gathered(i, own, k):
-        xb[i, t] = own
-        share(xb.at[i], t, k, t_peers)
-
-    def scaled_of(i, k):
-        arrived(xb.at[i, pl.ds(0, NT - 1)], k)
-        v = xb[i].astype(F32).reshape(64, ROWS)
+    def scaled_of(v, i):
         squares = jnp.sum(v * v, axis=1, keepdims=True)
         coarse = squares.astype(BF).astype(F32)
-        return v, (v * g_row[i, 0:1]).astype(BF), coarse, squares - coarse
-
-    gathered(0, own1, X2)
+        return (v * g_row[i, 0:1]).astype(BF), coarse, squares - coarse
+
+    xb[t] = own1
+    share(xb, t, X2, t_peers)
     y_done(mw, MW)
-    _, scaled, coarse, fine = scaled_of(0, X2)
+    arrived(xb.at[pl.ds(0, NT - 1)], X2)
+    x1 = xb[...].astype(F32).reshape(64, ROWS)
+    scaled, coarse, fine = scaled_of(x1, 0)
     last = iota((64, 128), 1)
     for a, b in ((0, 512), (512, 1024), (1024, 1536), (1536, MCOLS)):
         part = dot(scaled, mw[:, :, a:b].reshape(ROWS, b - a), 1, 0)
@@ -277,6 +274,16 @@
     k_t = [jnp.transpose(v) for v in k]
     kq = [jnp.sum(k[m] * q[m], axis=-1, keepdims=True) for m in range(2)]
     ext = ext * rowscale
+    by_k, by_q = [[] for _ in range(4)], [[] for _ in range(4)]
+    for m in range(2):
+        for i in range(8):
+            k_col = jnp.broadcast_to(k_t[m][:, i : i + 1], (HEAD, HEAD))
+            q_col = jnp.broadcast_to(q_t[m][:, i : i + 1], (HEAD, HEAD))
+            for h in (2 * m, 2 * m + 1):
+                s = s_buf[i, h]
+                by_k[h].append(jnp.sum(s * k_col, axis=0, keepdims=True))
+                by_q[h].append(jnp.sum(s * q_col, axis=0, keepdims=True))
+    new = []
     for h in range(4):
         m = h // 2
         val = silu(heads[4 + h])
@@ -285,36 +292,44 @@
         pre = ext[:, 4 + h : 5 + h] + bias[:, h : h + 1]
         soft = jnp.maximum(pre, 0.0) + jnp.log1p(jnp.exp(-jnp.abs(pre)))
         decay = jnp.exp(-jnp.exp(rate[:, h : h + 1]) * soft)
-        by_k, by_q = [], []
-        for i in range(8):
-            s = s_buf[i, h]
-            by_k.append(jnp.sum(s * k_t[m][:, i : i + 1], axis=0, keepdims=True))
-            by_q.append(jnp.sum(s * q_t[m][:, i : i + 1], axis=0, keepdims=True))
-        by_k = jnp.concatenate(by_k, axis=0)
-        by_q = jnp.concatenate(by_q, axis=0)
-        corr = beta * (val - decay * by_k)
-        reading = decay * by_q + kq[m] * corr
+        corr = beta * (val - decay * jnp.concatenate(by_k[h], axis=0))
+        reading = decay * jnp.concatenate(by_q[h], axis=0) + kq[m] * corr
         norm = lax.rsqrt(jnp.mean(reading * reading, axis=-1, keepdims=True) + EPS)
         nb[z, :, 128 * h : 128 * (h + 1)] = (reading * norm * hgain[...] * gate).astype(BF)
-        c_out[:, h] = corr
-        d_out[:, h : h + 1] = decay
-    for m in range(2):
-        k_out[:, m] = k[m]
+        new.append((decay, corr))
     share(nb, z, NRM, z_peers)
     y_pass(wo, WO)
     y_pass(gu2, GU2)
     y_start(d2, D2)
+    for i in range(8):
+        for m in range(2):
+            k_col = jnp.broadcast_to(k_t[m][:, i : i + 1], (HEAD, HEAD))
+            for h in (2 * m, 2 * m + 1):
+                decay, corr = new[h]
+                s_buf[i, h] = s_buf[i, h] * decay[i : i + 1] + k_col * corr[i : i + 1]
+    store = pltpu.make_async_copy(s_buf, state_out, out_sem)
+    store.start()
     y_done(wo, WO)
     arrived(nb.at[pl.ds(0, NZ - 1)], NRM)
     normed = nb[...].astype(F32).reshape(64, 512).astype(BF)
-    pr2_src[...] = dot(normed, wo[...].reshape(ROWS, 512), 1, 1).reshape(NT, 8, ROWS).astype(BF)
-    deal(pr2_src, pr2_rcv, t, PR2, t_peers)
-    arrived(pr2_rcv.at[pl.ds(0, NT - 1)], PR2)
-    own2 = (own1.astype(F32) + jnp.sum(pr2_rcv[...].astype(F32), axis=0)).astype(BF)
-
-    gathered(1, own2, X3)
+    part = dot(normed, wo[...].reshape(ROWS, 512), 1, 1)
+    pa_src[...] = part.reshape(2, 4, 8, ROWS).astype(BF)
+    put(pa_src.at[1 - core], pa_rcv, PR2, (kv, ts[0][1]))
+    mine = jnp.where(core == 0, part[0:32], part[32:64])
+    arrived(pa_rcv, PR2)
+    pb[t] = (mine.reshape(4, 8, ROWS) + pa_rcv[...].astype(F32)).astype(BF)
+    share(pb, t, X3, t_peers)
     y_done(gu2, GU2)
-    x3, scaled, coarse, fine = scaled_of(1, X3)
+    arrived(pb.at[pl.ds(0, NT - 1)], X3)
+    branch = []
+    for c in range(2):
+        half = pb[c].astype(F32)
+        for i in range(1, 4):
+            half = half + pb[2 * i + c].astype(F32)
+        branch.append(half.reshape(32, ROWS))
+
+    x3 = (x1 + jnp.concatenate(branch, axis=0)).astype(BF).astype(F32)
+    scaled, coarse, fine = scaled_of(x3, 1)
     gate = dot(scaled, gu2[:, 0].reshape(ROWS, FFT), 1, 0)
     up = dot(scaled, gu2[:, 1].reshape(ROWS, FFT), 1, 0)
     fill = jnp.where(iota((64, 64), 1) == 0, coarse, jnp.where(iota((64, 64), 1) == 1, fine, 0.0))
@@ -346,15 +361,16 @@
         place = one_hot((b == l + 24 * lax.shift_right_logical(l, 3) + 8 * p) & (l < 64))
         final = final + dot((base + 0.5 * total).astype(BF), place, 1, 0)
     out[...] = final.astype(BF)
+    store.wait()
 
     left(xg.at[pl.ds(0, PLANE - 1)], X1)
     left(pr1_src.at[pl.ds(0, PLANE - 1)], PR1)
     left(pr3_src.at[pl.ds(0, PLANE - 1)], PR3)
     left(rs_src.at[pl.ds(0, NZ - 1)], RS1)
     left(hg.at[pl.ds(0, NZ - 1)], AG1)
-    left(xb.at[0, pl.ds(0, NT - 1)], X2)
-    left(xb.at[1, pl.ds(0, NT - 1)], X3)
-    left(pr2_src.at[pl.ds(0, NT - 1)], PR2)
+    left(xb.at[pl.ds(0, NT - 1)], X2)
+    left(pb.at[pl.ds(0, NT - 1)], X3)
+    left(pa_rcv, PR2)
     left(m_src.at[pl.ds(0, NZ - 1)], MIX)
     left(nb.at[pl.ds(0, NZ - 1)], NRM)
     left(rs2_src.at[pl.ds(0, NZ - 1)], RS2)
@@ -368,6 +384,17 @@
     y_left(d2, D2)
 
 
+def deliver(out_in, state_in, out, state_out, held, s_held, arrive, leave):
+    pairs = [(out_in, held, out)] + [(state_in.at[i], s_held.at[i], state_out.at[i]) for i in range(8)]
+    for i, (src, mid, _) in enumerate(pairs):
+        pltpu.make_async_copy(src, mid, arrive.at[i]).start()
+    for i, (src, mid, dst) in enumerate(pairs):
+        pltpu.make_async_copy(src, mid, arrive.at[i]).wait()
+        pltpu.make_async_copy(mid, dst, leave.at[i]).start()
+    for i, (_, mid, dst) in enumerate(pairs):
+        pltpu.make_async_copy(mid, dst, leave.at[i]).wait()
+
+
 def layer(res, state, gain1, gate1, up1, down1, gain2, wq, wk, wv, wg, wbeta, wdecay, rate, bias, hgain, wo, gain3, gate2, up2, down2):
     vmem = pl.BlockSpec(memory_space=pltpu.VMEM)
     args = (
@@ -375,19 +402,17 @@
         wq, wk, wv, wg, wbeta.T, wdecay.T, rate[None], bias[None], hgain[None], wo.T,
     )
     held = [args[i] for i in (0, 1, 2, 3, 4, 5, 6, 7, 15, 16, 17, 18, 19)]
-    out, k, corr, decay = pl.pallas_call(
+    hbm = pl.BlockSpec(memory_space=pltpu.HBM)
+    shapes = (jax.ShapeDtypeStruct((8, ROWS), BF), jax.ShapeDtypeStruct(state.shape, F32))
+    out, new_state = pl.pallas_call(
         kernel,
-        out_shape=(
-            jax.ShapeDtypeStruct((8, ROWS), BF),
-            jax.ShapeDtypeStruct((8, 2, HEAD), F32),
-            jax.ShapeDtypeStruct((8, 4, HEAD), F32),
-            jax.ShapeDtypeStruct((8, 4), F32),
-        ),
-        in_specs=[pl.BlockSpec(memory_space=pltpu.HBM)] * len(args),
-        out_specs=(vmem,) * 4,
+        out_shape=shapes,
+        in_specs=[hbm] * len(args),
+        out_specs=(vmem, hbm),
         scratch_shapes=[pltpu.VMEM(a.shape, a.dtype) for a in held]
         + [
             pltpu.SemaphoreType.DMA((len(args),)),
+            pltpu.SemaphoreType.DMA,
             pltpu.SemaphoreType.DMA((N_SEM,)),
             pltpu.SemaphoreType.DMA((N_SEM,)),
             pltpu.VMEM((NY, HID, 128), BF),
@@ -410,12 +435,13 @@
             pltpu.VMEM((NZ, GROUP // 8, 8, ROWS), BF),
             pltpu.VMEM((PLANE, 8, ROWS), BF),
             pltpu.VMEM((PLANE, 8, ROWS), BF),
-            pltpu.VMEM((2, NT, 8, ROWS), BF),
+            pltpu.VMEM((NT, 8, ROWS), BF),
             pltpu.VMEM((NZ, 8, MCOLS), BF),
             pltpu.VMEM((NZ, 8, MCOLS), BF),
             pltpu.VMEM((NZ, 8, 512), BF),
-            pltpu.VMEM((NT, 8, ROWS), BF),
-            pltpu.VMEM((NT, 8, ROWS), BF),
+            pltpu.VMEM((2, 4, 8, ROWS), BF),
+            pltpu.VMEM((4, 8, ROWS), BF),
+            pltpu.VMEM((NT, 4, 8, ROWS), BF),
             pltpu.VMEM((NZ, 8, 2 * FFP), BF),
             pltpu.VMEM((NZ, 8, 2 * FFP), BF),
             pltpu.VMEM((NZ, 8, FFP), BF),
@@ -424,8 +450,20 @@
         ],
         compiler_params=pltpu.CompilerParams(collective_id=0, has_side_effects=True, vmem_limit_bytes=67_043_328),
     )(*args)
-    keys = jnp.repeat(k, 2, axis=1)
-    return out.T, state * decay[:, :, None, None] + keys[:, :, :, None] * corr[:, :, None, :]
+    out, new_state = pl.pallas_call(
+        deliver,
+        out_shape=shapes,
+        in_specs=[hbm, hbm],
+        out_specs=(hbm, hbm),
+        scratch_shapes=[
+            pltpu.VMEM(out.shape, out.dtype),
+            pltpu.VMEM(state.shape, F32),
+            pltpu.SemaphoreType.DMA((9,)),
+            pltpu.SemaphoreType.DMA((9,)),
+        ],
+        compiler_params=pltpu.CompilerParams(vmem_limit_bytes=67_043_328),
+    )(out, new_state)
+    return out.T, new_state
 
 
 def solution(mesh):

time: 81 us -> 76.6 us (0.946)
  other arithmetic: 2.96 us -> 0 us
  local copies, waits for them, and re-layouts: 1.3 us -> 0 us
    add x1 -> x0, other arithmetic: 2.96 us -> none  [layer(): state * decay[:, :, None, None] + keys[:, :, :, None] * corr[:, :, None, :]]
    pallas_call x1 -> x2, Pallas kernels: 75.9 us -> 75.8 us  [the longest x1 73.4 us: layer(): pl.pallas_call(kernel, out_shape=shapes, in_specs=[hbm] * len(args), out_...]
where the time goes in v4:
time: 76.6 us; the launch traced here: 76.5 us
  Pallas kernels  75.8 us (99%)
    pallas_call x1, Pallas kernels, layer(): pl.pallas_call(kernel, out_shape=shapes, in_specs=[hbm] * len(args), out_...  73.4 us
    pallas_call x1, Pallas kernels, layer(): pl.pallas_call(deliver, out_shape=shapes, in_specs=[hbm, hbm], out_specs=...  2.42 us

profile of v4, /device:TPU:1, one launch (start us, length us, event | category | flops | bytes accessed | tf_op | source)
XLA Modules:
  0.0 76.5 jit_solution(14113732545375020094)
XLA Ops:
  0.6 73.4 %shard_map.212 = (bf16[8,256]{1,0:T(8,128)(2,1)}, f32[8,4,128,128]{3,2,1,0:T(8,128)}) custom-call(bf16[8,256]{1,0:T(8,128)(2,1)} %bitcast.18, f32[8,4,128,128]{3,2,1,0:T(8,128)} %state.1, f32[1,64]{1,0:T(1,128)} %bitcast.19, f32[1,64]{1,0:T(1,128)} %bitcast.20, f32[1,64]{1,0:T(1,128)} %bitcast.21, bf16[64,704]{1,0:T(8,128)(2,1)} %gate1_h.1, ...), custom_call_target="tpu_custom_call" | custom-call | tf_op jit(solution)/shard_map/pallas_call | solution.py:407
  74.1 2.4 %shard_map.213 = (bf16[8,256]{1,0:T(8,128)(2,1)}, f32[8,4,128,128]{3,2,1,0:T(8,128)}) custom-call(bf16[8,256]{1,0:T(8,128)(2,1)} %get-tuple-element.6.out_in, f32[8,4,128,128]{3,2,1,0:T(8,128)} %get-tuple-element.7.state_in), custom_call_target="tpu_custom_call" | custom-call | tf_op jit(solution)/shard_map/pallas_call | solution.py:453

commit v5 on v4

--- a/solution.py
+++ b/solution.py
@@ -47,11 +47,11 @@
     wq_h, wk_h, wv_h, wg_h, wbeta_h, wdecay_h, rate_h, bias_h, hgain_h, wo_h,
     out, state_out,
     res, s_buf, gain1, gain2, gain3, gate1, up1, down1, wbeta, wdecay, rate, bias, hgain,
-    in_sem, out_sem, send, recv,
+    in_sem, send, recv,
     gu_src, gu_rcv, dd_src, dd_rcv, gn, mw, wo, gu2, d2,
     a_w, d_w, g_col, g_row, xrow,
     xg, rs_src, rs_rcv, hg, pr1_src, pr1_rcv,
-    xb, m_src, m_rcv, nb, pa_src, pa_rcv, pb, rs2_src, rs2_rcv, hg2, pr3_src, pr3_rcv,
+    xb, m_src, m_rcv, nb, pa_src, pa_rcv, pb, rs2_src, rs2_rcv, hg2, pr3_src, pr3_rcv, place,
 ):
     kv = lax.axis_index("kv")
     t = lax.axis_index("tp")
@@ -69,21 +69,22 @@
     plane.sort(key=lambda o: -(FAR[o[0]] + FAR[o[1]]))
     plane_peers = [(ys[dy] * NT + ts[dx][dc], (z * NY + ys[dy], ts[dx][dc])) for dy, dx, dc in plane]
 
-    barrier = pltpu.get_barrier_semaphore()
-    greet = z_peers[:3] + plane_peers[:10] + z_peers[3:5] + plane_peers[10:] + z_peers[5:]
-    for _, peer in greet:
-        pl.semaphore_signal(barrier, inc=1, device_id=peer, device_id_type=MESH)
-
-    named = {}
-    for i, (src, dst) in enumerate((
+    inputs = (
         (gate1_h, gate1), (up1_h, up1), (res_h, res), (gain1_h, gain1), (gain2_h, gain2), (gain3_h, gain3), (down1_h, down1),
         (wbeta_h, wbeta), (wdecay_h, wdecay),
         (wq_h, mw.at[y, :, 0:256]), (wk_h, mw.at[y, :, 256:512]), (wv_h, mw.at[y, :, 512:1024]), (wg_h, mw.at[y, :, 1024:1536]),
         (wo_h, wo.at[y]), (gate2_h, gu2.at[y, 0]), (up2_h, gu2.at[y, 1]), (down2_h, d2.at[y]),
         (rate_h, rate), (bias_h, bias), (hgain_h, hgain), (state, s_buf),
-    )):
-        named[id(src)] = pltpu.make_async_copy(src, dst, in_sem.at[i])
+    )
+    named = {id(src): pltpu.make_async_copy(src, dst, in_sem.at[i]) for i, (src, dst) in enumerate(inputs)}
+    early = 6
+    for src, _ in inputs[:early]:
         named[id(src)].start()
+
+    barrier = pltpu.get_barrier_semaphore()
+    greet = z_peers[:3] + plane_peers[:10] + z_peers[3:5] + plane_peers[10:] + z_peers[5:]
+    for _, peer in greet:
+        pl.semaphore_signal(barrier, inc=1, device_id=peer, device_id_type=MESH)
 
     def ready(*refs):
         for ref in refs:
@@ -158,6 +159,8 @@
     deal(gu_src, gu_rcv, y, GU1, y_peers)
     share(xg, me, X1, plane_peers)
 
+    for src, _ in inputs[early:]:
+        named[id(src)].start()
     ready(down1_h)
     dd_src[...] = dot(down1[...], low, 0, 0).astype(BF).reshape(NY, HID, 128)
     sel_b = one_hot((iota((32, 128), 0) == iota((32, 128), 1) + 4 * t) & (iota((32, 128), 1) < 4))
@@ -306,9 +309,7 @@
             k_col = jnp.broadcast_to(k_t[m][:, i : i + 1], (HEAD, HEAD))
             for h in (2 * m, 2 * m + 1):
                 decay, corr = new[h]
-                s_buf[i, h] = s_buf[i, h] * decay[i : i + 1] + k_col * corr[i : i + 1]
-    store = pltpu.make_async_copy(s_buf, state_out, out_sem)
-    store.start()
+                state_out[i, h] = s_buf[i, h] * decay[i : i + 1] + k_col * corr[i : i + 1]
     y_done(wo, WO)
     arrived(nb.at[pl.ds(0, NZ - 1)], NRM)
     normed = nb[...].astype(F32).reshape(64, 512).astype(BF)
@@ -345,6 +346,9 @@
     hidden = silu(gate * scale) * (up * scale)
     hg2[z] = jnp.where(iota((8, FFP), 1) < FFT, hidden, 0.0).astype(BF)
     share(hg2, z, AG2, z_peers)
+    l, b = iota((128, ROWS), 0), iota((128, ROWS), 1)
+    for p in range(NY):
+        place[128 * p : 128 * (p + 1)] = one_hot((b == l + 24 * lax.shift_right_logical(l, 3) + 8 * p) & (l < 64))
     y_done(d2, D2)
     arrived(hg2.at[pl.ds(0, NZ - 1)], AG2)
     h = hg2[...].astype(F32).reshape(64, FFP).astype(BF)[:, 0:FFT]
@@ -353,15 +357,13 @@
     pr3_src[...] = part.reshape(PLANE, 8, 128).astype(BF)
     deal(pr3_src, pr3_rcv, me, PR3, plane_peers)
     arrived(pr3_rcv.at[pl.ds(0, PLANE - 1)], PR3)
-    final = jnp.zeros((8, ROWS), F32)
-    l, b = iota((128, ROWS), 0), iota((128, ROWS), 1)
+    pieces = []
     for p in range(NY):
         total = jnp.sum(pr3_rcv[NT * p : NT * (p + 1)].astype(F32), axis=0)
         base = pltpu.roll(pr3_rcv[NT * p].astype(F32), 64, 1)
-        place = one_hot((b == l + 24 * lax.shift_right_logical(l, 3) + 8 * p) & (l < 64))
-        final = final + dot((base + 0.5 * total).astype(BF), place, 1, 0)
+        pieces.append((base + 0.5 * total).astype(BF))
+    final = dot(jnp.concatenate(pieces, axis=1), place[...], 1, 0)
     out[...] = final.astype(BF)
-    store.wait()
 
     left(xg.at[pl.ds(0, PLANE - 1)], X1)
     left(pr1_src.at[pl.ds(0, PLANE - 1)], PR1)
@@ -384,15 +386,12 @@
     y_left(d2, D2)
 
 
-def deliver(out_in, state_in, out, state_out, held, s_held, arrive, leave):
-    pairs = [(out_in, held, out)] + [(state_in.at[i], s_held.at[i], state_out.at[i]) for i in range(8)]
-    for i, (src, mid, _) in enumerate(pairs):
-        pltpu.make_async_copy(src, mid, arrive.at[i]).start()
-    for i, (src, mid, dst) in enumerate(pairs):
-        pltpu.make_async_copy(src, mid, arrive.at[i]).wait()
-        pltpu.make_async_copy(mid, dst, leave.at[i]).start()
-    for i, (_, mid, dst) in enumerate(pairs):
-        pltpu.make_async_copy(mid, dst, leave.at[i]).wait()
+def deliver(out_in, state_in, out, state_out, sems):
+    copies = [pltpu.make_async_copy(out_in, out, sems.at[0]), pltpu.make_async_copy(state_in, state_out, sems.at[1])]
+    for copy in copies:
+        copy.start()
+    for copy in copies:
+        copy.wait()
 
 
 def layer(res, state, gain1, gate1, up1, down1, gain2, wq, wk, wv, wg, wbeta, wdecay, rate, bias, hgain, wo, gain3, gate2, up2, down2):
@@ -401,18 +400,18 @@
         res.T, state, gain1[None], gain2[None], gain3[None], gate1, up1, down1.T, gate2, up2, down2.T,
         wq, wk, wv, wg, wbeta.T, wdecay.T, rate[None], bias[None], hgain[None], wo.T,
     )
+    args = tuple(pltpu.with_memory_space_constraint(a, pltpu.HBM) for a in args)
     held = [args[i] for i in (0, 1, 2, 3, 4, 5, 6, 7, 15, 16, 17, 18, 19)]
     hbm = pl.BlockSpec(memory_space=pltpu.HBM)
     shapes = (jax.ShapeDtypeStruct((8, ROWS), BF), jax.ShapeDtypeStruct(state.shape, F32))
     out, new_state = pl.pallas_call(
         kernel,
-        out_shape=shapes,
+        out_shape=(pltpu.VMEM((8, ROWS), BF), pltpu.VMEM(state.shape, F32)),
         in_specs=[hbm] * len(args),
-        out_specs=(vmem, hbm),
+        out_specs=(vmem, vmem),
         scratch_shapes=[pltpu.VMEM(a.shape, a.dtype) for a in held]
         + [
             pltpu.SemaphoreType.DMA((len(args),)),
-            pltpu.SemaphoreType.DMA,
             pltpu.SemaphoreType.DMA((N_SEM,)),
             pltpu.SemaphoreType.DMA((N_SEM,)),
             pltpu.VMEM((NY, HID, 128), BF),
@@ -447,21 +446,17 @@
             pltpu.VMEM((NZ, 8, FFP), BF),
             pltpu.VMEM((PLANE, 8, 128), BF),
             pltpu.VMEM((PLANE, 8, 128), BF),
+            pltpu.VMEM((NY * 128, ROWS), BF),
         ],
-        compiler_params=pltpu.CompilerParams(collective_id=0, has_side_effects=True, vmem_limit_bytes=67_043_328),
+        compiler_params=pltpu.CompilerParams(collective_id=0, has_side_effects=True, vmem_limit_bytes=40 << 20),
     )(*args)
     out, new_state = pl.pallas_call(
         deliver,
         out_shape=shapes,
-        in_specs=[hbm, hbm],
+        in_specs=[vmem, vmem],
         out_specs=(hbm, hbm),
-        scratch_shapes=[
-            pltpu.VMEM(out.shape, out.dtype),
-            pltpu.VMEM(state.shape, F32),
-            pltpu.SemaphoreType.DMA((9,)),
-            pltpu.SemaphoreType.DMA((9,)),
-        ],
-        compiler_params=pltpu.CompilerParams(vmem_limit_bytes=67_043_328),
+        scratch_shapes=[pltpu.SemaphoreType.DMA((2,))],
+        compiler_params=pltpu.CompilerParams(vmem_limit_bytes=40 << 20),
     )(out, new_state)
     return out.T, new_state
 

time: 76.6 us -> 75 us (0.979)
  Pallas kernels: 75.8 us -> 74.2 us
    pallas_call x2, Pallas kernels: 75.8 us -> 74.2 us  [the longest x1 72.9 us: layer(): pl.pallas_call(kernel, out_shape=(pltpu.VMEM((8, ROWS), BF), pltpu.VMEM(s...]
where the time goes in v5:
time: 75 us; the launch traced here: 74.9 us
  Pallas kernels  74.2 us (99%)
    pallas_call x1, Pallas kernels, layer(): pl.pallas_call(kernel, out_shape=(pltpu.VMEM((8, ROWS), BF), pltpu.VMEM(s...  72.9 us

profile of v5, /device:TPU:1, one launch (start us, length us, event | category | flops | bytes accessed | tf_op | source)
XLA Modules:
  0.0 74.9 jit_solution(15287293568608747139)
XLA Ops:
  0.6 72.9 %shard_map.212 = (bf16[8,256]{1,0:T(8,128)(2,1)S(1)}, f32[8,4,128,128]{3,2,1,0:T(8,128)S(1)}) custom-call(bf16[8,256]{1,0:T(8,128)(2,1)} %bitcast.18, f32[8,4,128,128]{3,2,1,0:T(8,128)} %state.1, f32[1,64]{1,0:T(1,128)} %bitcast.19, f32[1,64]{1,0:T(1,128)} %bitcast.20, f32[1,64]{1,0:T(1,128)} %bitcast.21, bf16[64,704]{1,0:T(8,128)(2,1)} %gate1_h.1, ...), custom_call_target="tpu_custom_call" | custom-call | tf_op jit(solution)/shard_map/pallas_call | solution.py:407
  73.5 1.3 %shard_map.213 = (bf16[8,256]{1,0:T(8,128)(2,1)}, f32[8,4,128,128]{3,2,1,0:T(8,128)}) custom-call(bf16[8,256]{1,0:T(8,128)(2,1)S(1)} %get-tuple-element.6.out_in, f32[8,4,128,128]{3,2,1,0:T(8,128)S(1)} %get-tuple-element.7.state_in), custom_call_target="tpu_custom_call" | custom-call | tf_op jit(solution)/shard_map/pallas_call | solution.py:453

commit v6 on v5

--- a/solution.py
+++ b/solution.py
@@ -12,18 +12,16 @@
 PLANE = NY * NT
 KV = NZ * NY
 ROWS = 256
-KEEP, GROUP = 22, 24
-HID = NZ * KEEP
-PAD = NZ * GROUP
+HID, PITCH = 176, 192
 HEAD = 128
 
-X1, X2, X3, RS1, RS2, AG1, AG2, PR1, PR2, PR3, MIX, NRM, GU1, DD, GN = range(15)
-MW, WO, GU2, D2 = 15, 19, 23, 27
-N_SEM = 31
+X1, X2, X3, RS1, RS2, AG1, AG2, PR1, PR2, PR3, MIX, NRM, GU1, GN = range(14)
+D1, MW, WO, GU2, D2 = 14, 18, 22, 26, 30
+N_SEM = 34
 MCOLS = 1664
 FFT, FFP = 704, 768
 RING_Z = (4, 3, 5, 2, 6, 1, 7)
-FAR = (0, 1, 2, 1)
+FAR, FAR_Z = (0, 1, 2, 1), (0, 1, 2, 3, 4, 3, 2, 1)
 
 
 def dot(a, b, ca, cb):
@@ -48,10 +46,9 @@
     out, state_out,
     res, s_buf, gain1, gain2, gain3, gate1, up1, down1, wbeta, wdecay, rate, bias, hgain,
     in_sem, send, recv,
-    gu_src, gu_rcv, dd_src, dd_rcv, gn, mw, wo, gu2, d2,
-    a_w, d_w, g_col, g_row, xrow,
-    xg, rs_src, rs_rcv, hg, pr1_src, pr1_rcv,
-    xb, m_src, m_rcv, nb, pa_src, pa_rcv, pb, rs2_src, rs2_rcv, hg2, pr3_src, pr3_rcv, place,
+    gu_src, gu_rcv, gn, d1, mw, wo, gu2, d2,
+    g_row, xrow, xg, f_src, f_rcv, hg, pa_src, pa_rcv, pb,
+    m_src, m_rcv, nb, rs2_src, rs2_rcv, pr3_src, pr3_rcv, place,
 ):
     kv = lax.axis_index("kv")
     t = lax.axis_index("tp")
@@ -65,6 +62,9 @@
     z_peers = [(zs[o], (zs[o] * NY + y, t)) for o in RING_Z]
     y_peers = [(ys[o], (z * NY + ys[o], t)) for o in (2, 1, 3)]
     t_peers = [(ts[dx][dc], (kv, ts[dx][dc])) for dx in (2, 1, 3, 0) for dc in (0, 1) if dx or dc]
+    kv_peers = [(dz, dy) for dz in range(NZ) for dy in range(NY) if dz or dy]
+    kv_peers.sort(key=lambda o: -(FAR_Z[o[0]] + FAR[o[1]]))
+    kv_peers = [(zs[dz] * NY + ys[dy], (zs[dz] * NY + ys[dy], t)) for dz, dy in kv_peers]
     plane = [(dy, dx, dc) for dy in range(4) for dx in range(4) for dc in range(2) if dy or dx or dc]
     plane.sort(key=lambda o: -(FAR[o[0]] + FAR[o[1]]))
     plane_peers = [(ys[dy] * NT + ts[dx][dc], (z * NY + ys[dy], ts[dx][dc])) for dy, dx, dc in plane]
@@ -140,13 +140,24 @@
         left(first, k + 2)
         left(second, k + 3)
 
-    low = one_hot(iota((64, 128), 0) == iota((64, 128), 1))
-    high = one_hot(iota((64, 128), 0) + 64 == iota((64, 128), 1))
-    eye64 = iota((64, 64), 0) == iota((64, 64), 1)
+    lane = iota((64, FFP), 1)
+    pos = lane - PITCH * sum(jnp.where(lane >= PITCH * p, 1, 0) for p in range(1, NY))
+
+    def spread(v):
+        v = jnp.concatenate([v.astype(F32), jnp.zeros((64, FFP - FFT), F32)], axis=1)
+        w = v
+        for p in range(1, NY):
+            w = jnp.where(lane >= PITCH * p, pltpu.roll(v, (PITCH - HID) * p, 1), w)
+        return jnp.where(pos < HID, w, 0.0)
 
     ready(gate1_h, up1_h)
-    both = dot(gate1[...], low, 0, 0) + dot(up1[...], high, 0, 0)
-    gu_src[...] = both.astype(BF).reshape(NY, HID, 128)
+    gate, up = spread(gate1[...]), spread(up1[...])
+    first = iota((64, 2 * PITCH), 1) < PITCH
+    for h in range(2):
+        a = gate[:, 2 * PITCH * h : 2 * PITCH * (h + 1)]
+        b = pltpu.roll(up[:, 2 * PITCH * h : 2 * PITCH * (h + 1)], PITCH, 1)
+        gu_src[2 * h] = jnp.where(first, a, b).astype(BF)
+        gu_src[2 * h + 1] = jnp.where(first, b, a).astype(BF)
     ready(res_h, gain1_h, gain2_h, gain3_h)
     xg[me] = res[...]
     gn[y, 0:8] = jnp.broadcast_to(gain1[...], (8, 64))
@@ -162,94 +173,87 @@
     for src, _ in inputs[early:]:
         named[id(src)].start()
     ready(down1_h)
-    dd_src[...] = dot(down1[...], low, 0, 0).astype(BF).reshape(NY, HID, 128)
+    d1[y] = spread(down1[...]).astype(BF)
     sel_b = one_hot((iota((32, 128), 0) == iota((32, 128), 1) + 4 * t) & (iota((32, 128), 1) < 4))
     sel_d = one_hot((iota((32, 128), 0) == iota((32, 128), 1) - 4 + 4 * t) & (iota((32, 128), 1) >= 4) & (iota((32, 128), 1) < 8))
     ready(wbeta_h, wdecay_h)
     mw[y, :, 1536:MCOLS] = (dot(wbeta[...], sel_b, 0, 0) + dot(wdecay[...], sel_d, 0, 0)).astype(BF)
 
-    r, c = iota((PAD, HID), 0), iota((PAD, HID), 1)
-    group = jnp.zeros_like(r)
-    for i in range(1, NZ):
-        group = group + jnp.where(r >= GROUP * i, 1, 0)
-    pick = one_hot((c == r - (GROUP - KEEP) * group) & (r - GROUP * group < KEEP))
-    lane = iota((PAD, 128), 1)
+    eye64 = iota((64, 64), 0) == iota((64, 64), 1)
+    lane64 = iota((64, 128), 1)
 
     def column(p, i):
         row = gn[p, 8 * i : 8 * i + 1]
         return jnp.sum(jnp.where(eye64, jnp.broadcast_to(row, (64, 64)), 0.0), axis=1, keepdims=True)
 
     arrived(gn.at[pl.ds(0, NY - 1)], GN)
-    for p in range(NY):
-        g_col[64 * p : 64 * (p + 1)] = jnp.broadcast_to(column(p, 0), (64, ROWS))
-    arrived(gu_rcv.at[pl.ds(0, NY - 1)], GU1)
-    parts = [dot(pick, gu_rcv[p], 1, 0) for p in range(NY)]
-    for h in range(2):
-        a, b = parts[2 * h], parts[2 * h + 1]
-        a_w[0:PAD, 128 * h : 128 * (h + 1)] = jnp.where(lane < 64, a, pltpu.roll(b, 64, 1)).astype(BF)
-        a_w[PAD : 2 * PAD, 128 * h : 128 * (h + 1)] = jnp.where(lane < 64, pltpu.roll(a, 64, 1), b).astype(BF)
-
-    arrived(xg.at[pl.ds(0, PLANE - 1)], X1)
-    x0 = xg[...].astype(F32).reshape(ROWS, ROWS)
-    part = dot(a_w[...], (x0 * g_col[...]).astype(BF), 1, 0)
-    total = jnp.sum(x0 * x0, axis=0, keepdims=True)
-    coarse = total.astype(BF).astype(F32)
-    row = iota((NZ, GROUP, ROWS), 1)
-    gate = part[0:PAD].reshape(NZ, GROUP, ROWS)
-    up = part[PAD : 2 * PAD].reshape(NZ, GROUP, ROWS)
-    gate = jnp.where(row == KEEP, coarse.reshape(1, 1, ROWS), gate)
-    gate = jnp.where(row == KEEP + 1, (total - coarse).reshape(1, 1, ROWS), gate)
-    rs_src[...] = jnp.concatenate([gate, up], axis=1).astype(BF).reshape(NZ, 2 * GROUP // 8, 8, ROWS)
-    deal(rs_src, rs_rcv, z, RS1, z_peers)
-
-    for p, peer in y_peers:
-        put(dd_src.at[p], dd_rcv.at[y], DD, peer)
-    dd_rcv[y] = dd_src[y]
-    ready(wq_h, wk_h, wv_h, wg_h)
-    y_start(mw, MW)
-    xrow[...] = jnp.transpose(x0).reshape(KV, 8, ROWS).astype(BF)
-    lane64 = iota((64, 128), 1)
-    for i in range(2):
+    for i in range(3):
         for h in range(2):
-            spread = jnp.where(lane64 == iota((64, 128), 0), column(2 * h, i + 1), 0.0)
-            spread = spread + jnp.where(lane64 == iota((64, 128), 0) + 64, column(2 * h + 1, i + 1), 0.0)
-            g_row[i, :, 128 * h : 128 * (h + 1)] = jnp.broadcast_to(jnp.sum(spread, axis=0, keepdims=True), (8, 128))
-
-    arrived(rs_rcv.at[pl.ds(0, NZ - 1)], RS1)
-    both = jnp.sum(rs_rcv[...].astype(F32), axis=0).reshape(2 * GROUP, ROWS)
-    gate, up = both[0:GROUP], both[GROUP:]
-    scale = lax.rsqrt((gate[KEEP : KEEP + 1] + gate[KEEP + 1 : KEEP + 2]) / D + EPS)
-    hidden = silu(gate * scale) * (up * scale)
-    hidden = jnp.where(iota((GROUP, ROWS), 0) < KEEP, hidden, 0.0)
-    hg[z] = hidden.reshape(GROUP // 8, 8, ROWS).astype(BF)
-    share(hg, z, AG1, z_peers)
-
-    arrived(dd_rcv.at[pl.ds(0, NY - 1)], DD)
-    for h in range(2):
-        a, b = dot(pick, dd_rcv[2 * h], 1, 0), dot(pick, dd_rcv[2 * h + 1], 1, 0)
-        d_w[:, 128 * h : 128 * (h + 1)] = (a + pltpu.roll(b, 64, 1)).astype(BF)
-    y_pass(mw, MW)
-    arrived(hg.at[pl.ds(0, NZ - 1)], AG1)
-    h = hg[...].astype(F32).reshape(PAD, ROWS).astype(BF)
-    pr1_src[...] = dot(h, d_w[...], 0, 0).reshape(KV, 8, ROWS).astype(BF)
-    for (dy, dx, dc), (_, peer) in zip(plane, plane_peers):
-        put(pr1_src.at[ts[dx][dc] * NY + ys[dy]], pr1_rcv.at[me], PR1, peer)
-    pr1_rcv[me] = pr1_src[t * NY + y]
-    arrived(pr1_rcv.at[pl.ds(0, PLANE - 1)], PR1)
-    branch = jnp.sum(pr1_rcv[...].astype(F32), axis=0)
-    own1 = (xrow[t * NY + y].astype(F32) + 0.5 * branch).astype(BF)
+            wide = jnp.where(lane64 == iota((64, 128), 0), column(2 * h, i), 0.0)
+            wide = wide + jnp.where(lane64 == iota((64, 128), 0) + 64, column(2 * h + 1, i), 0.0)
+            g_row[i, :, 128 * h : 128 * (h + 1)] = jnp.broadcast_to(jnp.sum(wide, axis=0, keepdims=True), (8, 128))
 
     def scaled_of(v, i):
         squares = jnp.sum(v * v, axis=1, keepdims=True)
         coarse = squares.astype(BF).astype(F32)
         return (v * g_row[i, 0:1]).astype(BF), coarse, squares - coarse
 
-    xb[t] = own1
-    share(xb, t, X2, t_peers)
+    arrived(xg.at[pl.ds(0, PLANE - 1)], X1)
+    x0 = jnp.transpose(xg[...].astype(F32).reshape(ROWS, ROWS))
+    scaled, coarse, fine = scaled_of(x0, 0)
+    arrived(gu_rcv.at[pl.ds(0, NY - 1)], GU1)
+    part = dot(scaled, gu_rcv[...].reshape(ROWS, 2 * PITCH), 1, 0)
+    at = iota((ROWS, 2 * PITCH), 1)
+    part = part + jnp.where(at == HID, coarse, 0.0) + jnp.where(at == HID + 1, fine, 0.0)
+    f_src[...] = part.reshape(KV, 8, 2 * PITCH).astype(BF)
+    deal(f_src, f_rcv, kv, RS1, kv_peers)
+    y_start(d1, D1)
+    ready(wq_h, wk_h, wv_h, wg_h)
+    y_start(mw, MW)
+    xrow[...] = x0.reshape(NZ, NY, 8, ROWS).astype(BF)
+    arrived(f_rcv.at[pl.ds(0, KV - 1)], RS1)
+    quarters = jnp.sum(f_rcv[...].astype(F32).reshape(NZ, NY, 8, 2 * PITCH), axis=0)
+    scale = lax.rsqrt((quarters[0, :, HID : HID + 1] + quarters[0, :, HID + 1 : HID + 2]) / D + EPS)
+    at = iota((8, 2 * PITCH), 1)
+    pos = at - PITCH * jnp.where(at >= PITCH, 1, 0)
+    for h in range(2):
+        a, b = quarters[2 * h], quarters[2 * h + 1]
+        gate = jnp.where(at < PITCH, a, b) * scale
+        up = pltpu.roll(jnp.where(at < PITCH, b, a), PITCH, 1) * scale
+        hg[0, z, :, 2 * PITCH * h : 2 * PITCH * (h + 1)] = jnp.where(pos < HID, silu(gate) * up, 0.0).astype(BF)
+    share(hg.at[0], z, AG1, z_peers)
+    y_pass(d1, D1)
+    y_pass(mw, MW)
+    y_done(d1, D1)
+
+    def gathered_hidden(i, k):
+        arrived(hg.at[i, pl.ds(0, NZ - 1)], k)
+        return hg[i].astype(F32).reshape(64, FFP).astype(BF)
+
+    def swap(part, i, k):
+        pa_src[i] = part.reshape(2, 4, 8, ROWS).astype(BF)
+        put(pa_src.at[i, 1 - core], pa_rcv.at[i], k, (kv, ts[0][1]))
+        mine = jnp.where(core == 0, part[0:32], part[32:64])
+        arrived(pa_rcv.at[i], k)
+        pb[i, t] = (mine.reshape(4, 8, ROWS) + pa_rcv[i].astype(F32)).astype(BF)
+
+    def everyones(i, k):
+        arrived(pb.at[i, pl.ds(0, NT - 1)], k)
+        branch = []
+        for c in range(2):
+            half = pb[i, c].astype(F32)
+            for j in range(1, 4):
+                half = half + pb[i, 2 * j + c].astype(F32)
+            branch.append(half.reshape(32, ROWS))
+        return jnp.concatenate(branch, axis=0)
+
+    h = gathered_hidden(0, AG1)
+    swap(dot(h, d1[...].reshape(ROWS, FFP), 1, 1), 0, PR1)
+    share(pb.at[0], t, X2, t_peers)
     y_done(mw, MW)
-    arrived(xb.at[pl.ds(0, NT - 1)], X2)
-    x1 = xb[...].astype(F32).reshape(64, ROWS)
-    scaled, coarse, fine = scaled_of(x1, 0)
+    x1 = xrow[:, y].astype(F32).reshape(64, ROWS)
+    x1 = (x1 + 0.5 * everyones(0, X2)).astype(BF).astype(F32)
+    scaled, coarse, fine = scaled_of(x1, 1)
     last = iota((64, 128), 1)
     for a, b in ((0, 512), (512, 1024), (1024, 1536), (1536, MCOLS)):
         part = dot(scaled, mw[:, :, a:b].reshape(ROWS, b - a), 1, 0)
@@ -267,15 +271,16 @@
     rowscale = lax.rsqrt((ext[:, 8:9] + ext[:, 9:10]) / D + EPS)
     heads = [mixed[:, 128 * i : 128 * (i + 1)] * rowscale for i in range(12)]
 
-    def unit(v):
-        a = silu(v)
-        return a * lax.rsqrt(jnp.sum(a * a, axis=-1, keepdims=True) + EPS)
-
-    q = [unit(heads[m]) * HEAD**-0.5 for m in range(2)]
-    k = [unit(heads[2 + m]) for m in range(2)]
+    def factor(v):
+        return lax.rsqrt(jnp.sum(v * v, axis=-1, keepdims=True) + EPS)
+
+    q = [silu(heads[m]) for m in range(2)]
+    k = [silu(heads[2 + m]) for m in range(2)]
     q_t = [jnp.transpose(v) for v in q]
     k_t = [jnp.transpose(v) for v in k]
-    kq = [jnp.sum(k[m] * q[m], axis=-1, keepdims=True) for m in range(2)]
+    q_f = [factor(v) * HEAD**-0.5 for v in q]
+    k_f = [factor(v) for v in k]
+    kq = [jnp.sum(k[m] * q[m], axis=-1, keepdims=True) * k_f[m] * q_f[m] for m in range(2)]
     ext = ext * rowscale
     by_k, by_q = [[] for _ in range(4)], [[] for _ in range(4)]
     for m in range(2):
@@ -295,11 +300,11 @@
         pre = ext[:, 4 + h : 5 + h] + bias[:, h : h + 1]
         soft = jnp.maximum(pre, 0.0) + jnp.log1p(jnp.exp(-jnp.abs(pre)))
         decay = jnp.exp(-jnp.exp(rate[:, h : h + 1]) * soft)
-        corr = beta * (val - decay * jnp.concatenate(by_k[h], axis=0))
-        reading = decay * jnp.concatenate(by_q[h], axis=0) + kq[m] * corr
+        corr = beta * (val - decay * k_f[m] * jnp.concatenate(by_k[h], axis=0))
+        reading = decay * q_f[m] * jnp.concatenate(by_q[h], axis=0) + kq[m] * corr
         norm = lax.rsqrt(jnp.mean(reading * reading, axis=-1, keepdims=True) + EPS)
         nb[z, :, 128 * h : 128 * (h + 1)] = (reading * norm * hgain[...] * gate).astype(BF)
-        new.append((decay, corr))
+        new.append((decay, corr * k_f[m]))
     share(nb, z, NRM, z_peers)
     y_pass(wo, WO)
     y_pass(gu2, GU2)
@@ -314,23 +319,12 @@
     arrived(nb.at[pl.ds(0, NZ - 1)], NRM)
     normed = nb[...].astype(F32).reshape(64, 512).astype(BF)
     part = dot(normed, wo[...].reshape(ROWS, 512), 1, 1)
-    pa_src[...] = part.reshape(2, 4, 8, ROWS).astype(BF)
-    put(pa_src.at[1 - core], pa_rcv, PR2, (kv, ts[0][1]))
-    mine = jnp.where(core == 0, part[0:32], part[32:64])
-    arrived(pa_rcv, PR2)
-    pb[t] = (mine.reshape(4, 8, ROWS) + pa_rcv[...].astype(F32)).astype(BF)
-    share(pb, t, X3, t_peers)
+    swap(part, 1, PR2)
+    share(pb.at[1], t, X3, t_peers)
     y_done(gu2, GU2)
-    arrived(pb.at[pl.ds(0, NT - 1)], X3)
-    branch = []
-    for c in range(2):
-        half = pb[c].astype(F32)
-        for i in range(1, 4):
-            half = half + pb[2 * i + c].astype(F32)
-        branch.append(half.reshape(32, ROWS))
-
-    x3 = (x1 + jnp.concatenate(branch, axis=0)).astype(BF).astype(F32)
-    scaled, coarse, fine = scaled_of(x3, 1)
+
+    x3 = (x1 + everyones(1, X3)).astype(BF).astype(F32)
+    scaled, coarse, fine = scaled_of(x3, 2)
     gate = dot(scaled, gu2[:, 0].reshape(ROWS, FFT), 1, 0)
     up = dot(scaled, gu2[:, 1].reshape(ROWS, FFT), 1, 0)
     fill = jnp.where(iota((64, 64), 1) == 0, coarse, jnp.where(iota((64, 64), 1) == 1, fine, 0.0))
@@ -344,14 +338,13 @@
     gate, up = both[:, 0:FFP], both[:, FFP:]
     scale = lax.rsqrt((gate[:, FFT : FFT + 1] + gate[:, FFT + 1 : FFT + 2]) / D + EPS)
     hidden = silu(gate * scale) * (up * scale)
-    hg2[z] = jnp.where(iota((8, FFP), 1) < FFT, hidden, 0.0).astype(BF)
-    share(hg2, z, AG2, z_peers)
+    hg[1, z] = jnp.where(iota((8, FFP), 1) < FFT, hidden, 0.0).astype(BF)
+    share(hg.at[1], z, AG2, z_peers)
     l, b = iota((128, ROWS), 0), iota((128, ROWS), 1)
     for p in range(NY):
         place[128 * p : 128 * (p + 1)] = one_hot((b == l + 24 * lax.shift_right_logical(l, 3) + 8 * p) & (l < 64))
     y_done(d2, D2)
-    arrived(hg2.at[pl.ds(0, NZ - 1)], AG2)
-    h = hg2[...].astype(F32).reshape(64, FFP).astype(BF)[:, 0:FFT]
+    h = gathered_hidden(1, AG2)[:, 0:FFT]
     h = jnp.concatenate([h, jnp.zeros((64, FFT), BF)], axis=0)
     part = dot(d2[...].reshape(ROWS, FFT), h, 1, 1) + x3_t
     pr3_src[...] = part.reshape(PLANE, 8, 128).astype(BF)
@@ -366,20 +359,18 @@
     out[...] = final.astype(BF)
 
     left(xg.at[pl.ds(0, PLANE - 1)], X1)
-    left(pr1_src.at[pl.ds(0, PLANE - 1)], PR1)
+    left(f_src.at[pl.ds(0, KV - 1)], RS1)
     left(pr3_src.at[pl.ds(0, PLANE - 1)], PR3)
-    left(rs_src.at[pl.ds(0, NZ - 1)], RS1)
-    left(hg.at[pl.ds(0, NZ - 1)], AG1)
-    left(xb.at[pl.ds(0, NT - 1)], X2)
-    left(pb.at[pl.ds(0, NT - 1)], X3)
-    left(pa_rcv, PR2)
+    for i, (ag, pr, xx) in enumerate(((AG1, PR1, X2), (AG2, PR2, X3))):
+        left(hg.at[i, pl.ds(0, NZ - 1)], ag)
+        left(pa_rcv.at[i], pr)
+        left(pb.at[i, pl.ds(0, NT - 1)], xx)
     left(m_src.at[pl.ds(0, NZ - 1)], MIX)
     left(nb.at[pl.ds(0, NZ - 1)], NRM)
     left(rs2_src.at[pl.ds(0, NZ - 1)], RS2)
-    left(hg2.at[pl.ds(0, NZ - 1)], AG2)
     left(gu_src.at[pl.ds(0, NY - 1)], GU1)
-    left(dd_src.at[pl.ds(0, NY - 1)], DD)
     left(gn.at[pl.ds(0, NY - 1)], GN)
+    y_left(d1, D1)
     y_left(mw, MW)
     y_left(wo, WO)
     y_left(gu2, GU2)
@@ -414,36 +405,28 @@
             pltpu.SemaphoreType.DMA((len(args),)),
             pltpu.SemaphoreType.DMA((N_SEM,)),
             pltpu.SemaphoreType.DMA((N_SEM,)),
-            pltpu.VMEM((NY, HID, 128), BF),
-            pltpu.VMEM((NY, HID, 128), BF),
-            pltpu.VMEM((NY, HID, 128), BF),
-            pltpu.VMEM((NY, HID, 128), BF),
+            pltpu.VMEM((NY, 64, 2 * PITCH), BF),
+            pltpu.VMEM((NY, 64, 2 * PITCH), BF),
             pltpu.VMEM((NY, 24, 64), F32),
+            pltpu.VMEM((NY, 64, FFP), BF),
             pltpu.VMEM((NY, 64, MCOLS), BF),
             pltpu.VMEM((NY, 64, 512), BF),
             pltpu.VMEM((NY, 2, 64, FFT), BF),
             pltpu.VMEM((NY, 64, FFT), BF),
-            pltpu.VMEM((2 * PAD, ROWS), BF),
-            pltpu.VMEM((PAD, ROWS), BF),
-            pltpu.VMEM((ROWS, ROWS), F32),
-            pltpu.VMEM((2, 8, ROWS), F32),
-            pltpu.VMEM((KV, 8, ROWS), BF),
+            pltpu.VMEM((3, 8, ROWS), F32),
+            pltpu.VMEM((NZ, NY, 8, ROWS), BF),
             pltpu.VMEM((PLANE, 8, ROWS), BF),
-            pltpu.VMEM((NZ, 2 * GROUP // 8, 8, ROWS), BF),
-            pltpu.VMEM((NZ, 2 * GROUP // 8, 8, ROWS), BF),
-            pltpu.VMEM((NZ, GROUP // 8, 8, ROWS), BF),
-            pltpu.VMEM((PLANE, 8, ROWS), BF),
-            pltpu.VMEM((PLANE, 8, ROWS), BF),
-            pltpu.VMEM((NT, 8, ROWS), BF),
+            pltpu.VMEM((KV, 8, 2 * PITCH), BF),
+            pltpu.VMEM((KV, 8, 2 * PITCH), BF),
+            pltpu.VMEM((2, NZ, 8, FFP), BF),
+            pltpu.VMEM((2, 2, 4, 8, ROWS), BF),
+            pltpu.VMEM((2, 4, 8, ROWS), BF),
+            pltpu.VMEM((2, NT, 4, 8, ROWS), BF),
             pltpu.VMEM((NZ, 8, MCOLS), BF),
             pltpu.VMEM((NZ, 8, MCOLS), BF),
             pltpu.VMEM((NZ, 8, 512), BF),
-            pltpu.VMEM((2, 4, 8, ROWS), BF),
-            pltpu.VMEM((4, 8, ROWS), BF),
-            pltpu.VMEM((NT, 4, 8, ROWS), BF),
             pltpu.VMEM((NZ, 8, 2 * FFP), BF),
             pltpu.VMEM((NZ, 8, 2 * FFP), BF),
-            pltpu.VMEM((NZ, 8, FFP), BF),
             pltpu.VMEM((PLANE, 8, 128), BF),
             pltpu.VMEM((PLANE, 8, 128), BF),
             pltpu.VMEM((NY * 128, ROWS), BF),

time: 75 us -> 72.8 us (0.971)
  Pallas kernels: 74.2 us -> 72 us
    pallas_call x1, Pallas kernels: 72.9 us -> 70.6 us  [layer(): pl.pallas_call(kernel, out_shape=(pltpu.VMEM((8, ROWS), BF), pltpu.VMEM(s...]
where the time goes in v6:
time: 72.8 us; the launch traced here: 72.6 us
  Pallas kernels  72 us (99%)
    pallas_call x1, Pallas kernels, layer(): pl.pallas_call(kernel, out_shape=(pltpu.VMEM((8, ROWS), BF), pltpu.VMEM(s...  70.6 us

profile of v6, /device:TPU:1, one launch (start us, length us, event | category | flops | bytes accessed | tf_op | source)
XLA Modules:
  0.0 72.6 jit_solution(2479240491035814297)
XLA Ops:
  0.6 70.6 %shard_map.212 = (bf16[8,256]{1,0:T(8,128)(2,1)S(1)}, f32[8,4,128,128]{3,2,1,0:T(8,128)S(1)}) custom-call(bf16[8,256]{1,0:T(8,128)(2,1)} %bitcast.18, f32[8,4,128,128]{3,2,1,0:T(8,128)} %state.1, f32[1,64]{1,0:T(1,128)} %bitcast.19, f32[1,64]{1,0:T(1,128)} %bitcast.20, f32[1,64]{1,0:T(1,128)} %bitcast.21, bf16[64,704]{1,0:T(8,128)(2,1)} %gate1_h.1, ...), custom_call_target="tpu_custom_call" | custom-call | tf_op jit(solution)/shard_map/pallas_call | solution.py:398
  71.3 1.3 %shard_map.213 = (bf16[8,256]{1,0:T(8,128)(2,1)}, f32[8,4,128,128]{3,2,1,0:T(8,128)}) custom-call(bf16[8,256]{1,0:T(8,128)(2,1)S(1)} %get-tuple-element.6.out_in, f32[8,4,128,128]{3,2,1,0:T(8,128)S(1)} %get-tuple-element.7.state_in), custom_call_target="tpu_custom_call" | custom-call | tf_op jit(solution)/shard_map/pallas_call | solution.py:436

commit v7 on v6

--- a/solution.py
+++ b/solution.py
@@ -15,10 +15,11 @@
 HID, PITCH = 176, 192
 HEAD = 128
 
-X1, X2, X3, RS1, RS2, AG1, AG2, PR1, PR2, PR3, MIX, NRM, GU1, GN = range(14)
-D1, MW, WO, GU2, D2 = 14, 18, 22, 26, 30
-N_SEM = 34
+X1, X2, X3, RS1, RS2, AG1, AG2, PR1, PR2, PR3, MIX, VG, NRM, GU1, GN = range(15)
+D1, MW, WO, GU2, D2 = 15, 19, 23, 27, 31
+N_SEM = 35
 MCOLS = 1664
+QK = 640
 FFT, FFP = 704, 768
 RING_Z = (4, 3, 5, 2, 6, 1, 7)
 FAR, FAR_Z = (0, 1, 2, 1), (0, 1, 2, 3, 4, 3, 2, 1)
@@ -48,7 +49,7 @@
     in_sem, send, recv,
     gu_src, gu_rcv, gn, d1, mw, wo, gu2, d2,
     g_row, xrow, xg, f_src, f_rcv, hg, pa_src, pa_rcv, pb,
-    m_src, m_rcv, nb, rs2_src, rs2_rcv, pr3_src, pr3_rcv, place,
+    m_src, m_rcv, v_src, v_rcv, nb, rs2_src, rs2_rcv, pr3_src, pr3_rcv, place,
 ):
     kv = lax.axis_index("kv")
     t = lax.axis_index("tp")
@@ -72,7 +73,7 @@
     inputs = (
         (gate1_h, gate1), (up1_h, up1), (res_h, res), (gain1_h, gain1), (gain2_h, gain2), (gain3_h, gain3), (down1_h, down1),
         (wbeta_h, wbeta), (wdecay_h, wdecay),
-        (wq_h, mw.at[y, :, 0:256]), (wk_h, mw.at[y, :, 256:512]), (wv_h, mw.at[y, :, 512:1024]), (wg_h, mw.at[y, :, 1024:1536]),
+        (wq_h, mw.at[y, :, 0:256]), (wk_h, mw.at[y, :, 256:512]), (wv_h, mw.at[y, :, 640:1152]), (wg_h, mw.at[y, :, 1152:MCOLS]),
         (wo_h, wo.at[y]), (gate2_h, gu2.at[y, 0]), (up2_h, gu2.at[y, 1]), (down2_h, d2.at[y]),
         (rate_h, rate), (bias_h, bias), (hgain_h, hgain), (state, s_buf),
     )
@@ -160,15 +161,16 @@
         gu_src[2 * h + 1] = jnp.where(first, b, a).astype(BF)
     ready(res_h, gain1_h, gain2_h, gain3_h)
     xg[me] = res[...]
-    gn[y, 0:8] = jnp.broadcast_to(gain1[...], (8, 64))
-    gn[y, 8:16] = jnp.broadcast_to(gain2[...], (8, 64))
-    gn[y, 16:24] = jnp.broadcast_to(gain3[...], (8, 64))
+    gn[y, 0:1] = gain1[...]
+    gn[y, 1:2] = gain2[...]
+    gn[y, 2:3] = gain3[...]
 
     pl.semaphore_wait(barrier, len(greet))
 
     share(gn, y, GN, y_peers)
+    share(xg, me, X1, plane_peers[:18])
     deal(gu_src, gu_rcv, y, GU1, y_peers)
-    share(xg, me, X1, plane_peers)
+    share(xg, me, X1, plane_peers[18:])
 
     for src, _ in inputs[early:]:
         named[id(src)].start()
@@ -177,13 +179,13 @@
     sel_b = one_hot((iota((32, 128), 0) == iota((32, 128), 1) + 4 * t) & (iota((32, 128), 1) < 4))
     sel_d = one_hot((iota((32, 128), 0) == iota((32, 128), 1) - 4 + 4 * t) & (iota((32, 128), 1) >= 4) & (iota((32, 128), 1) < 8))
     ready(wbeta_h, wdecay_h)
-    mw[y, :, 1536:MCOLS] = (dot(wbeta[...], sel_b, 0, 0) + dot(wdecay[...], sel_d, 0, 0)).astype(BF)
+    mw[y, :, 512:QK] = (dot(wbeta[...], sel_b, 0, 0) + dot(wdecay[...], sel_d, 0, 0)).astype(BF)
 
     eye64 = iota((64, 64), 0) == iota((64, 64), 1)
     lane64 = iota((64, 128), 1)
 
     def column(p, i):
-        row = gn[p, 8 * i : 8 * i + 1]
+        row = gn[p, i : i + 1]
         return jnp.sum(jnp.where(eye64, jnp.broadcast_to(row, (64, 64)), 0.0), axis=1, keepdims=True)
 
     arrived(gn.at[pl.ds(0, NY - 1)], GN)
@@ -211,6 +213,7 @@
     ready(wq_h, wk_h, wv_h, wg_h)
     y_start(mw, MW)
     xrow[...] = x0.reshape(NZ, NY, 8, ROWS).astype(BF)
+    y_pass(d1, D1)
     arrived(f_rcv.at[pl.ds(0, KV - 1)], RS1)
     quarters = jnp.sum(f_rcv[...].astype(F32).reshape(NZ, NY, 8, 2 * PITCH), axis=0)
     scale = lax.rsqrt((quarters[0, :, HID : HID + 1] + quarters[0, :, HID + 1 : HID + 2]) / D + EPS)
@@ -222,7 +225,6 @@
         up = pltpu.roll(jnp.where(at < PITCH, b, a), PITCH, 1) * scale
         hg[0, z, :, 2 * PITCH * h : 2 * PITCH * (h + 1)] = jnp.where(pos < HID, silu(gate) * up, 0.0).astype(BF)
     share(hg.at[0], z, AG1, z_peers)
-    y_pass(d1, D1)
     y_pass(mw, MW)
     y_done(d1, D1)
 
@@ -255,21 +257,24 @@
     x1 = (x1 + 0.5 * everyones(0, X2)).astype(BF).astype(F32)
     scaled, coarse, fine = scaled_of(x1, 1)
     last = iota((64, 128), 1)
-    for a, b in ((0, 512), (512, 1024), (1024, 1536), (1536, MCOLS)):
-        part = dot(scaled, mw[:, :, a:b].reshape(ROWS, b - a), 1, 0)
-        if a == 1536:
-            part = part + jnp.where(last == 8, coarse, 0.0) + jnp.where(last == 9, fine, 0.0)
-        m_src[:, :, a:b] = part.reshape(NZ, 8, b - a).astype(BF)
+    part = dot(scaled, mw[:, :, 0:512].reshape(ROWS, 512), 1, 0)
+    m_src[:, :, 0:512] = part.reshape(NZ, 8, 512).astype(BF)
+    part = dot(scaled, mw[:, :, 512:QK].reshape(ROWS, 128), 1, 0)
+    part = part + jnp.where(last == 8, coarse, 0.0) + jnp.where(last == 9, fine, 0.0)
+    m_src[:, :, 512:QK] = part.reshape(NZ, 8, 128).astype(BF)
     deal(m_src, m_rcv, z, MIX, z_peers)
+    part = dot(scaled, mw[:, :, QK:MCOLS].reshape(ROWS, 1024), 1, 0)
+    v_src[...] = part.reshape(NZ, 8, 1024).astype(BF)
+    deal(v_src, v_rcv, z, VG, z_peers)
     ready(wo_h, gate2_h, up2_h, down2_h, state, rate_h, bias_h, hgain_h)
     y_start(wo, WO)
     y_start(gu2, GU2)
     arrived(m_rcv.at[pl.ds(0, NZ - 1)], MIX)
 
     mixed = jnp.sum(m_rcv[...].astype(F32), axis=0)
-    ext = mixed[:, 1536:MCOLS]
+    ext = mixed[:, 512:QK]
     rowscale = lax.rsqrt((ext[:, 8:9] + ext[:, 9:10]) / D + EPS)
-    heads = [mixed[:, 128 * i : 128 * (i + 1)] * rowscale for i in range(12)]
+    heads = [mixed[:, 128 * i : 128 * (i + 1)] * rowscale for i in range(4)]
 
     def factor(v):
         return lax.rsqrt(jnp.sum(v * v, axis=-1, keepdims=True) + EPS)
@@ -291,17 +296,26 @@
                 s = s_buf[i, h]
                 by_k[h].append(jnp.sum(s * k_col, axis=0, keepdims=True))
                 by_q[h].append(jnp.sum(s * q_col, axis=0, keepdims=True))
-    new = []
+    gates = []
     for h in range(4):
-        m = h // 2
-        val = silu(heads[4 + h])
-        gate = silu(heads[8 + h])
         beta = 1.0 / (1.0 + jnp.exp(-ext[:, h : h + 1]))
         pre = ext[:, 4 + h : 5 + h] + bias[:, h : h + 1]
         soft = jnp.maximum(pre, 0.0) + jnp.log1p(jnp.exp(-jnp.abs(pre)))
         decay = jnp.exp(-jnp.exp(rate[:, h : h + 1]) * soft)
-        corr = beta * (val - decay * k_f[m] * jnp.concatenate(by_k[h], axis=0))
-        reading = decay * q_f[m] * jnp.concatenate(by_q[h], axis=0) + kq[m] * corr
+        by_k[h] = decay * k_f[h // 2] * jnp.concatenate(by_k[h], axis=0)
+        by_q[h] = decay * q_f[h // 2] * jnp.concatenate(by_q[h], axis=0)
+        gates.append((beta, decay))
+    arrived(v_rcv.at[pl.ds(0, NZ - 1)], VG)
+    mixed = jnp.sum(v_rcv[...].astype(F32), axis=0)
+    heads = [mixed[:, 128 * i : 128 * (i + 1)] * rowscale for i in range(8)]
+    new = []
+    for h in range(4):
+        m = h // 2
+        beta, decay = gates[h]
+        val = silu(heads[h])
+        gate = silu(heads[4 + h])
+        corr = beta * (val - by_k[h])
+        reading = by_q[h] + kq[m] * corr
         norm = lax.rsqrt(jnp.mean(reading * reading, axis=-1, keepdims=True) + EPS)
         nb[z, :, 128 * h : 128 * (h + 1)] = (reading * norm * hgain[...] * gate).astype(BF)
         new.append((decay, corr * k_f[m]))
@@ -349,23 +363,14 @@
     part = dot(d2[...].reshape(ROWS, FFT), h, 1, 1) + x3_t
     pr3_src[...] = part.reshape(PLANE, 8, 128).astype(BF)
     deal(pr3_src, pr3_rcv, me, PR3, plane_peers)
-    arrived(pr3_rcv.at[pl.ds(0, PLANE - 1)], PR3)
-    pieces = []
-    for p in range(NY):
-        total = jnp.sum(pr3_rcv[NT * p : NT * (p + 1)].astype(F32), axis=0)
-        base = pltpu.roll(pr3_rcv[NT * p].astype(F32), 64, 1)
-        pieces.append((base + 0.5 * total).astype(BF))
-    final = dot(jnp.concatenate(pieces, axis=1), place[...], 1, 0)
-    out[...] = final.astype(BF)
-
     left(xg.at[pl.ds(0, PLANE - 1)], X1)
     left(f_src.at[pl.ds(0, KV - 1)], RS1)
-    left(pr3_src.at[pl.ds(0, PLANE - 1)], PR3)
     for i, (ag, pr, xx) in enumerate(((AG1, PR1, X2), (AG2, PR2, X3))):
         left(hg.at[i, pl.ds(0, NZ - 1)], ag)
         left(pa_rcv.at[i], pr)
         left(pb.at[i, pl.ds(0, NT - 1)], xx)
     left(m_src.at[pl.ds(0, NZ - 1)], MIX)
+    left(v_src.at[pl.ds(0, NZ - 1)], VG)
     left(nb.at[pl.ds(0, NZ - 1)], NRM)
     left(rs2_src.at[pl.ds(0, NZ - 1)], RS2)
     left(gu_src.at[pl.ds(0, NY - 1)], GU1)
@@ -375,10 +380,20 @@
     y_left(wo, WO)
     y_left(gu2, GU2)
     y_left(d2, D2)
+    arrived(pr3_rcv.at[pl.ds(0, PLANE - 1)], PR3)
+    pieces = []
+    for p in range(NY):
+        total = jnp.sum(pr3_rcv[NT * p : NT * (p + 1)].astype(F32), axis=0)
+        base = pltpu.roll(pr3_rcv[NT * p].astype(F32), 64, 1)
+        pieces.append((base + 0.5 * total).astype(BF))
+    final = dot(jnp.concatenate(pieces, axis=1), place[...], 1, 0)
+    out[...] = final.astype(BF)
+    left(pr3_src.at[pl.ds(0, PLANE - 1)], PR3)
 
 
 def deliver(out_in, state_in, out, state_out, sems):
-    copies = [pltpu.make_async_copy(out_in, out, sems.at[0]), pltpu.make_async_copy(state_in, state_out, sems.at[1])]
+    copies = [pltpu.make_async_copy(state_in.at[i], state_out.at[i], sems.at[i]) for i in range(8)]
+    copies.append(pltpu.make_async_copy(out_in, out, sems.at[8]))
     for copy in copies:
         copy.start()
     for copy in copies:
@@ -407,7 +422,7 @@
             pltpu.SemaphoreType.DMA((N_SEM,)),
             pltpu.VMEM((NY, 64, 2 * PITCH), BF),
             pltpu.VMEM((NY, 64, 2 * PITCH), BF),
-            pltpu.VMEM((NY, 24, 64), F32),
+            pltpu.VMEM((NY, 8, 64), F32),
             pltpu.VMEM((NY, 64, FFP), BF),
             pltpu.VMEM((NY, 64, MCOLS), BF),
             pltpu.VMEM((NY, 64, 512), BF),
@@ -422,8 +437,10 @@
             pltpu.VMEM((2, 2, 4, 8, ROWS), BF),
             pltpu.VMEM((2, 4, 8, ROWS), BF),
             pltpu.VMEM((2, NT, 4, 8, ROWS), BF),
-            pltpu.VMEM((NZ, 8, MCOLS), BF),
-            pltpu.VMEM((NZ, 8, MCOLS), BF),
+            pltpu.VMEM((NZ, 8, QK), BF),
+            pltpu.VMEM((NZ, 8, QK), BF),
+            pltpu.VMEM((NZ, 8, 1024), BF),
+            pltpu.VMEM((NZ, 8, 1024), BF),
             pltpu.VMEM((NZ, 8, 512), BF),
             pltpu.VMEM((NZ, 8, 2 * FFP), BF),
             pltpu.VMEM((NZ, 8, 2 * FFP), BF),
@@ -438,7 +455,7 @@
         out_shape=shapes,
         in_specs=[vmem, vmem],
         out_specs=(hbm, hbm),
-        scratch_shapes=[pltpu.SemaphoreType.DMA((2,))],
+        scratch_shapes=[pltpu.SemaphoreType.DMA((9,))],
         compiler_params=pltpu.CompilerParams(vmem_limit_bytes=40 << 20),
     )(out, new_state)
     return out.T, new_state

time: 72.8 us -> 71.5 us (0.982)
  Pallas kernels: 72 us -> 70.7 us
    pallas_call x1, Pallas kernels: 70.6 us -> 69.3 us  [layer(): pl.pallas_call(kernel, out_shape=(pltpu.VMEM((8, ROWS), BF), pltpu.VMEM(s...]
where the time goes in v7:
time: 71.5 us; the launch traced here: 71.3 us
  Pallas kernels  70.7 us (99%)
    pallas_call x1, Pallas kernels, layer(): pl.pallas_call(kernel, out_shape=(pltpu.VMEM((8, ROWS), BF), pltpu.VMEM(s...  69.3 us

profile of v7, /device:TPU:1, one launch (start us, length us, event | category | flops | bytes accessed | tf_op | source)
XLA Modules:
  0.0 71.3 jit_solution(16210506997869771967)
XLA Ops:
  0.6 69.3 %shard_map.212 = (bf16[8,256]{1,0:T(8,128)(2,1)S(1)}, f32[8,4,128,128]{3,2,1,0:T(8,128)S(1)}) custom-call(bf16[8,256]{1,0:T(8,128)(2,1)} %bitcast.18, f32[8,4,128,128]{3,2,1,0:T(8,128)} %state.1, f32[1,64]{1,0:T(1,128)} %bitcast.19, f32[1,64]{1,0:T(1,128)} %bitcast.20, f32[1,64]{1,0:T(1,128)} %bitcast.21, bf16[64,704]{1,0:T(8,128)(2,1)} %gate1_h.1, ...), custom_call_target="tpu_custom_call" | custom-call | tf_op jit(solution)/shard_map/pallas_call | solution.py:413
  70.0 1.4 %shard_map.213 = (bf16[8,256]{1,0:T(8,128)(2,1)}, f32[8,4,128,128]{3,2,1,0:T(8,128)}) custom-call(bf16[8,256]{1,0:T(8,128)(2,1)S(1)} %get-tuple-element.6.out_in, f32[8,4,128,128]{3,2,1,0:T(8,128)S(1)} %get-tuple-element.7.state_in), custom_call_target="tpu_custom_call" | custom-call | tf_op jit(solution)/shard_map/pallas_call | solution.py:453

commit v8 on v7

--- a/solution.py
+++ b/solution.py
@@ -15,11 +15,10 @@
 HID, PITCH = 176, 192
 HEAD = 128
 
-X1, X2, X3, RS1, RS2, AG1, AG2, PR1, PR2, PR3, MIX, VG, NRM, GU1, GN = range(15)
-D1, MW, WO, GU2, D2 = 15, 19, 23, 27, 31
-N_SEM = 35
-MCOLS = 1664
-QK = 640
+X1, X2, X3, RS1, RS2, AG1, AG2, PR1, PR2, PR3, MIX, VG, NRM, GU1, GN, SQ = range(16)
+D1, MW, WO, GU2, D2, MV = 16, 20, 24, 28, 32, 36
+N_SEM = 40
+QK, VGC = 640, 1024
 FFT, FFP = 704, 768
 RING_Z = (4, 3, 5, 2, 6, 1, 7)
 FAR, FAR_Z = (0, 1, 2, 1), (0, 1, 2, 3, 4, 3, 2, 1)
@@ -45,11 +44,11 @@
     res_h, state, gain1_h, gain2_h, gain3_h, gate1_h, up1_h, down1_h, gate2_h, up2_h, down2_h,
     wq_h, wk_h, wv_h, wg_h, wbeta_h, wdecay_h, rate_h, bias_h, hgain_h, wo_h,
     out, state_out,
-    res, s_buf, gain1, gain2, gain3, gate1, up1, down1, wbeta, wdecay, rate, bias, hgain,
+    res, s_buf, gain1, gain2, gain3, gate1, up1, down1, gate2, up2, wbeta, wdecay, rate, bias, hgain,
     in_sem, send, recv,
-    gu_src, gu_rcv, gn, d1, mw, wo, gu2, d2,
+    gu_src, gu_rcv, gn, d1, mw, mv, wo, gu2, d2,
     g_row, xrow, xg, f_src, f_rcv, hg, pa_src, pa_rcv, pb,
-    m_src, m_rcv, v_src, v_rcv, nb, rs2_src, rs2_rcv, pr3_src, pr3_rcv, place,
+    m_src, m_rcv, v_src, v_rcv, nb, sq_src, sq_rcv, rs2_src, rs2_rcv, pr3_src, pr3_rcv,
 ):
     kv = lax.axis_index("kv")
     t = lax.axis_index("tp")
@@ -73,8 +72,8 @@
     inputs = (
         (gate1_h, gate1), (up1_h, up1), (res_h, res), (gain1_h, gain1), (gain2_h, gain2), (gain3_h, gain3), (down1_h, down1),
         (wbeta_h, wbeta), (wdecay_h, wdecay),
-        (wq_h, mw.at[y, :, 0:256]), (wk_h, mw.at[y, :, 256:512]), (wv_h, mw.at[y, :, 640:1152]), (wg_h, mw.at[y, :, 1152:MCOLS]),
-        (wo_h, wo.at[y]), (gate2_h, gu2.at[y, 0]), (up2_h, gu2.at[y, 1]), (down2_h, d2.at[y]),
+        (wq_h, mw.at[y, :, 0:256]), (wk_h, mw.at[y, :, 256:512]), (wv_h, mv.at[y, :, 0:512]), (wg_h, mv.at[y, :, 512:VGC]),
+        (wo_h, wo.at[y]), (gate2_h, gate2), (up2_h, up2), (down2_h, d2.at[y]),
         (rate_h, rate), (bias_h, bias), (hgain_h, hgain), (state, s_buf),
     )
     named = {id(src): pltpu.make_async_copy(src, dst, in_sem.at[i]) for i, (src, dst) in enumerate(inputs)}
@@ -210,10 +209,12 @@
     f_src[...] = part.reshape(KV, 8, 2 * PITCH).astype(BF)
     deal(f_src, f_rcv, kv, RS1, kv_peers)
     y_start(d1, D1)
-    ready(wq_h, wk_h, wv_h, wg_h)
+    ready(wq_h, wk_h)
     y_start(mw, MW)
     xrow[...] = x0.reshape(NZ, NY, 8, ROWS).astype(BF)
     y_pass(d1, D1)
+    ready(wv_h, wg_h)
+    y_start(mv, MV)
     arrived(f_rcv.at[pl.ds(0, KV - 1)], RS1)
     quarters = jnp.sum(f_rcv[...].astype(F32).reshape(NZ, NY, 8, 2 * PITCH), axis=0)
     scale = lax.rsqrt((quarters[0, :, HID : HID + 1] + quarters[0, :, HID + 1 : HID + 2]) / D + EPS)
@@ -232,10 +233,11 @@
         arrived(hg.at[i, pl.ds(0, NZ - 1)], k)
         return hg[i].astype(F32).reshape(64, FFP).astype(BF)
 
-    def swap(part, i, k):
+    def swap(part, i, k, between):
         pa_src[i] = part.reshape(2, 4, 8, ROWS).astype(BF)
         put(pa_src.at[i, 1 - core], pa_rcv.at[i], k, (kv, ts[0][1]))
         mine = jnp.where(core == 0, part[0:32], part[32:64])
+        between()
         arrived(pa_rcv.at[i], k)
         pb[i, t] = (mine.reshape(4, 8, ROWS) + pa_rcv[i].astype(F32)).astype(BF)
 
@@ -250,7 +252,7 @@
         return jnp.concatenate(branch, axis=0)
 
     h = gathered_hidden(0, AG1)
-    swap(dot(h, d1[...].reshape(ROWS, FFP), 1, 1), 0, PR1)
+    swap(dot(h, d1[...].reshape(ROWS, FFP), 1, 1), 0, PR1, lambda: y_pass(mv, MV))
     share(pb.at[0], t, X2, t_peers)
     y_done(mw, MW)
     x1 = xrow[:, y].astype(F32).reshape(64, ROWS)
@@ -263,11 +265,13 @@
     part = part + jnp.where(last == 8, coarse, 0.0) + jnp.where(last == 9, fine, 0.0)
     m_src[:, :, 512:QK] = part.reshape(NZ, 8, 128).astype(BF)
     deal(m_src, m_rcv, z, MIX, z_peers)
-    part = dot(scaled, mw[:, :, QK:MCOLS].reshape(ROWS, 1024), 1, 0)
+    y_done(mv, MV)
+    part = dot(scaled, mv[...].reshape(ROWS, VGC), 1, 0)
     v_src[...] = part.reshape(NZ, 8, 1024).astype(BF)
     deal(v_src, v_rcv, z, VG, z_peers)
     ready(wo_h, gate2_h, up2_h, down2_h, state, rate_h, bias_h, hgain_h)
     y_start(wo, WO)
+    gu2[y] = jnp.concatenate([gate2[...].astype(F32), up2[...].astype(F32)], axis=1).astype(BF)
     y_start(gu2, GU2)
     arrived(m_rcv.at[pl.ds(0, NZ - 1)], MIX)
 
@@ -333,30 +337,28 @@
     arrived(nb.at[pl.ds(0, NZ - 1)], NRM)
     normed = nb[...].astype(F32).reshape(64, 512).astype(BF)
     part = dot(normed, wo[...].reshape(ROWS, 512), 1, 1)
-    swap(part, 1, PR2)
+    swap(part, 1, PR2, lambda: None)
     share(pb.at[1], t, X3, t_peers)
     y_done(gu2, GU2)
 
     x3 = (x1 + everyones(1, X3)).astype(BF).astype(F32)
     scaled, coarse, fine = scaled_of(x3, 2)
-    gate = dot(scaled, gu2[:, 0].reshape(ROWS, FFT), 1, 0)
-    up = dot(scaled, gu2[:, 1].reshape(ROWS, FFT), 1, 0)
-    fill = jnp.where(iota((64, 64), 1) == 0, coarse, jnp.where(iota((64, 64), 1) == 1, fine, 0.0))
-    rs2_src[:, :, 0:FFP] = jnp.concatenate([gate, fill], axis=1).reshape(NZ, 8, FFP).astype(BF)
-    rs2_src[:, :, FFP:] = jnp.concatenate([up, jnp.zeros((64, 64), F32)], axis=1).reshape(NZ, 8, FFP).astype(BF)
+    squares = jnp.where(last == 0, coarse, jnp.where(last == 1, fine, 0.0))
+    sq_src[...] = squares.reshape(NZ, 8, 128).astype(BF)
+    deal(sq_src, sq_rcv, z, SQ, z_peers)
+    part = dot(scaled, gu2[...].reshape(ROWS, 2 * FFT), 1, 0)
+    rs2_src[...] = part.reshape(NZ, 8, 2 * FFT).astype(BF)
     deal(rs2_src, rs2_rcv, z, RS2, z_peers)
     y_pass(d2, D2)
     x3_t = jnp.transpose(jnp.concatenate([jnp.zeros((64, ROWS), F32), x3], axis=0))
+    arrived(sq_rcv.at[pl.ds(0, NZ - 1)], SQ)
+    squares = jnp.sum(sq_rcv[...].astype(F32), axis=0)
+    scale = lax.rsqrt((squares[:, 0:1] + squares[:, 1:2]) / D + EPS)
     arrived(rs2_rcv.at[pl.ds(0, NZ - 1)], RS2)
-    both = jnp.sum(rs2_rcv[...].astype(F32), axis=0)
-    gate, up = both[:, 0:FFP], both[:, FFP:]
-    scale = lax.rsqrt((gate[:, FFT : FFT + 1] + gate[:, FFT + 1 : FFT + 2]) / D + EPS)
-    hidden = silu(gate * scale) * (up * scale)
-    hg[1, z] = jnp.where(iota((8, FFP), 1) < FFT, hidden, 0.0).astype(BF)
+    both = jnp.sum(rs2_rcv[...].astype(F32), axis=0) * scale
+    hidden = silu(both[:, 0:FFT]) * both[:, FFT:]
+    hg[1, z] = jnp.concatenate([hidden, jnp.zeros((8, FFP - FFT), F32)], axis=1).astype(BF)
     share(hg.at[1], z, AG2, z_peers)
-    l, b = iota((128, ROWS), 0), iota((128, ROWS), 1)
-    for p in range(NY):
-        place[128 * p : 128 * (p + 1)] = one_hot((b == l + 24 * lax.shift_right_logical(l, 3) + 8 * p) & (l < 64))
     y_done(d2, D2)
     h = gathered_hidden(1, AG2)[:, 0:FFT]
     h = jnp.concatenate([h, jnp.zeros((64, FFT), BF)], axis=0)
@@ -377,25 +379,31 @@
     left(gn.at[pl.ds(0, NY - 1)], GN)
     y_left(d1, D1)
     y_left(mw, MW)
+    y_left(mv, MV)
+    left(sq_src.at[pl.ds(0, NZ - 1)], SQ)
     y_left(wo, WO)
     y_left(gu2, GU2)
     y_left(d2, D2)
     arrived(pr3_rcv.at[pl.ds(0, PLANE - 1)], PR3)
-    pieces = []
     for p in range(NY):
         total = jnp.sum(pr3_rcv[NT * p : NT * (p + 1)].astype(F32), axis=0)
         base = pltpu.roll(pr3_rcv[NT * p].astype(F32), 64, 1)
-        pieces.append((base + 0.5 * total).astype(BF))
-    final = dot(jnp.concatenate(pieces, axis=1), place[...], 1, 0)
-    out[...] = final.astype(BF)
+        out[:, 128 * p : 128 * (p + 1)] = (base + 0.5 * total).astype(BF)
     left(pr3_src.at[pl.ds(0, PLANE - 1)], PR3)
 
 
-def deliver(out_in, state_in, out, state_out, sems):
+def deliver(out_in, state_in, out, state_out, placed, sems):
     copies = [pltpu.make_async_copy(state_in.at[i], state_out.at[i], sems.at[i]) for i in range(8)]
-    copies.append(pltpu.make_async_copy(out_in, out, sems.at[8]))
     for copy in copies:
         copy.start()
+    line, b = iota((128, ROWS), 0), iota((128, ROWS), 1)
+    final = jnp.zeros((8, ROWS), F32)
+    for p in range(NY):
+        place = one_hot((b == line + 24 * lax.shift_right_logical(line, 3) + 8 * p) & (line < 64))
+        final = final + dot(out_in[:, 128 * p : 128 * (p + 1)], place, 1, 0)
+    placed[...] = final.astype(BF)
+    copies.append(pltpu.make_async_copy(placed, out, sems.at[8]))
+    copies[-1].start()
     for copy in copies:
         copy.wait()
 
@@ -407,12 +415,12 @@
         wq, wk, wv, wg, wbeta.T, wdecay.T, rate[None], bias[None], hgain[None], wo.T,
     )
     args = tuple(pltpu.with_memory_space_constraint(a, pltpu.HBM) for a in args)
-    held = [args[i] for i in (0, 1, 2, 3, 4, 5, 6, 7, 15, 16, 17, 18, 19)]
+    held = [args[i] for i in (0, 1, 2, 3, 4, 5, 6, 7, 8, 9, 15, 16, 17, 18, 19)]
     hbm = pl.BlockSpec(memory_space=pltpu.HBM)
     shapes = (jax.ShapeDtypeStruct((8, ROWS), BF), jax.ShapeDtypeStruct(state.shape, F32))
     out, new_state = pl.pallas_call(
         kernel,
-        out_shape=(pltpu.VMEM((8, ROWS), BF), pltpu.VMEM(state.shape, F32)),
+        out_shape=(pltpu.VMEM((8, NY * 128), BF), pltpu.VMEM(state.shape, F32)),
         in_specs=[hbm] * len(args),
         out_specs=(vmem, vmem),
         scratch_shapes=[pltpu.VMEM(a.shape, a.dtype) for a in held]
@@ -424,9 +432,10 @@
             pltpu.VMEM((NY, 64, 2 * PITCH), BF),
             pltpu.VMEM((NY, 8, 64), F32),
             pltpu.VMEM((NY, 64, FFP), BF),
-            pltpu.VMEM((NY, 64, MCOLS), BF),
+            pltpu.VMEM((NY, 64, QK), BF),
+            pltpu.VMEM((NY, 64, VGC), BF),
             pltpu.VMEM((NY, 64, 512), BF),
-            pltpu.VMEM((NY, 2, 64, FFT), BF),
+            pltpu.VMEM((NY, 64, 2 * FFT), BF),
             pltpu.VMEM((NY, 64, FFT), BF),
             pltpu.VMEM((3, 8, ROWS), F32),
             pltpu.VMEM((NZ, NY, 8, ROWS), BF),
@@ -442,11 +451,12 @@
             pltpu.VMEM((NZ, 8, 1024), BF),
             pltpu.VMEM((NZ, 8, 1024), BF),
             pltpu.VMEM((NZ, 8, 512), BF),
-            pltpu.VMEM((NZ, 8, 2 * FFP), BF),
-            pltpu.VMEM((NZ, 8, 2 * FFP), BF),
+            pltpu.VMEM((NZ, 8, 128), BF),
+            pltpu.VMEM((NZ, 8, 128), BF),
+            pltpu.VMEM((NZ, 8, 2 * FFT), BF),
+            pltpu.VMEM((NZ, 8, 2 * FFT), BF),
             pltpu.VMEM((PLANE, 8, 128), BF),
             pltpu.VMEM((PLANE, 8, 128), BF),
-            pltpu.VMEM((NY * 128, ROWS), BF),
         ],
         compiler_params=pltpu.CompilerParams(collective_id=0, has_side_effects=True, vmem_limit_bytes=40 << 20),
     )(*args)
@@ -455,7 +465,7 @@
         out_shape=shapes,
         in_specs=[vmem, vmem],
         out_specs=(hbm, hbm),
-        scratch_shapes=[pltpu.SemaphoreType.DMA((9,))],
+        scratch_shapes=[pltpu.VMEM((8, ROWS), BF), pltpu.SemaphoreType.DMA((9,))],
         compiler_params=pltpu.CompilerParams(vmem_limit_bytes=40 << 20),
     )(out, new_state)
     return out.T, new_state

time: 71.5 us -> 71 us (level)
  no operation moved by 1% of the time
where the time goes in v8:
time: 71 us; the launch traced here: 70.9 us
  Pallas kernels  70.2 us (99%)
    pallas_call x1, Pallas kernels, layer(): pl.pallas_call(kernel, out_shape=(pltpu.VMEM((8, NY * 128), BF), pltpu.VM...  68.8 us

profile of v8, /device:TPU:1, one launch (start us, length us, event | category | flops | bytes accessed | tf_op | source)
XLA Modules:
  0.0 70.9 jit_solution(17271072231074370443)
XLA Ops:
  0.6 68.8 %shard_map.212 = (bf16[8,512]{1,0:T(8,128)(2,1)S(1)}, f32[8,4,128,128]{3,2,1,0:T(8,128)S(1)}) custom-call(bf16[8,256]{1,0:T(8,128)(2,1)} %bitcast.18, f32[8,4,128,128]{3,2,1,0:T(8,128)} %state.1, f32[1,64]{1,0:T(1,128)} %bitcast.19, f32[1,64]{1,0:T(1,128)} %bitcast.20, f32[1,64]{1,0:T(1,128)} %bitcast.21, bf16[64,704]{1,0:T(8,128)(2,1)} %gate1_h.1, ...), custom_call_target="tpu_custom_call" | custom-call | tf_op jit(solution)/shard_map/pallas_call | solution.py:421
  69.5 1.4 %shard_map.213 = (bf16[8,256]{1,0:T(8,128)(2,1)}, f32[8,4,128,128]{3,2,1,0:T(8,128)}) custom-call(bf16[8,512]{1,0:T(8,128)(2,1)S(1)} %get-tuple-element.6.out_in, f32[8,4,128,128]{3,2,1,0:T(8,128)S(1)} %get-tuple-element.7.state_in), custom_call_target="tpu_custom_call" | custom-call | tf_op jit(solution)/shard_map/pallas_call | solution.py:463

commit v9 on v8

--- a/solution.py
+++ b/solution.py
@@ -16,10 +16,12 @@
 HEAD = 128
 
 X1, X2, X3, RS1, RS2, AG1, AG2, PR1, PR2, PR3, MIX, VG, NRM, GU1, GN, SQ = range(16)
-D1, MW, WO, GU2, D2, MV = 16, 20, 24, 28, 32, 36
-N_SEM = 40
+D1, MW, WO, GU2, D2, MV = range(16, 28, 2)
+TILES, GAINS, DOWN2 = range(3)
+I_W1, I_RES, I_GAIN, I_DOWN, I_BD, I_QK, I_VG, I_WO, I_W2, I_D2, I_RB, I_HEAD, I_STATE = range(13)
 QK, VGC = 640, 1024
 FFT, FFP = 704, 768
+SENT = 31 * 2 + 3 * 24 + 31 * 3 + 14 * 6 + 2 * 8 + 14 * 8 + 7 * (5 + 8 + 4 + 1 + 11) + 31 + 3 * 8 * (6 + 5 + 8 + 4 + 11)
 RING_Z = (4, 3, 5, 2, 6, 1, 7)
 FAR, FAR_Z = (0, 1, 2, 1), (0, 1, 2, 3, 4, 3, 2, 1)
 
@@ -44,8 +46,8 @@
     res_h, state, gain1_h, gain2_h, gain3_h, gate1_h, up1_h, down1_h, gate2_h, up2_h, down2_h,
     wq_h, wk_h, wv_h, wg_h, wbeta_h, wdecay_h, rate_h, bias_h, hgain_h, wo_h,
     out, state_out,
-    res, s_buf, gain1, gain2, gain3, gate1, up1, down1, gate2, up2, wbeta, wdecay, rate, bias, hgain,
-    in_sem, send, recv,
+    res, s_buf, gains, w1, w2, bd, rb, hgain,
+    in_sem, send, recv, tiles,
     gu_src, gu_rcv, gn, d1, mw, mv, wo, gu2, d2,
     g_row, xrow, xg, f_src, f_rcv, hg, pa_src, pa_rcv, pb,
     m_src, m_rcv, v_src, v_rcv, nb, sq_src, sq_rcv, rs2_src, rs2_rcv, pr3_src, pr3_rcv,
@@ -70,29 +72,45 @@
     plane_peers = [(ys[dy] * NT + ts[dx][dc], (z * NY + ys[dy], ts[dx][dc])) for dy, dx, dc in plane]
 
     inputs = (
-        (gate1_h, gate1), (up1_h, up1), (res_h, res), (gain1_h, gain1), (gain2_h, gain2), (gain3_h, gain3), (down1_h, down1),
-        (wbeta_h, wbeta), (wdecay_h, wdecay),
-        (wq_h, mw.at[y, :, 0:256]), (wk_h, mw.at[y, :, 256:512]), (wv_h, mv.at[y, :, 0:512]), (wg_h, mv.at[y, :, 512:VGC]),
-        (wo_h, wo.at[y]), (gate2_h, gate2), (up2_h, up2), (down2_h, d2.at[y]),
-        (rate_h, rate), (bias_h, bias), (hgain_h, hgain), (state, s_buf),
+        (I_W1, w1.at[pl.ds(0, 2)], (gate1_h, w1.at[0]), (up1_h, w1.at[1])),
+        (I_RES, res, (res_h, res)),
+        (I_GAIN, gains, (gain1_h, gains.at[0]), (gain2_h, gains.at[1]), (gain3_h, gains.at[2])),
+        (I_DOWN, w1.at[2], (down1_h, w1.at[2])),
+        (I_BD, bd, (wbeta_h, bd.at[0]), (wdecay_h, bd.at[1])),
+        (I_QK, mw.at[y, :, 0:512], (wq_h, mw.at[y, :, 0:256]), (wk_h, mw.at[y, :, 256:512])),
+        (I_VG, mv.at[y], (wv_h, mv.at[y, :, 0:512]), (wg_h, mv.at[y, :, 512:VGC])),
+        (I_WO, wo.at[y], (wo_h, wo.at[y])),
+        (I_W2, w2, (gate2_h, w2.at[0]), (up2_h, w2.at[1])),
+        (I_D2, d2.at[y], (down2_h, d2.at[y])),
+        (I_RB, rb, (rate_h, rb.at[0]), (bias_h, rb.at[1])),
+        (I_HEAD, hgain, (hgain_h, hgain)),
+        (I_STATE, s_buf, (state, s_buf)),
     )
-    named = {id(src): pltpu.make_async_copy(src, dst, in_sem.at[i]) for i, (src, dst) in enumerate(inputs)}
-    early = 6
-    for src, _ in inputs[:early]:
-        named[id(src)].start()
+
+    def fetch(groups):
+        for i, _, *copies in groups:
+            for src, dst in copies:
+                pltpu.make_async_copy(src, dst, in_sem.at[i]).start()
+
+    def ready(*groups):
+        for i in groups:
+            whole = inputs[i][1]
+            pltpu.make_async_copy(whole, whole, in_sem.at[i]).wait()
+
+    fetch(inputs[:3])
 
     barrier = pltpu.get_barrier_semaphore()
     greet = z_peers[:3] + plane_peers[:10] + z_peers[3:5] + plane_peers[10:] + z_peers[5:]
     for _, peer in greet:
         pl.semaphore_signal(barrier, inc=1, device_id=peer, device_id_type=MESH)
 
-    def ready(*refs):
-        for ref in refs:
-            named[id(ref)].wait()
-
-    def put(src, dst, k, peer):
+    counted = []
+
+    def put(src, dst, k, peer, by=TILES):
+        if by == TILES:
+            counted.append(src.size * src.dtype.itemsize)
         pltpu.make_async_remote_copy(
-            src_ref=src, dst_ref=dst, send_sem=send.at[k], recv_sem=recv.at[k], device_id=peer, device_id_type=MESH
+            src_ref=src, dst_ref=dst, send_sem=send.at[by], recv_sem=recv.at[k], device_id=peer, device_id_type=MESH
         ).start()
 
     def arrived(part, k):
@@ -101,9 +119,9 @@
     def left(part, k):
         pltpu.make_async_copy(part, part, send.at[k]).wait()
 
-    def share(buf, own, k, peers):
+    def share(buf, own, k, peers, by=TILES):
         for _, peer in peers:
-            put(buf.at[own], buf.at[own], k, peer)
+            put(buf.at[own], buf.at[own], k, peer, by)
 
     def deal(src, dst, own, k, peers):
         for p, peer in peers:
@@ -112,33 +130,23 @@
 
     above, below = (z * NY + ys[1], t), (z * NY + ys[3], t)
 
-    def y_start(buf, k):
-        put(buf.at[y], buf.at[y], k, above)
-        put(buf.at[y], buf.at[y], k + 1, below)
+    def y_start(buf, k, by=TILES):
+        put(buf.at[y], buf.at[y], k, above, by)
+        put(buf.at[y], buf.at[y], k, below, by)
 
     def halves(buf, p):
         n = buf.shape[1] // 2
         return buf.at[p, pl.ds(0, n)], buf.at[p, pl.ds(n, n)]
 
-    def y_pass(buf, k):
-        arrived(buf.at[ys[3]], k)
-        first, second = halves(buf, ys[3])
-        put(first, first, k + 2, above)
-        arrived(buf.at[ys[1]], k + 1)
-        first, second = halves(buf, ys[1])
-        put(second, second, k + 3, below)
+    def y_pass(buf, k, by=TILES):
+        arrived(buf.at[pl.ds(0, 2)], k)
+        first, _ = halves(buf, ys[3])
+        put(first, first, k + 1, above, by)
+        _, second = halves(buf, ys[1])
+        put(second, second, k + 1, below, by)
 
     def y_done(buf, k):
-        first, second = halves(buf, ys[2])
-        arrived(first, k + 2)
-        arrived(second, k + 3)
-
-    def y_left(buf, k):
-        first, second = halves(buf, 0)
-        left(buf.at[0], k)
-        left(buf.at[0], k + 1)
-        left(first, k + 2)
-        left(second, k + 3)
+        arrived(buf.at[0], k + 1)
 
     lane = iota((64, FFP), 1)
     pos = lane - PITCH * sum(jnp.where(lane >= PITCH * p, 1, 0) for p in range(1, NY))
@@ -150,35 +158,34 @@
             w = jnp.where(lane >= PITCH * p, pltpu.roll(v, (PITCH - HID) * p, 1), w)
         return jnp.where(pos < HID, w, 0.0)
 
-    ready(gate1_h, up1_h)
-    gate, up = spread(gate1[...]), spread(up1[...])
+    ready(I_W1)
+    gate, up = spread(w1[0]), spread(w1[1])
     first = iota((64, 2 * PITCH), 1) < PITCH
     for h in range(2):
         a = gate[:, 2 * PITCH * h : 2 * PITCH * (h + 1)]
         b = pltpu.roll(up[:, 2 * PITCH * h : 2 * PITCH * (h + 1)], PITCH, 1)
         gu_src[2 * h] = jnp.where(first, a, b).astype(BF)
         gu_src[2 * h + 1] = jnp.where(first, b, a).astype(BF)
-    ready(res_h, gain1_h, gain2_h, gain3_h)
+    ready(I_RES, I_GAIN)
     xg[me] = res[...]
-    gn[y, 0:1] = gain1[...]
-    gn[y, 1:2] = gain2[...]
-    gn[y, 2:3] = gain3[...]
+    gn[y, 0:1] = gains[0]
+    gn[y, 1:2] = gains[1]
+    gn[y, 2:3] = gains[2]
 
     pl.semaphore_wait(barrier, len(greet))
 
-    share(gn, y, GN, y_peers)
+    share(gn, y, GN, y_peers, GAINS)
     share(xg, me, X1, plane_peers[:18])
     deal(gu_src, gu_rcv, y, GU1, y_peers)
     share(xg, me, X1, plane_peers[18:])
 
-    for src, _ in inputs[early:]:
-        named[id(src)].start()
-    ready(down1_h)
-    d1[y] = spread(down1[...]).astype(BF)
+    fetch(inputs[3:])
+    ready(I_DOWN)
+    d1[y] = spread(w1[2]).astype(BF)
     sel_b = one_hot((iota((32, 128), 0) == iota((32, 128), 1) + 4 * t) & (iota((32, 128), 1) < 4))
     sel_d = one_hot((iota((32, 128), 0) == iota((32, 128), 1) - 4 + 4 * t) & (iota((32, 128), 1) >= 4) & (iota((32, 128), 1) < 8))
-    ready(wbeta_h, wdecay_h)
-    mw[y, :, 512:QK] = (dot(wbeta[...], sel_b, 0, 0) + dot(wdecay[...], sel_d, 0, 0)).astype(BF)
+    ready(I_BD)
+    mw[y, :, 512:QK] = (dot(bd[0], sel_b, 0, 0) + dot(bd[1], sel_d, 0, 0)).astype(BF)
 
     eye64 = iota((64, 64), 0) == iota((64, 64), 1)
     lane64 = iota((64, 128), 1)
@@ -209,11 +216,11 @@
     f_src[...] = part.reshape(KV, 8, 2 * PITCH).astype(BF)
     deal(f_src, f_rcv, kv, RS1, kv_peers)
     y_start(d1, D1)
-    ready(wq_h, wk_h)
+    ready(I_QK)
     y_start(mw, MW)
     xrow[...] = x0.reshape(NZ, NY, 8, ROWS).astype(BF)
     y_pass(d1, D1)
-    ready(wv_h, wg_h)
+    ready(I_VG)
     y_start(mv, MV)
     arrived(f_rcv.at[pl.ds(0, KV - 1)], RS1)
     quarters = jnp.sum(f_rcv[...].astype(F32).reshape(NZ, NY, 8, 2 * PITCH), axis=0)
@@ -269,9 +276,9 @@
     part = dot(scaled, mv[...].reshape(ROWS, VGC), 1, 0)
     v_src[...] = part.reshape(NZ, 8, 1024).astype(BF)
     deal(v_src, v_rcv, z, VG, z_peers)
-    ready(wo_h, gate2_h, up2_h, down2_h, state, rate_h, bias_h, hgain_h)
+    ready(I_WO, I_W2, I_D2, I_RB, I_HEAD, I_STATE)
     y_start(wo, WO)
-    gu2[y] = jnp.concatenate([gate2[...].astype(F32), up2[...].astype(F32)], axis=1).astype(BF)
+    gu2[y] = jnp.concatenate([w2[0].astype(F32), w2[1].astype(F32)], axis=1).astype(BF)
     y_start(gu2, GU2)
     arrived(m_rcv.at[pl.ds(0, NZ - 1)], MIX)
 
@@ -303,9 +310,9 @@
     gates = []
     for h in range(4):
         beta = 1.0 / (1.0 + jnp.exp(-ext[:, h : h + 1]))
-        pre = ext[:, 4 + h : 5 + h] + bias[:, h : h + 1]
+        pre = ext[:, 4 + h : 5 + h] + rb[1, :, h : h + 1]
         soft = jnp.maximum(pre, 0.0) + jnp.log1p(jnp.exp(-jnp.abs(pre)))
-        decay = jnp.exp(-jnp.exp(rate[:, h : h + 1]) * soft)
+        decay = jnp.exp(-jnp.exp(rb[0, :, h : h + 1]) * soft)
         by_k[h] = decay * k_f[h // 2] * jnp.concatenate(by_k[h], axis=0)
         by_q[h] = decay * q_f[h // 2] * jnp.concatenate(by_q[h], axis=0)
         gates.append((beta, decay))
@@ -326,7 +333,7 @@
     share(nb, z, NRM, z_peers)
     y_pass(wo, WO)
     y_pass(gu2, GU2)
-    y_start(d2, D2)
+    y_start(d2, D2, DOWN2)
     for i in range(8):
         for m in range(2):
             k_col = jnp.broadcast_to(k_t[m][:, i : i + 1], (HEAD, HEAD))
@@ -349,7 +356,7 @@
     part = dot(scaled, gu2[...].reshape(ROWS, 2 * FFT), 1, 0)
     rs2_src[...] = part.reshape(NZ, 8, 2 * FFT).astype(BF)
     deal(rs2_src, rs2_rcv, z, RS2, z_peers)
-    y_pass(d2, D2)
+    y_pass(d2, D2, DOWN2)
     x3_t = jnp.transpose(jnp.concatenate([jnp.zeros((64, ROWS), F32), x3], axis=0))
     arrived(sq_rcv.at[pl.ds(0, NZ - 1)], SQ)
     squares = jnp.sum(sq_rcv[...].astype(F32), axis=0)
@@ -365,44 +372,27 @@
     part = dot(d2[...].reshape(ROWS, FFT), h, 1, 1) + x3_t
     pr3_src[...] = part.reshape(PLANE, 8, 128).astype(BF)
     deal(pr3_src, pr3_rcv, me, PR3, plane_peers)
-    left(xg.at[pl.ds(0, PLANE - 1)], X1)
-    left(f_src.at[pl.ds(0, KV - 1)], RS1)
-    for i, (ag, pr, xx) in enumerate(((AG1, PR1, X2), (AG2, PR2, X3))):
-        left(hg.at[i, pl.ds(0, NZ - 1)], ag)
-        left(pa_rcv.at[i], pr)
-        left(pb.at[i, pl.ds(0, NT - 1)], xx)
-    left(m_src.at[pl.ds(0, NZ - 1)], MIX)
-    left(v_src.at[pl.ds(0, NZ - 1)], VG)
-    left(nb.at[pl.ds(0, NZ - 1)], NRM)
-    left(rs2_src.at[pl.ds(0, NZ - 1)], RS2)
-    left(gu_src.at[pl.ds(0, NY - 1)], GU1)
-    left(gn.at[pl.ds(0, NY - 1)], GN)
-    y_left(d1, D1)
-    y_left(mw, MW)
-    y_left(mv, MV)
-    left(sq_src.at[pl.ds(0, NZ - 1)], SQ)
-    y_left(wo, WO)
-    y_left(gu2, GU2)
-    y_left(d2, D2)
     arrived(pr3_rcv.at[pl.ds(0, PLANE - 1)], PR3)
     for p in range(NY):
         total = jnp.sum(pr3_rcv[NT * p : NT * (p + 1)].astype(F32), axis=0)
         base = pltpu.roll(pr3_rcv[NT * p].astype(F32), 64, 1)
         out[:, 128 * p : 128 * (p + 1)] = (base + 0.5 * total).astype(BF)
-    left(pr3_src.at[pl.ds(0, PLANE - 1)], PR3)
+    assert sum(counted) == SENT * 2048, sum(counted) / 2048
+    left(tiles, TILES)
+    left(gn.at[pl.ds(0, NY - 1)], GAINS)
+    left(d2.at[pl.ds(0, NY - 1)], DOWN2)
 
 
 def deliver(out_in, state_in, out, state_out, placed, sems):
-    copies = [pltpu.make_async_copy(state_in.at[i], state_out.at[i], sems.at[i]) for i in range(8)]
-    for copy in copies:
-        copy.start()
+    copies = [pltpu.make_async_copy(state_in, state_out, sems.at[0])]
+    copies[0].start()
     line, b = iota((128, ROWS), 0), iota((128, ROWS), 1)
     final = jnp.zeros((8, ROWS), F32)
     for p in range(NY):
         place = one_hot((b == line + 24 * lax.shift_right_logical(line, 3) + 8 * p) & (line < 64))
         final = final + dot(out_in[:, 128 * p : 128 * (p + 1)], place, 1, 0)
     placed[...] = final.astype(BF)
-    copies.append(pltpu.make_async_copy(placed, out, sems.at[8]))
+    copies.append(pltpu.make_async_copy(placed, out, sems.at[1]))
     copies[-1].start()
     for copy in copies:
         copy.wait()
@@ -415,7 +405,6 @@
         wq, wk, wv, wg, wbeta.T, wdecay.T, rate[None], bias[None], hgain[None], wo.T,
     )
     args = tuple(pltpu.with_memory_space_constraint(a, pltpu.HBM) for a in args)
-    held = [args[i] for i in (0, 1, 2, 3, 4, 5, 6, 7, 8, 9, 15, 16, 17, 18, 19)]
     hbm = pl.BlockSpec(memory_space=pltpu.HBM)
     shapes = (jax.ShapeDtypeStruct((8, ROWS), BF), jax.ShapeDtypeStruct(state.shape, F32))
     out, new_state = pl.pallas_call(
@@ -423,11 +412,19 @@
         out_shape=(pltpu.VMEM((8, NY * 128), BF), pltpu.VMEM(state.shape, F32)),
         in_specs=[hbm] * len(args),
         out_specs=(vmem, vmem),
-        scratch_shapes=[pltpu.VMEM(a.shape, a.dtype) for a in held]
-        + [
-            pltpu.SemaphoreType.DMA((len(args),)),
-            pltpu.SemaphoreType.DMA((N_SEM,)),
-            pltpu.SemaphoreType.DMA((N_SEM,)),
+        scratch_shapes=[
+            pltpu.VMEM((8, ROWS), BF),
+            pltpu.VMEM(state.shape, F32),
+            pltpu.VMEM((3, 1, 64), F32),
+            pltpu.VMEM((3, 64, FFT), BF),
+            pltpu.VMEM((2, 64, FFT), BF),
+            pltpu.VMEM((2, 32, 64), BF),
+            pltpu.VMEM((2, 1, 4), F32),
+            pltpu.VMEM((1, HEAD), F32),
+            pltpu.SemaphoreType.DMA((13,)),
+            pltpu.SemaphoreType.DMA((3,)),
+            pltpu.SemaphoreType.DMA((28,)),
+            pltpu.VMEM((SENT, 8, 128), BF),
             pltpu.VMEM((NY, 64, 2 * PITCH), BF),
             pltpu.VMEM((NY, 64, 2 * PITCH), BF),
             pltpu.VMEM((NY, 8, 64), F32),
@@ -465,7 +462,7 @@
         out_shape=shapes,
         in_specs=[vmem, vmem],
         out_specs=(hbm, hbm),
-        scratch_shapes=[pltpu.VMEM((8, ROWS), BF), pltpu.SemaphoreType.DMA((9,))],
+        scratch_shapes=[pltpu.VMEM((8, ROWS), BF), pltpu.SemaphoreType.DMA((2,))],
         compiler_params=pltpu.CompilerParams(vmem_limit_bytes=40 << 20),
     )(out, new_state)
     return out.T, new_state

time: 71 us -> 70.8 us (level)
  no operation moved by 1% of the time
where the time goes in v9:
time: 70.8 us; the launch traced here: 70.7 us
  Pallas kernels  70 us (99%)
    pallas_call x1, Pallas kernels, layer(): pl.pallas_call(kernel, out_shape=(pltpu.VMEM((8, NY * 128), BF), pltpu.VM...  68.7 us

profile of v9, /device:TPU:1, one launch (start us, length us, event | category | flops | bytes accessed | tf_op | source)
XLA Modules:
  0.0 70.7 jit_solution(11740161443713617376)
XLA Ops:
  0.6 68.7 %shard_map.212 = (bf16[8,512]{1,0:T(8,128)(2,1)S(1)}, f32[8,4,128,128]{3,2,1,0:T(8,128)S(1)}) custom-call(bf16[8,256]{1,0:T(8,128)(2,1)} %bitcast.18, f32[8,4,128,128]{3,2,1,0:T(8,128)} %state.1, f32[1,64]{1,0:T(1,128)} %bitcast.19, f32[1,64]{1,0:T(1,128)} %bitcast.20, f32[1,64]{1,0:T(1,128)} %bitcast.21, bf16[64,704]{1,0:T(8,128)(2,1)} %gate1_h.1, ...), custom_call_target="tpu_custom_call" | custom-call | tf_op jit(solution)/shard_map/pallas_call | solution.py:410
  69.3 1.3 %shard_map.213 = (bf16[8,256]{1,0:T(8,128)(2,1)}, f32[8,4,128,128]{3,2,1,0:T(8,128)}) custom-call(bf16[8,512]{1,0:T(8,128)(2,1)S(1)} %get-tuple-element.6.out_in, f32[8,4,128,128]{3,2,1,0:T(8,128)S(1)} %get-tuple-element.7.state_in), custom_call_target="tpu_custom_call" | custom-call | tf_op jit(solution)/shard_map/pallas_call | solution.py:460

commit v10 on v9

--- a/solution.py
+++ b/solution.py
@@ -175,9 +175,8 @@
     pl.semaphore_wait(barrier, len(greet))
 
     share(gn, y, GN, y_peers, GAINS)
-    share(xg, me, X1, plane_peers[:18])
+    share(xg, me, X1, plane_peers)
     deal(gu_src, gu_rcv, y, GU1, y_peers)
-    share(xg, me, X1, plane_peers[18:])
 
     fetch(inputs[3:])
     ready(I_DOWN)

time: 70.8 us -> 70.2 us (level)
  no operation moved by 1% of the time
where the time goes in v10:
time: 70.2 us; the launch traced here: 70.1 us
  Pallas kernels  69.5 us (99%)
    pallas_call x1, Pallas kernels, layer(): pl.pallas_call(kernel, out_shape=(pltpu.VMEM((8, NY * 128), BF), pltpu.VM...  68.1 us

profile of v10, /device:TPU:1, one launch (start us, length us, event | category | flops | bytes accessed | tf_op | source)
XLA Modules:
  0.0 70.1 jit_solution(12006728577552762234)
XLA Ops:
  0.6 68.1 %shard_map.212 = (bf16[8,512]{1,0:T(8,128)(2,1)S(1)}, f32[8,4,128,128]{3,2,1,0:T(8,128)S(1)}) custom-call(bf16[8,256]{1,0:T(8,128)(2,1)} %bitcast.18, f32[8,4,128,128]{3,2,1,0:T(8,128)} %state.1, f32[1,64]{1,0:T(1,128)} %bitcast.19, f32[1,64]{1,0:T(1,128)} %bitcast.20, f32[1,64]{1,0:T(1,128)} %bitcast.21, bf16[64,704]{1,0:T(8,128)(2,1)} %gate1_h.1, ...), custom_call_target="tpu_custom_call" | custom-call | tf_op jit(solution)/shard_map/pallas_call | solution.py:409
  68.8 1.3 %shard_map.213 = (bf16[8,256]{1,0:T(8,128)(2,1)}, f32[8,4,128,128]{3,2,1,0:T(8,128)}) custom-call(bf16[8,512]{1,0:T(8,128)(2,1)S(1)} %get-tuple-element.6.out_in, f32[8,4,128,128]{3,2,1,0:T(8,128)S(1)} %get-tuple-element.7.state_in), custom_call_target="tpu_custom_call" | custom-call | tf_op jit(solution)/shard_map/pallas_call | solution.py:459

commit v11 on v10

--- a/solution.py
+++ b/solution.py
@@ -15,8 +15,8 @@
 HID, PITCH = 176, 192
 HEAD = 128
 
-X1, X2, X3, RS1, RS2, AG1, AG2, PR1, PR2, PR3, MIX, VG, NRM, GU1, GN, SQ = range(16)
-D1, MW, WO, GU2, D2, MV = range(16, 28, 2)
+X1, X2, X3, RS1, RS2, AG1, AG2, PR1, PR2, PR3, MIX, VG, NRM, GU1, GN, SQ, EXT = range(17)
+D1, MW, WO, GU2, D2, MV = range(17, 29, 2)
 TILES, GAINS, DOWN2 = range(3)
 I_W1, I_RES, I_GAIN, I_DOWN, I_BD, I_QK, I_VG, I_WO, I_W2, I_D2, I_RB, I_HEAD, I_STATE = range(13)
 QK, VGC = 640, 1024
@@ -50,7 +50,7 @@
     in_sem, send, recv, tiles,
     gu_src, gu_rcv, gn, d1, mw, mv, wo, gu2, d2,
     g_row, xrow, xg, f_src, f_rcv, hg, pa_src, pa_rcv, pb,
-    m_src, m_rcv, v_src, v_rcv, nb, sq_src, sq_rcv, rs2_src, rs2_rcv, pr3_src, pr3_rcv,
+    m_src, m_rcv, e_src, e_rcv, v_src, v_rcv, nb, sq_src, sq_rcv, rs2_src, rs2_rcv, pr3_src, pr3_rcv,
 ):
     kv = lax.axis_index("kv")
     t = lax.axis_index("tp")
@@ -265,11 +265,12 @@
     x1 = (x1 + 0.5 * everyones(0, X2)).astype(BF).astype(F32)
     scaled, coarse, fine = scaled_of(x1, 1)
     last = iota((64, 128), 1)
-    part = dot(scaled, mw[:, :, 0:512].reshape(ROWS, 512), 1, 0)
-    m_src[:, :, 0:512] = part.reshape(NZ, 8, 512).astype(BF)
     part = dot(scaled, mw[:, :, 512:QK].reshape(ROWS, 128), 1, 0)
     part = part + jnp.where(last == 8, coarse, 0.0) + jnp.where(last == 9, fine, 0.0)
-    m_src[:, :, 512:QK] = part.reshape(NZ, 8, 128).astype(BF)
+    e_src[...] = part.reshape(NZ, 8, 128).astype(BF)
+    deal(e_src, e_rcv, z, EXT, z_peers)
+    part = dot(scaled, mw[:, :, 0:512].reshape(ROWS, 512), 1, 0)
+    m_src[...] = part.reshape(NZ, 8, 512).astype(BF)
     deal(m_src, m_rcv, z, MIX, z_peers)
     y_done(mv, MV)
     part = dot(scaled, mv[...].reshape(ROWS, VGC), 1, 0)
@@ -279,11 +280,11 @@
     y_start(wo, WO)
     gu2[y] = jnp.concatenate([w2[0].astype(F32), w2[1].astype(F32)], axis=1).astype(BF)
     y_start(gu2, GU2)
+    arrived(e_rcv.at[pl.ds(0, NZ - 1)], EXT)
+    ext = jnp.sum(e_rcv[...].astype(F32), axis=0)
+    rowscale = lax.rsqrt((ext[:, 8:9] + ext[:, 9:10]) / D + EPS)
     arrived(m_rcv.at[pl.ds(0, NZ - 1)], MIX)
-
     mixed = jnp.sum(m_rcv[...].astype(F32), axis=0)
-    ext = mixed[:, 512:QK]
-    rowscale = lax.rsqrt((ext[:, 8:9] + ext[:, 9:10]) / D + EPS)
     heads = [mixed[:, 128 * i : 128 * (i + 1)] * rowscale for i in range(4)]
 
     def factor(v):
@@ -422,7 +423,7 @@
             pltpu.VMEM((1, HEAD), F32),
             pltpu.SemaphoreType.DMA((13,)),
             pltpu.SemaphoreType.DMA((3,)),
-            pltpu.SemaphoreType.DMA((28,)),
+            pltpu.SemaphoreType.DMA((29,)),
             pltpu.VMEM((SENT, 8, 128), BF),
             pltpu.VMEM((NY, 64, 2 * PITCH), BF),
             pltpu.VMEM((NY, 64, 2 * PITCH), BF),
@@ -442,8 +443,10 @@
             pltpu.VMEM((2, 2, 4, 8, ROWS), BF),
             pltpu.VMEM((2, 4, 8, ROWS), BF),
             pltpu.VMEM((2, NT, 4, 8, ROWS), BF),
-            pltpu.VMEM((NZ, 8, QK), BF),
-            pltpu.VMEM((NZ, 8, QK), BF),
+            pltpu.VMEM((NZ, 8, 512), BF),
+            pltpu.VMEM((NZ, 8, 512), BF),
+            pltpu.VMEM((NZ, 8, 128), BF),
+            pltpu.VMEM((NZ, 8, 128), BF),
             pltpu.VMEM((NZ, 8, 1024), BF),
             pltpu.VMEM((NZ, 8, 1024), BF),
             pltpu.VMEM((NZ, 8, 512), BF),

time: 70.2 us -> 70.4 us (level)
  no operation moved by 1% of the time
where the time goes in v11:
time: 70.4 us; the launch traced here: 70.3 us
  Pallas kernels  69.7 us (99%)
    pallas_call x1, Pallas kernels, layer(): pl.pallas_call(kernel, out_shape=(pltpu.VMEM((8, NY * 128), BF), pltpu.VM...  68.3 us

profile of v11, /device:TPU:1, one launch (start us, length us, event | category | flops | bytes accessed | tf_op | source)
XLA Modules:
  0.0 70.3 jit_solution(12214382765326888975)
XLA Ops:
  0.6 68.3 %shard_map.212 = (bf16[8,512]{1,0:T(8,128)(2,1)S(1)}, f32[8,4,128,128]{3,2,1,0:T(8,128)S(1)}) custom-call(bf16[8,256]{1,0:T(8,128)(2,1)} %bitcast.18, f32[8,4,128,128]{3,2,1,0:T(8,128)} %state.1, f32[1,64]{1,0:T(1,128)} %bitcast.19, f32[1,64]{1,0:T(1,128)} %bitcast.20, f32[1,64]{1,0:T(1,128)} %bitcast.21, bf16[64,704]{1,0:T(8,128)(2,1)} %gate1_h.1, ...), custom_call_target="tpu_custom_call" | custom-call | tf_op jit(solution)/shard_map/pallas_call | solution.py:410
  69.0 1.3 %shard_map.213 = (bf16[8,256]{1,0:T(8,128)(2,1)}, f32[8,4,128,128]{3,2,1,0:T(8,128)}) custom-call(bf16[8,512]{1,0:T(8,128)(2,1)S(1)} %get-tuple-element.6.out_in, f32[8,4,128,128]{3,2,1,0:T(8,128)S(1)} %get-tuple-element.7.state_in), custom_call_target="tpu_custom_call" | custom-call | tf_op jit(solution)/shard_map/pallas_call | solution.py:462
